TPU v7x, 256 devices: a whole 4x4x8 slice. The times are simulated.
256 devices in a mesh: ep: 32 (over z, x), tp: 8 (over y, core).
Axes of the slice: x: 4, y: 4, z: 8, core: 2. Of those that a mesh axis runs over, the one named last changes fastest.
Arguments:
- tokens: bfloat16 [512, 2048], P('ep'), may hold values from -6 to 6
- attn_gain: float32 [2048], replicated, may hold values from 0.1 to 1.9
- w_query: bfloat16 [2048, 1024], P(None, 'tp'), may hold values from -0.125 to 0.125
- stick_bias: float32 [16], P('tp'), may hold values from -8.5 to -2.5
- kv_cache: bfloat16 [512, 8, 1024, 128], P('ep', 'tp'), may hold values from -6 to 6
- lengths: int32 [512], P('ep'), may hold values from 1 to 1024, as said below
- head_gain: float32 [1024], P('tp'), may hold values from 0.1 to 1.9
- w_attn_out: bfloat16 [1024, 2048], P('tp'), may hold values from -0.1875 to 0.1875
- ffn_gain: float32 [2048], replicated, may hold values from 0.1 to 1.9
- route_expert: int32 [512, 2], P('ep'), may hold values from 0 to 31, as said below
- route_weight: bfloat16 [512, 2], P('ep'), may hold values from 0.049804688 to 1
- w_exp_gate: bfloat16 [32, 2048, 2048], P('ep', None, 'tp'), may hold values from -0.125 to 0.125
- w_exp_up: bfloat16 [32, 2048, 2048], P('ep', None, 'tp'), may hold values from -0.125 to 0.125
- w_exp_down: bfloat16 [32, 2048, 2048], P('ep', 'tp'), may hold values from -0.125 to 0.125
- branch_gate: bfloat16 [2048], replicated, may hold values from -0.125 to 0.125
- w_dense_gate: bfloat16 [8192, 2048], P(('ep', 'tp')), may hold values from -0.125 to 0.125
- w_dense_up: bfloat16 [8192, 2048], P(('ep', 'tp')), may hold values from -0.125 to 0.125
- w_dense_down: bfloat16 [8192, 2048], P(('ep', 'tp')), may hold values from -0.25 to 0.25
Outputs:
- mixed: bfloat16 [512, 2048], P('ep', 'tp')
Inputs may be any that keep to these rules, and one draw needn't show every extreme that they name: `route_expert`: each row names 2 different experts of one group (expert x lies in group x // 8). The rows of one index of ep name no expert more than 2 times; one group, the same for every index of ep, has each of its experts named exactly 2 times by the rows of every index of ep. `lengths`: some sequence has length 1024.
All inputs are finite; a program needn't handle non-finite values.
Results may differ from a plain program's by a relative error of at most 0.0076.
Values may be sent and summed in bfloat16 or wider, within the bound.
No kernel may reach another device: no remote copies, remote signals or barrier semaphores. Data moves between devices by JAX's collectives and lax.ppermute only.
A program may use at most 64 MiB of HBM per device.

v0:
```python
import math

import jax
import jax.numpy as jnp
from jax import lax
from jax.sharding import PartitionSpec as P

HEADS = 16
HEAD = 64
KV_HEADS = 8
EXPERTS = 32
CAP = 2


epsilon = 1e-06
highest = lax.Precision.HIGHEST


def sent_together(arrays, axis, dim, along):
    ends, at = ([], 0)
    for a in arrays[:-1]:
        at += a.shape[along]
        ends.append(at)
    both = jnp.concatenate(arrays, axis=along)
    return tuple(jnp.split(lax.all_gather(both, axis, axis=dim, tiled=True), ends, axis=along))


def in_blocks(x, dim, size):
    before, after = (x.shape[:dim], x.shape[dim + 1 :])
    return jnp.moveaxis(x.reshape(*before, size, -1, *after), dim, 0)


def summed_on_arrival(x, axis, dim):
    size = lax.axis_size(axis)
    blocks = lax.all_to_all(in_blocks(x, dim, size), axis, 0, 0, tiled=True)
    return jnp.sum(blocks.astype(jnp.float32), axis=0)


def copy_for_each(x, axis):
    size = lax.axis_size(axis)
    return lax.all_to_all(jnp.broadcast_to(x[None], (size, *x.shape)), axis, 0, 0, tiled=True)


def taken_together(x, axis):
    return copy_for_each(x, axis).astype(jnp.float32).sum(axis=0)


def sent_together_2(arrays, axis, dim, along):
    widths = [math.prod(a.shape[along:]) for a in arrays]
    both = jnp.concatenate(
        [a.reshape(*a.shape[:along], w) for a, w in zip(arrays, widths)], axis=along
    )
    result = lax.all_gather(both, axis, axis=dim, tiled=True)
    blocks = jnp.split(result, [sum(widths[:k]) for k in range(1, len(widths))], axis=along)
    return tuple(
        (b.reshape(*result.shape[:along], *a.shape[along:]) for a, b in zip(arrays, blocks))
    )


def rms_scale(matrix, gain):
    wide = matrix.astype(jnp.float32)
    return wide * lax.rsqrt(jnp.mean(wide * wide, axis=-1, keepdims=True) + epsilon) * gain


def stick_attend(query_rows, key_cols, value_cols, bias_grid, lengths):
    scores = jnp.einsum("shge,shke->shgk", query_rows, key_cols, preferred_element_type=jnp.float32)
    scores = scores / math.sqrt(HEAD) + bias_grid[None, :, :, None]
    position = lax.broadcasted_iota(jnp.int32, scores.shape, 3)
    valid_keys = position < lengths[:, None, None, None]
    log_keep = jnp.where(valid_keys, -jax.nn.softplus(scores), 0.0)
    later_sum = lax.cumsum(log_keep, axis=3, reverse=True) - log_keep
    weights = jnp.where(valid_keys, jnp.exp(jax.nn.log_sigmoid(scores) + later_sum), 0.0).astype(
        jnp.bfloat16
    )
    return jnp.einsum("shgk,shke->shge", weights, value_cols, preferred_element_type=jnp.float32)


def slot_table(routes, expert_ids, capacity):
    id_count = expert_ids.shape[0]
    hit_table = (routes[..., None] == expert_ids).astype(jnp.int32)
    per_row = jnp.sum(hit_table, axis=-2)
    earlier = jnp.cumsum(per_row, axis=-2) - per_row
    slot_rank = jnp.sum(hit_table * earlier[..., None, :], axis=-1)
    local_index = jnp.sum(hit_table * jnp.arange(id_count, dtype=jnp.int32), axis=-1)
    found_any = jnp.sum(hit_table, axis=-1)
    slot_index = jnp.where(found_any > 0, local_index * capacity + slot_rank, -1)
    return (slot_index[..., None] == jnp.arange(id_count * capacity, dtype=jnp.int32)).astype(
        jnp.float32
    )


def expert_apply(expert_rows, w_exp_gate, w_exp_up, w_exp_down):
    gate_pre = jnp.einsum(
        "bxcd,xdf->bxcf", expert_rows, w_exp_gate, preferred_element_type=jnp.float32
    )
    up_pre = jnp.einsum("bxcd,xdf->bxcf", expert_rows, w_exp_up, preferred_element_type=jnp.float32)
    hidden = (jax.nn.silu(gate_pre) * up_pre).astype(jnp.bfloat16)
    return jnp.einsum("bxcf,xfd->bxcd", hidden, w_exp_down, preferred_element_type=jnp.float32)


def dense_hidden(matrix, w_gate_rows, w_up_rows):
    contract = (((1,), (1,)), ((), ()))
    gate_pre = lax.dot_general(matrix, w_gate_rows, contract, preferred_element_type=jnp.float32)
    up_pre = lax.dot_general(matrix, w_up_rows, contract, preferred_element_type=jnp.float32)
    return (jax.nn.silu(gate_pre) * up_pre).astype(jnp.bfloat16)


def quarter_dense(quarter_rows, quarter_branch, w_dense_gate, w_dense_up, w_dense_down, tp_count):
    gate_rows, up_rows, down_rows = sent_together(
        (w_dense_gate, w_dense_up, w_dense_down), "tp", 0, 1
    )
    hidden = dense_hidden(quarter_rows, gate_rows, up_rows)
    partial_value = jnp.dot(hidden, down_rows, preferred_element_type=jnp.float32)
    partial_value = partial_value * quarter_branch.astype(jnp.float32)[:, None]
    mine = summed_on_arrival(partial_value.astype(jnp.bfloat16), "ep", 0)
    quarter = mine.shape[0]
    moved = lax.all_to_all(
        mine.reshape(quarter, tp_count, -1), "tp", split_axis=1, concat_axis=0, tiled=True
    )
    return moved.reshape(quarter * tp_count, -1)


def shards(
    tokens,
    attn_gain,
    w_query,
    stick_bias,
    kv_cache,
    lengths,
    head_gain,
    w_attn_out,
    ffn_gain,
    route_expert,
    route_weight,
    w_exp_gate,
    w_exp_up,
    w_exp_down,
    branch_gate,
    w_dense_gate,
    w_dense_up,
    w_dense_down,
):
    ep_count = lax.axis_size("ep")
    tp_count = lax.axis_size("tp")
    seq_rows, model_width = tokens.shape
    part_width = model_width // tp_count
    quarter = seq_rows // tp_count
    kv_local = kv_cache.shape[1]
    group_size = HEADS // KV_HEADS
    experts_here = w_exp_gate.shape[0]
    normed = rms_scale(tokens, attn_gain).astype(jnp.bfloat16)
    query_rows = jnp.dot(normed, w_query, preferred_element_type=jnp.float32).astype(jnp.bfloat16)
    query_rows = query_rows.reshape(seq_rows, kv_local, group_size, HEAD)
    head_out = stick_attend(
        query_rows,
        kv_cache[..., :HEAD],
        kv_cache[..., HEAD:],
        stick_bias.reshape(kv_local, group_size),
        lengths,
    )
    head_out = head_out * lax.rsqrt(jnp.mean(head_out * head_out, axis=-1, keepdims=True) + epsilon)
    head_out = head_out * head_gain.reshape(kv_local, group_size, HEAD)
    head_rows = head_out.astype(jnp.bfloat16).reshape(seq_rows, kv_local * group_size * HEAD)
    attention = taken_together(
        jnp.dot(head_rows, w_attn_out, preferred_element_type=jnp.float32).astype(jnp.bfloat16),
        "tp",
    ).astype(jnp.float32)
    residual = tokens.astype(jnp.float32) + attention
    normed2 = rms_scale(residual, ffn_gain).astype(jnp.bfloat16)
    branch = jax.nn.sigmoid(
        jnp.dot(normed2, branch_gate, preferred_element_type=jnp.float32)
    ).astype(jnp.bfloat16)
    residual_cols = lax.dynamic_slice_in_dim(
        residual, lax.axis_index("tp") * part_width, part_width, 1
    )
    table = slot_table(route_expert, jnp.arange(EXPERTS, dtype=jnp.int32), CAP)
    send = jnp.einsum(
        "skc,sd->cd", table.astype(jnp.bfloat16), normed2, preferred_element_type=jnp.float32
    ).astype(jnp.bfloat16)
    send = send.reshape(ep_count, experts_here, CAP, model_width)
    partial_value = expert_apply(
        lax.all_to_all(send, "ep", split_axis=0, concat_axis=0, tiled=True),
        w_exp_gate,
        w_exp_up,
        w_exp_down,
    )
    summed = summed_on_arrival(partial_value.astype(jnp.bfloat16), "tp", 3)
    returned = lax.all_to_all(
        summed.astype(jnp.bfloat16), "ep", split_axis=0, concat_axis=0, tiled=True
    ).astype(summed.dtype)
    combine = jnp.einsum("skc,sk->cs", table, route_weight.astype(jnp.float32), precision=highest)
    routed_cols = jnp.einsum(
        "cs,cd->sd", combine, returned.reshape(EXPERTS * CAP, part_width), precision=highest
    )
    start = lax.axis_index("tp") * quarter
    local_rows = lax.dynamic_slice_in_dim(normed2, start, quarter, 0)
    local_branch = lax.dynamic_slice_in_dim(branch, start, quarter, 0)
    quarter_rows, quarter_branch = sent_together_2((local_rows, local_branch), "ep", 0, 1)
    mixed = routed_cols + quarter_dense(
        quarter_rows, quarter_branch, w_dense_gate, w_dense_up, w_dense_down, tp_count
    )
    return (residual_cols + mixed).astype(jnp.bfloat16)


def solution(mesh):
    return jax.shard_map(
        shards,
        mesh=mesh,
        in_specs=(
            P("ep", None),
            P(),
            P(None, "tp"),
            P("tp"),
            P("ep", "tp", None, None),
            P("ep"),
            P("tp"),
            P("tp", None),
            P(),
            P("ep", None),
            P("ep", None),
            P("ep", None, "tp"),
            P("ep", None, "tp"),
            P("ep", "tp", None),
            P(),
            P(("ep", "tp"), None),
            P(("ep", "tp"), None),
            P(("ep", "tp"), None),
        ),
        out_specs=P("ep", "tp"),
        check_vma=False,
    )
```

profile of v0, /device:TPU:1, one launch (start us, length us, event | category | flops | bytes accessed | tf_op | source)
XLA Modules:
  0.0 204.2 jit_solution(1150948434649779946)
XLA Ops:
  6.5 1.9 pad_maximum_fusion
  8.5 1.0 fusion.43
  9.4 1.3 convolution_convert_fusion.3
  10.9 3.4 %fusion.51 = (f32[16,2,1024]{2,1,0:T(2,128)S(1)}, f32[16,2,1024]{2,1,0:T(2,128)S(1)}) fusion(s32[16]{0:T(128)} %param.23, f32[2]{0:T(128)} %param.21, bf16[16,2,64]{2,1,0:T(2,128)(2,1)S(1)} %reshape.177, bf16[16,1,1024,128]{3,2,1,0:T(8,128)(2,1)} %param.22), kind=kOutput, calls=%fused_computation.60 | convolution fusion | flops 4554752 | bytes 4460616 | tf_op jit(solution)/shard_map/shge,shke->shgk/dot_general | solution.py:66
  14.4 39.6 %reduce-window.6 = f32[16,1,2,8,128]{4,3,2,1,0:T(8,128)S(1)} reduce-window(f32[16,1,2,8,128]{4,3,2,1,0:T(8,128)S(1)} %bitcast.124, f32[]{:T(128)} %constant.16.clone.1), window={size=1x1x1x1x128 pad=0_0x0_0x0_0x0_0x0_127}, to_apply=%region_1.2 | reduce-window | flops 4161536 | bytes 262148 | tf_op jit(solution)/shard_map/reduce-window
  54.7 4.3 %multiply_reduce_fusion.1 = (f32[16,2]{1,0:T(8,128)S(1)}, f32[16,2,64]{2,1,0:T(2,128)S(1)}) fusion(bf16[16,1,1024,128]{3,2,1,0:T(8,128)(2,1)} %param.22, f32[16,2,1024]{2,1,0:T(2,128)S(1)} %reshape.180, f32[16,2,1024]{2,1,0:T(2,128)S(1)} %reshape.183, f32[16,2,1024]{2,1,0:T(2,128)S(1)} %get-tuple-element.11, s32[16]{0:T(128)S(1)} %copy-done.9), kind=kOutput, calls=%fused_computation.92 | convolution fusion | flops 4919264 | bytes 4595904 | tf_op jit(solution)/shard_map/shgk,shke->shge/dot_general | solution.py:75
  59.4 0.9 broadcast_in_dim.8
  60.2 6.6 %all-to-all-start = ((bf16[8,16,2048]{2,1,0:T(8,128)(2,1)}), bf16[8,16,2048]{2,1,0:T(8,128)(2,1)S(1)}, u32[]{:S(2)}, u32[]{:S(2)}) async-start(bf16[8,16,2048]{2,1,0:T(8,128)(2,1)} %broadcast_in_dim.8), calls=%async_computation | async-start | bytes 1048576 | tf_op jit(solution)/shard_map/all_to_all | solution.py:41
  66.8 0.2 select_reduce_fusion.1
  67.4 8.8 %all-to-all-done = bf16[8,16,2048]{2,1,0:T(8,128)(2,1)S(1)} async-done(((bf16[8,16,2048]{2,1,0:T(8,128)(2,1)}), bf16[8,16,2048]{2,1,0:T(8,128)(2,1)S(1)}, u32[]{:S(2)}, u32[]{:S(2)}) %all-to-all-start) | async-done | bytes 524320 | tf_op jit(solution)/shard_map/all_to_all | solution.py:41
  76.8 0.3 fusion.77
  77.1 0.9 reshape.186
  78.0 10.4 %all-to-all-start.1 = ((bf16[32,1,2,2048]{3,2,1,0:T(2,128)(2,1)}), bf16[32,1,2,2048]{3,2,1,0:T(2,128)(2,1)S(1)}, u32[]{:S(2)}, u32[]{:S(2)}) async-start(bf16[32,1,2,2048]{3,2,1,0:T(2,128)(2,1)} %bitcast.8), calls=%async_computation.1 | async-start | bytes 524288 | tf_op jit(solution)/shard_map/all_to_all | solution.py:182
  88.4 38.7 %all-gather = bf16[32,2,2049]{2,1,0:T(2,128)(2,1)S(1)} all-gather(bf16[1,2,2049]{2,1,0:T(2,128)(2,1)S(1)} %maximum_bitcast_fusion), channel_id=1, replica_groups=mesh['ep'=32,'tp'=8] {'ep'}, dimensions={0}, use_global_device_ids=true | all-gather | bytes 270468 | tf_op jit(solution)/shard_map/all_gather | solution.py:53
  127.2 0.2 reshape.200
  127.5 0.3 convolution_bitcast_fusion.1
  127.8 2.0 convolution_convert_fusion
  129.9 0.7 copy.80
  130.6 16.0 %all-to-all-start.2 = ((bf16[8,32,1,2,256]{4,1,3,2,0:T(8,128)(2,1)}), bf16[8,32,1,2,256]{4,1,3,2,0:T(8,128)(2,1)S(1)}, u32[]{:S(2)}, u32[]{:S(2)}) async-start(bf16[8,32,1,2,256]{4,1,3,2,0:T(8,128)(2,1)} %bitcast.120), calls=%async_computation.2 | async-start | bytes 524288 | tf_op jit(solution)/shard_map/all_to_all | solution.py:35
  146.6 1.7 fusion.27
  148.3 2.5 %fusion.6 = bf16[64,2048]{1,0:T(8,128)(2,1)S(1)} fusion(bf16[256,6144]{1,0:T(8,128)(2,1)} %all-gather.3.cloned.1.call-done, f32[64]{0:T(128)S(1)} %bitcast_convert_fusion, bf16[64,2049]{1,0:T(8,128)(2,1)S(1)} %reshape.200, f32[64,256]{1,0:T(8,128)S(1)} %fusion.27), kind=kOutput, calls=%fused_computation.7 | convolution fusion | flops 134578176 | bytes 2687488 | tf_op jit(solution)/shard_map/dot_general | solution.py:113
  150.8 0.9 reshape.195
  151.7 1.5 all-to-all-done.2
  153.1 8.0 %all-to-all-start.4 = ((bf16[32,2,2048]{2,1,0:T(2,128)(2,1)}), bf16[32,2,2048]{2,1,0:T(2,128)(2,1)S(1)}, u32[]{:S(2)}, u32[]{:S(2)}) async-start(bf16[32,2,2048]{2,1,0:T(2,128)(2,1)} %reshape.195), calls=%async_computation.4 | async-start | bytes 524288 | tf_op jit(solution)/shard_map/all_to_all | solution.py:35
  161.4 0.6 copy.57
  162.0 9.8 %all-to-all-done.4 = bf16[32,2,2048]{2,1,0:T(2,128)(2,1)S(1)} async-done(((bf16[32,2,2048]{2,1,0:T(2,128)(2,1)}), bf16[32,2,2048]{2,1,0:T(2,128)(2,1)S(1)}, u32[]{:S(2)}, u32[]{:S(2)}) %all-to-all-start.4) | async-done | bytes 262176 | tf_op jit(solution)/shard_map/all_to_all | solution.py:35
  171.8 5.3 %all-to-all-start.3 = ((bf16[32,1,2,256]{3,2,1,0:T(2,128)(2,1)}), bf16[32,1,2,256]{3,2,1,0:T(2,128)(2,1)S(1)}, u32[]{:S(2)}, u32[]{:S(2)}) async-start(bf16[32,1,2,256]{3,2,1,0:T(2,128)(2,1)} %copy.57), calls=%async_computation.3 | async-start | bytes 65536 | tf_op jit(solution)/shard_map/all_to_all | solution.py:188
  177.1 0.8 convert_reduce_fusion.1
  177.9 7.9 %all-to-all-done.3 = bf16[32,1,2,256]{3,2,1,0:T(2,128)(2,1)S(1)} async-done(((bf16[32,1,2,256]{3,2,1,0:T(2,128)(2,1)}), bf16[32,1,2,256]{3,2,1,0:T(2,128)(2,1)S(1)}, u32[]{:S(2)}, u32[]{:S(2)}) %all-to-all-start.3) | async-done | bytes 32800 | tf_op jit(solution)/shard_map/all_to_all | solution.py:188
  185.8 6.2 %all-to-all-start.5 = ((f32[2,8,256]{2,0,1:T(2,128)}), f32[2,8,256]{2,0,1:T(2,128)S(1)}, u32[]{:S(2)}, u32[]{:S(2)}) async-start(f32[2,8,256]{2,0,1:T(2,128)} %bitcast.34), calls=%async_computation.5 | async-start | bytes 32768 | tf_op jit(solution)/shard_map/all_to_all | solution.py:117
  192.1 4.5 %all-to-all-done.5 = f32[2,8,256]{2,0,1:T(2,128)S(1)} async-done(((f32[2,8,256]{2,0,1:T(2,128)}), f32[2,8,256]{2,0,1:T(2,128)S(1)}, u32[]{:S(2)}, u32[]{:S(2)}) %all-to-all-start.5) | async-done | bytes 16416 | tf_op jit(solution)/shard_map/all_to_all | solution.py:117
  196.6 0.7 fusion.18
  (63 shorter events, 2.7 us)
Async XLA Ops:
  6.5 121.3 %copy-start = (bf16[1,256,2048]{2,1,0:T(8,128)(2,1)S(1)}, bf16[1,256,2048]{2,1,0:T(8,128)(2,1)}, u32[]{:S(2)}) copy-start(bf16[1,256,2048]{2,1,0:T(8,128)(2,1)} %param.31) | copy-start | bytes 3145732
  6.5 140.1 %all-gather.3.cloned.1.call-start = ((), (), s32[]{:S(2)}) async-start(), calls=%async_computation.6 | async-start | bytes 3538944 | tf_op jit(solution)/shard_map/all_gather | solution.py:25
  8.4 46.2 %copy-start.8 = (f32[128]{0:T(128)S(1)}, f32[128]{0:T(128)}, u32[]{:S(2)}) copy-start(f32[128]{0:T(128)} %param.24) | copy-start | bytes 1540
  8.4 46.3 %copy-start.9 = (s32[16]{0:T(128)S(1)}, s32[16]{0:T(128)}, u32[]{:S(2)}) copy-start(s32[16]{0:T(128)} %param.23) | copy-start | bytes 196
  54.4 4.8 %copy-start.3 = (bf16[128,2048]{1,0:T(8,128)(2,1)S(1)}, bf16[128,2048]{1,0:T(8,128)(2,1)}, u32[]{:S(2)}) copy-start(bf16[128,2048]{1,0:T(8,128)(2,1)} %param.25) | copy-start | bytes 1572868
  54.7 12.1 %copy-start.6 = (s32[16,2]{0,1:T(2,128)S(1)}, s32[16,2]{0,1:T(2,128)}, u32[]{:S(2)}) copy-start(s32[16,2]{0,1:T(2,128)} %param.27) | copy-start | bytes 388
  54.7 12.3 %copy-start.5 = (bf16[2048]{0:T(1024)(128)(2,1)S(1)}, bf16[2048]{0:T(1024)(128)(2,1)}, u32[]{:S(2)}) copy-start(bf16[2048]{0:T(1024)(128)(2,1)} %param.32) | copy-start | bytes 12292
  54.7 21.6 %copy-start.2 = (bf16[16,2048]{1,0:T(8,128)(2,1)S(1)}, bf16[16,2048]{1,0:T(8,128)(2,1)}, u32[]{:S(2)}) copy-start(bf16[16,2048]{1,0:T(8,128)(2,1)} %param.18) | copy-start | bytes 196612
  54.7 21.7 %copy-start.4 = (f32[2048]{0:T(1024)S(1)}, f32[2048]{0:T(1024)}, u32[]{:S(2)}) copy-start(f32[2048]{0:T(1024)} %param.26) | copy-start | bytes 24580
  59.0 68.5 %copy-start.1 = (bf16[1,2048,256]{2,1,0:T(8,128)(2,1)S(1)}, bf16[1,2048,256]{2,1,0:T(8,128)(2,1)}, u32[]{:S(2)}) copy-start(bf16[1,2048,256]{2,1,0:T(8,128)(2,1)} %param.29) | copy-start | bytes 3145732
  60.2 16.0 %all-to-all-start = ((bf16[8,16,2048]{2,1,0:T(8,128)(2,1)}), bf16[8,16,2048]{2,1,0:T(8,128)(2,1)S(1)}, u32[]{:S(2)}, u32[]{:S(2)}) async-start(bf16[8,16,2048]{2,1,0:T(8,128)(2,1)} %broadcast_in_dim.8), calls=%async_computation | async-start | bytes 1048576 | tf_op jit(solution)/shard_map/all_to_all | solution.py:41
  78.0 49.5 %all-to-all-start.1 = ((bf16[32,1,2,2048]{3,2,1,0:T(2,128)(2,1)}), bf16[32,1,2,2048]{3,2,1,0:T(2,128)(2,1)S(1)}, u32[]{:S(2)}, u32[]{:S(2)}) async-start(bf16[32,1,2,2048]{3,2,1,0:T(2,128)(2,1)} %bitcast.8), calls=%async_computation.1 | async-start | bytes 524288 | tf_op jit(solution)/shard_map/all_to_all | solution.py:182
  127.8 33.4 %copy-start.7 = (bf16[16,2]{0,1:T(2,128)(2,1)S(1)}, bf16[16,2]{0,1:T(2,128)(2,1)}, u32[]{:S(2)}) copy-start(bf16[16,2]{0,1:T(2,128)(2,1)} %param.28) | copy-start | bytes 196
  130.6 22.5 %all-to-all-start.2 = ((bf16[8,32,1,2,256]{4,1,3,2,0:T(8,128)(2,1)}), bf16[8,32,1,2,256]{4,1,3,2,0:T(8,128)(2,1)S(1)}, u32[]{:S(2)}, u32[]{:S(2)}) async-start(bf16[8,32,1,2,256]{4,1,3,2,0:T(8,128)(2,1)} %bitcast.120), calls=%async_computation.2 | async-start | bytes 524288 | tf_op jit(solution)/shard_map/all_to_all | solution.py:35
  153.1 18.7 %all-to-all-start.4 = ((bf16[32,2,2048]{2,1,0:T(2,128)(2,1)}), bf16[32,2,2048]{2,1,0:T(2,128)(2,1)S(1)}, u32[]{:S(2)}, u32[]{:S(2)}) async-start(bf16[32,2,2048]{2,1,0:T(2,128)(2,1)} %reshape.195), calls=%async_computation.4 | async-start | bytes 524288 | tf_op jit(solution)/shard_map/all_to_all | solution.py:35
  171.8 14.0 %all-to-all-start.3 = ((bf16[32,1,2,256]{3,2,1,0:T(2,128)(2,1)}), bf16[32,1,2,256]{3,2,1,0:T(2,128)(2,1)S(1)}, u32[]{:S(2)}, u32[]{:S(2)}) async-start(bf16[32,1,2,256]{3,2,1,0:T(2,128)(2,1)} %copy.57), calls=%async_computation.3 | async-start | bytes 65536 | tf_op jit(solution)/shard_map/all_to_all | solution.py:188
  185.8 10.8 %all-to-all-start.5 = ((f32[2,8,256]{2,0,1:T(2,128)}), f32[2,8,256]{2,0,1:T(2,128)S(1)}, u32[]{:S(2)}, u32[]{:S(2)}) async-start(f32[2,8,256]{2,0,1:T(2,128)} %bitcast.34), calls=%async_computation.5 | async-start | bytes 32768 | tf_op jit(solution)/shard_map/all_to_all | solution.py:117
Sparse Core Ops, SparseCore 0:
  9.2 34.4 all-gather.2
where the time goes:
time: 205 us; the launch traced here: 204 us
  starting transfers between devices  52.4 us (26%)
  other arithmetic  44.4 us (22%)
  blocking collectives  38.7 us (19%)
  waiting for transfers between devices  32.5 us (16%)
  matrix products  17 us (8%)
  between operations  13.7 us (7%)
  local copies, waits for them, and re-layouts  5.55 us (3%)
    another operation x2, other arithmetic  39.7 us
    all_gather x1, blocking collectives, sent_together_2(): result = lax.all_gather(both, axis, axis=dim, tiled=True)  38.7 us
    all_to_all x2, starting transfers between devices, summed_on_arrival(): blocks = lax.all_to_all(in_blocks(x, dim, size), axis, 0, 0, tiled=True)  24.1 us
    all_to_all x2, waiting for transfers between devices, summed_on_arrival(): blocks = lax.all_to_all(in_blocks(x, dim, size), axis, 0, 0, tiled=True)  11.2 us
    all_to_all x1, starting transfers between devices, shards(): lax.all_to_all(send, 'ep', split_axis=0, concat_axis=0, tiled=True)  10.4 us
    all_to_all x1, waiting for transfers between devices, copy_for_each(): lax.all_to_all(jnp.broadcast_to(x[None], (size, *x.shape)), axis, 0, 0, t...  8.82 us
    all_to_all x1, waiting for transfers between devices, shards(): lax.all_to_all(summed.astype(jnp.bfloat16), 'ep', split_axis=0, concat_ax...  7.88 us
    all_to_all x1, starting transfers between devices, copy_for_each(): lax.all_to_all(jnp.broadcast_to(x[None], (size, *x.shape)), axis, 0, 0, t...  6.59 us
  transfers between devices with their start and end apart: 7, of which 5 were waited for; matrix products, arithmetic and copies ran while one was open for 31% of the time, Pallas kernels for 0%

commit v1 on v0

v1 whole, which is shorter than its diff:
```python
import jax
import jax.numpy as jnp
from jax import lax
from jax.experimental import pallas as pl
from jax.experimental.pallas import tpu as pltpu
from jax.sharding import PartitionSpec as P

HEADS = 16
HEAD = 64
KV_HEADS = 8
EXPERTS = 32
CAP = 2
CACHE = 1024
WIDTH = 2048
ROWS = 16
LANES = 128
HALF = 8
epsilon = 1e-06
NT = (((1,), (1,)), ((), ()))


def attention_kernel(
    len_ref, bias_ref, tok_ref, gain_ref, hgain_ref, wq_hbm, kv_hbm, wo_hbm,
    out_ref, wq_v, kv_v, wo_v, q_sem, kv_sem, o_sem,
):
    copy_q = pltpu.make_async_copy(wq_hbm, wq_v, q_sem)
    copy_q.start()
    copies = []
    for s in range(ROWS):
        half, j = divmod(s, HALF)
        copy = pltpu.make_async_copy(
            kv_hbm.at[s, 0], kv_v.at[half, :, pl.ds(j * LANES, LANES)], kv_sem.at[s]
        )
        copy.start()
        copies.append(copy)
    copy_o = pltpu.make_async_copy(wo_hbm, wo_v, o_sem)
    copy_o.start()

    wide = tok_ref[...].astype(jnp.float32)
    scale = lax.rsqrt(jnp.mean(wide * wide, axis=-1, keepdims=True) + epsilon)
    normed = (wide * scale * gain_ref[...]).astype(jnp.bfloat16)
    copy_q.wait()
    query = jnp.dot(normed, wq_v[...], preferred_element_type=jnp.float32)
    query = query.astype(jnp.bfloat16).astype(jnp.float32)

    lane8 = lax.broadcasted_iota(jnp.int32, (HALF, LANES), 1)
    row8 = lax.broadcasted_iota(jnp.int32, (HALF, LANES), 0)
    lane16 = lax.broadcasted_iota(jnp.int32, (2 * HALF, LANES), 1)
    row16 = lax.broadcasted_iota(jnp.int32, (2 * HALF, LANES), 0)
    tri_row = lax.broadcasted_iota(jnp.int32, (LANES, 2 * LANES), 0)
    tri_col = lax.broadcasted_iota(jnp.int32, (LANES, 2 * LANES), 1)
    tri = ((tri_row >= tri_col) | (tri_col >= LANES)).astype(jnp.bfloat16)
    position = lax.broadcasted_iota(jnp.int32, (2 * HALF, CACHE), 1)
    bias = jnp.where(row16[:, :1] < HALF, bias_ref[0], bias_ref[1])
    hgain = hgain_ref[...]
    gain_rows = jnp.where(row16 < HALF, pltpu.roll(hgain, HEAD, 1), hgain)
    chunks = CACHE // LANES

    heads = []
    for half in range(2):
        part = query[half * HALF : (half + 1) * HALF]
        first = jnp.where(lane8 < HEAD, part, 0.0)
        second = jnp.where(lane8 < HEAD, pltpu.roll(part, HEAD, 1), 0.0)
        blocks = [
            jnp.concatenate(
                [jnp.where(row8 == j, first, 0.0), jnp.where(row8 == j, second, 0.0)], axis=0
            )
            for j in range(HALF)
        ]
        lhs = jnp.concatenate(blocks, axis=1).astype(jnp.bfloat16)
        length = jnp.full((2 * HALF, 1), len_ref[half * HALF], jnp.int32)
        for j in range(1, HALF):
            length = jnp.where(row16[:, :1] % HALF == j, len_ref[half * HALF + j], length)
        valid = position < length
        for j in range(HALF):
            copies[half * HALF + j].wait()
        scores = lax.dot_general(lhs, kv_v[half], NT, preferred_element_type=jnp.float32)
        scores = scores * 0.125 + bias
        soft = jnp.maximum(scores, 0.0) + jnp.log1p(jnp.exp(-jnp.abs(scores)))
        soft = jnp.where(valid, soft, 0.0)
        stacked = jnp.concatenate(
            [soft[:, c * LANES : (c + 1) * LANES] for c in range(chunks)], axis=0
        )
        high = stacked.astype(jnp.bfloat16)
        rest = stacked - high.astype(jnp.float32)
        middle = rest.astype(jnp.bfloat16)
        low = (rest - middle.astype(jnp.float32)).astype(jnp.bfloat16)
        sums = jnp.dot(high, tri, preferred_element_type=jnp.float32)
        sums = sums + jnp.dot(middle, tri, preferred_element_type=jnp.float32)
        sums = sums + jnp.dot(low, tri, preferred_element_type=jnp.float32)
        pieces = [None] * chunks
        carry = jnp.zeros((2 * HALF, LANES), jnp.float32)
        for c in reversed(range(chunks)):
            rows = sums[c * 2 * HALF : (c + 1) * 2 * HALF]
            pieces[c] = rows[:, :LANES] + carry
            carry = carry + rows[:, LANES:]
        later = jnp.concatenate(pieces, axis=1)
        weights = jnp.where(valid, jnp.exp(scores - later), 0.0).astype(jnp.bfloat16)
        mixed = jnp.dot(weights, kv_v[half], preferred_element_type=jnp.float32)
        own = jnp.zeros((2 * HALF, LANES), jnp.float32)
        for j in range(HALF):
            own = jnp.where(row16 % HALF == j, mixed[:, j * LANES : (j + 1) * LANES], own)
        square = jnp.where(lane16 >= HEAD, own * own, 0.0)
        mean = jnp.sum(square, axis=-1, keepdims=True) * (1.0 / HEAD)
        own = own * lax.rsqrt(mean + epsilon) * gain_rows
        heads.append(
            jnp.where(lane8 < HEAD, pltpu.roll(own[:HALF], HEAD, 1), own[HALF:])
        )
    head_rows = jnp.concatenate(heads, axis=0).astype(jnp.bfloat16)
    copy_o.wait()
    share = jnp.dot(head_rows, wo_v[...], preferred_element_type=jnp.float32)
    share = share.astype(jnp.bfloat16)
    for i in range(8):
        out_ref[i] = share


def attention(tokens, attn_gain, w_query, stick_bias, kv_cache, lengths, head_gain, w_attn_out):
    vmem = pl.BlockSpec(memory_space=pltpu.VMEM)
    smem = pl.BlockSpec(memory_space=pltpu.SMEM)
    anywhere = pl.BlockSpec(memory_space=pl.ANY)
    return pl.pallas_call(
        attention_kernel,
        out_shape=jax.ShapeDtypeStruct((8, ROWS, WIDTH), jnp.bfloat16),
        in_specs=[smem, smem, vmem, vmem, vmem, anywhere, anywhere, anywhere],
        out_specs=vmem,
        scratch_shapes=[
            pltpu.VMEM((WIDTH, LANES), jnp.bfloat16),
            pltpu.VMEM((2, CACHE, HALF * LANES), jnp.bfloat16),
            pltpu.VMEM((LANES, WIDTH), jnp.bfloat16),
            pltpu.SemaphoreType.DMA,
            pltpu.SemaphoreType.DMA((ROWS,)),
            pltpu.SemaphoreType.DMA,
        ],
        cost_estimate=pl.CostEstimate(
            flops=400_000_000, bytes_accessed=6_000_000, transcendentals=200_000
        ),
    )(
        lengths, stick_bias, tokens, attn_gain.reshape(1, -1), head_gain.reshape(1, -1),
        w_query, kv_cache, w_attn_out,
    )


def slot_table(routes):
    ids = jnp.arange(EXPERTS, dtype=jnp.int32)
    hits = (routes[..., None] == ids).astype(jnp.int32)
    per_row = jnp.sum(hits, axis=1)
    before = jnp.arange(ROWS)[:, None] > jnp.arange(ROWS)[None, :]
    earlier = jnp.sum(jnp.where(before[:, :, None], per_row[None], 0), axis=1)
    rank = jnp.sum(hits * earlier[:, None, :], axis=-1)
    slot = jnp.arange(CAP, dtype=jnp.int32)
    return (routes[:, :, None, None] == ids[:, None]) & (rank[:, :, None, None] == slot)


def gated(rows, gate, up, down, dims):
    a = lax.dot_general(rows, gate, dims, preferred_element_type=jnp.float32)
    b = lax.dot_general(rows, up, dims, preferred_element_type=jnp.float32)
    hidden = (jax.nn.silu(a) * b).astype(jnp.bfloat16)
    return jnp.dot(hidden, down, preferred_element_type=jnp.float32).astype(jnp.bfloat16)


def shards(
    tokens, attn_gain, w_query, stick_bias, kv_cache, lengths, head_gain, w_attn_out, ffn_gain,
    route_expert, route_weight, w_exp_gate, w_exp_up, w_exp_down, branch_gate,
    w_dense_gate, w_dense_up, w_dense_down,
):
    single = jnp.float32
    t = lax.axis_index("tp")
    core = t % 2
    copies = attention(
        tokens, attn_gain, w_query, stick_bias, kv_cache, lengths, head_gain, w_attn_out
    )
    copies, route_expert, w_dense_gate, w_dense_up, w_dense_down = lax.optimization_barrier(
        (copies, route_expert, w_dense_gate, w_dense_up, w_dense_down)
    )
    shares = lax.all_to_all(copies, "tp", 0, 0, tiled=True)

    own = jnp.stack([w_dense_gate, w_dense_up, w_dense_down])
    groups = [[z * 4 + x for x in range(4)] for z in range(8)]
    four = lax.all_to_all(
        jnp.broadcast_to(own[None], (4, *own.shape)), "ep", 0, 0, tiled=True,
        axis_index_groups=groups,
    )
    other = lax.ppermute(four, "tp", [(i, i ^ 1) for i in range(8)])

    table = slot_table(route_expert)
    taken = jnp.any(table, axis=1)
    expert_dest = jnp.moveaxis(taken, 0, -1)
    quarter = 4 * (jnp.arange(32) % 4)[:, None] + 2 * core + jnp.arange(2)
    dense_dest = quarter[..., None] == jnp.arange(ROWS)
    picks = jnp.concatenate([expert_dest, dense_dest], axis=1)

    residual = tokens.astype(single) + jnp.sum(shares.astype(single), axis=0)
    scale = lax.rsqrt(jnp.mean(residual * residual, axis=-1, keepdims=True) + epsilon)
    normed = (residual * scale * ffn_gain).astype(jnp.bfloat16)
    branch = jax.nn.sigmoid(jnp.dot(normed, branch_gate, preferred_element_type=single))
    branch = branch.astype(jnp.bfloat16)
    residual_cols = lax.dynamic_slice_in_dim(residual, t * 256, 256, 1)

    send = jnp.einsum(
        "cks,sd->ckd", picks.astype(jnp.bfloat16), normed, preferred_element_type=single
    ).astype(jnp.bfloat16)
    got = lax.all_to_all(send, "ep", 0, 0, tiled=True)

    expert_rows = got[:, :2].reshape(64, WIDTH)
    dense_rows = got[:, 2:].reshape(64, WIDTH)
    expert_out = gated(
        expert_rows, w_exp_gate[0], w_exp_up[0], w_exp_down[0], (((1,), (0,)), ((), ()))
    )
    weights = jnp.concatenate([four, other], axis=0)
    gate_all = weights[:, 0].reshape(256, WIDTH)
    up_all = weights[:, 1].reshape(256, WIDTH)
    down_all = weights[:, 2].reshape(256, WIDTH)
    dense_out = gated(dense_rows, gate_all, up_all, down_all, NT)
    back = jnp.concatenate(
        [expert_out.reshape(32, 2, WIDTH), dense_out.reshape(32, 2, WIDTH)], axis=1
    )
    returned = lax.all_to_all(back, "ep", 0, 0, tiled=True).reshape(128, WIDTH)

    weight = jnp.sum(
        jnp.where(table, route_weight[:, :, None, None].astype(single), 0.0), axis=1
    ).astype(jnp.bfloat16)
    dense_weight = jnp.where(
        jnp.moveaxis(dense_dest, -1, 0), branch[:, None, None], jnp.bfloat16(0)
    )
    mix = jnp.concatenate([weight, dense_weight], axis=2).reshape(ROWS, 128)
    partial = jnp.dot(mix, returned, preferred_element_type=single).astype(jnp.bfloat16)
    partial = jnp.moveaxis(partial.reshape(ROWS, 8, 256), 1, 0)
    columns = lax.all_to_all(partial, "tp", 0, 0, tiled=True)
    total = jnp.sum(columns.astype(single), axis=0)
    return (residual_cols + total).astype(jnp.bfloat16)


def solution(mesh):
    return jax.shard_map(
        shards,
        mesh=mesh,
        in_specs=(
            P("ep", None), P(), P(None, "tp"), P("tp"), P("ep", "tp", None, None), P("ep"),
            P("tp"), P("tp", None), P(), P("ep", None), P("ep", None), P("ep", None, "tp"),
            P("ep", None, "tp"), P("ep", "tp", None), P(), P(("ep", "tp"), None),
            P(("ep", "tp"), None), P(("ep", "tp"), None),
        ),
        out_specs=P("ep", "tp"),
        check_vma=False,
    )
```

time: 205 us -> 126 us (0.61)
  other arithmetic: 44.4 us -> 5.24 us
  blocking collectives: 38.7 us -> 0 us
  waiting for transfers between devices: 32.5 us -> 53.5 us
  starting transfers between devices: 52.4 us -> 35.2 us
  between operations: 13.7 us -> 0.23 us
  local copies, waits for them, and re-layouts: 5.55 us -> 14.8 us
  matrix products: 17 us -> 9.28 us
  Pallas kernels: 0 us -> 7.45 us
    another operation x3 -> x1, other arithmetic: 39.7 us -> 0.05 us  [shards(): own = jnp.stack([w_dense_gate, w_dense_up, w_dense_down])]
    all_gather x1 -> x0, blocking collectives: 38.7 us -> none  [sent_together_2(): result = lax.all_gather(both, axis, axis=dim, tiled=True)]
    all_to_all x6 -> x5, waiting for transfers between devices: 32.4 us -> 53.5 us  [the longest x1 17.3 us: shards(): lax.all_to_all(jnp.broadcast_to(own[None], (4, *own.shape)), 'ep', 0, 0,...]
    all_to_all x6 -> x5, starting transfers between devices: 52.4 us -> 32.7 us  [the longest x1 8.83 us: shards(): got = lax.all_to_all(send, 'ep', 0, 0, tiled=True)]
    dot_general x12 -> x7, matrix products: 17 us -> 9.28 us  [the longest x2 4.48 us: gated(): jnp.dot(hidden, down, preferred_element_type=jnp.float32)]
    pallas_call x0 -> x1, Pallas kernels: none -> 7.45 us  [attention(): pl.pallas_call(attention_kernel, out_shape=jax.ShapeDtypeStruct((8, ROWS,...]
    slice x1 -> x2, local copies, waits for them, and re-layouts: 0.18 us -> 3.21 us  [the longest x1 2.13 us: shards(): gate_all = weights[:, 0].reshape(256, WIDTH)]
    concatenate x0 -> x1, local copies, waits for them, and re-layouts: none -> 2.73 us  [shards(): weights = jnp.concatenate([four, other], axis=0)]
  transfers between devices with their start and end apart: 7 -> 6, of which waited for: 5 -> 5; matrix products, arithmetic and copies ran while one was open for 31% -> 11% of each run, Pallas kernels for 0% -> 0%
where the time goes in v1:
time: 126 us
  waiting for transfers between devices  53.5 us (42%)
  starting transfers between devices  35.2 us (28%)
  local copies, waits for them, and re-layouts  14.8 us (12%)
  matrix products  9.28 us (7%)
  Pallas kernels  7.45 us (6%)
  other arithmetic  5.24 us (4%)
    all_to_all x1, waiting for transfers between devices, shards(): lax.all_to_all(jnp.broadcast_to(own[None], (4, *own.shape)), 'ep', 0, 0,...  17.3 us
    all_to_all x1, waiting for transfers between devices, shards(): returned = lax.all_to_all(back, 'ep', 0, 0, tiled=True).reshape(128, WIDTH)  11.6 us
    all_to_all x1, waiting for transfers between devices, shards(): got = lax.all_to_all(send, 'ep', 0, 0, tiled=True)  10.9 us
    all_to_all x1, starting transfers between devices, shards(): got = lax.all_to_all(send, 'ep', 0, 0, tiled=True)  8.83 us
    all_to_all x1, waiting for transfers between devices, shards(): shares = lax.all_to_all(copies, 'tp', 0, 0, tiled=True)  8.77 us
    pallas_call x1, Pallas kernels, attention(): pl.pallas_call(attention_kernel, out_shape=jax.ShapeDtypeStruct((8, ROWS,...  7.45 us
    all_to_all x1, starting transfers between devices, shards(): columns = lax.all_to_all(partial, 'tp', 0, 0, tiled=True)  7.43 us
    all_to_all x1, starting transfers between devices, shards(): shares = lax.all_to_all(copies, 'tp', 0, 0, tiled=True)  6.6 us
  transfers between devices with their start and end apart: 6, of which 5 were waited for; matrix products, arithmetic and copies ran while one was open for 11% of the time, Pallas kernels for 0%

profile of v1, /device:TPU:1, one launch (start us, length us, event | category | flops | bytes accessed | tf_op | source)
XLA Modules:
  0.0 125.6 jit_solution(9473326355979756820)
XLA Ops:
  0.0 7.5 %shard_map.172 = bf16[8,16,2048]{2,1,0:T(8,128)(2,1)} custom-call(s32[16]{0:T(128)} %len_ref.1, f32[2]{0:T(128)} %bias_ref.1, bf16[16,2048]{1,0:T(8,128)(2,1)} %tok_ref.1, f32[1,2048]{1,0:T(1,128)} %bitcast.61, f32[1,128]{1,0:T(1,128)} %bitcast.62, bf16[2048,128]{1,0:T(8,128)(2,1)} %wq_hbm.1, bf16[16,1,1024,128]{3,2,1,0:T(8,128)(2,1)} %kv_hbm.1, ...), custom_call_target="tpu_custom_call" | custom-call | flops 400000000 | bytes 6000000 | tf_op jit(solution)/shard_map/pallas_call | solution.py:121
  7.5 6.6 %all-to-all-start = ((bf16[8,16,2048]{2,1,0:T(8,128)(2,1)}), bf16[8,16,2048]{2,1,0:T(8,128)(2,1)S(1)}, u32[]{:S(2)}, u32[]{:S(2)}) async-start(bf16[8,16,2048]{2,1,0:T(8,128)(2,1)} %shard_map.172), calls=%async_computation | async-start | bytes 1048576 | tf_op jit(solution)/shard_map/all_to_all | solution.py:175
  14.7 8.8 %all-to-all-done = bf16[8,16,2048]{2,1,0:T(8,128)(2,1)S(1)} async-done(((bf16[8,16,2048]{2,1,0:T(8,128)(2,1)}), bf16[8,16,2048]{2,1,0:T(8,128)(2,1)S(1)}, u32[]{:S(2)}, u32[]{:S(2)}) %all-to-all-start) | async-done | bytes 524320 | tf_op jit(solution)/shard_map/all_to_all | solution.py:175
  23.5 1.3 %broadcast_in_dim.75 = bf16[4,3,32,2048]{3,2,1,0:T(8,128)(2,1)} broadcast(bf16[3,32,2048]{2,1,0:T(8,128)(2,1)S(1)} %pad_maximum_fusion.1), dimensions={1,2,3} | broadcast | bytes 1966080 | tf_op jit(solution)/shard_map/broadcast_in_dim | solution.py:180
  24.8 3.6 %all-to-all-start.2 = ((bf16[4,3,32,2048]{3,2,1,0:T(8,128)(2,1)}), bf16[4,3,32,2048]{3,2,1,0:T(8,128)(2,1)S(1)}, u32[]{:S(2)}, u32[]{:S(2)}) async-start(bf16[4,3,32,2048]{3,2,1,0:T(8,128)(2,1)} %broadcast_in_dim.75), calls=%async_computation.2 | async-start | bytes 3145728 | tf_op jit(solution)/shard_map/all_to_all | solution.py:179
  29.6 1.2 copy.34
  30.8 17.3 %all-to-all-done.2 = bf16[4,3,32,2048]{3,2,1,0:T(8,128)(2,1)S(1)} async-done(((bf16[4,3,32,2048]{3,2,1,0:T(8,128)(2,1)}), bf16[4,3,32,2048]{3,2,1,0:T(8,128)(2,1)S(1)}, u32[]{:S(2)}, u32[]{:S(2)}) %all-to-all-start.2) | async-done | bytes 1572896 | tf_op jit(solution)/shard_map/all_to_all | solution.py:179
  48.1 8.8 %all-to-all-start.1 = ((bf16[32,4,2048]{2,1,0:T(4,128)(2,1)}), bf16[32,4,2048]{2,1,0:T(4,128)(2,1)S(1)}, u32[]{:S(2)}, u32[]{:S(2)}) async-start(bf16[32,4,2048]{2,1,0:T(4,128)(2,1)} %copy.34), calls=%async_computation.1 | async-start | bytes 1048576 | tf_op jit(solution)/shard_map/all_to_all | solution.py:202
  56.9 2.5 %collective-permute-start = (bf16[4,3,32,2048]{3,2,1,0:T(8,128)(2,1)S(1)}, bf16[4,3,32,2048]{3,2,1,0:T(8,128)(2,1)}, u32[]{:S(2)}, u32[]{:S(2)}) collective-permute-start(bf16[4,3,32,2048]{3,2,1,0:T(8,128)(2,1)S(1)} %all-to-all-done.2), channel_id=1, source_target_pairs={{0,1},{1,0},{2,3},{3,2},{4,5},{5,4},{6,7},{7,6},{8,9},{9,8},{10,11... | collective-permute-start | bytes 4718600 | tf_op jit(solution)/shard_map/ppermute | solution.py:183
  59.4 1.3 constant_dynamic-update-slice_fusion.1
  60.7 10.9 %all-to-all-done.1 = bf16[32,4,2048]{2,1,0:T(4,128)(2,1)S(1)} async-done(((bf16[32,4,2048]{2,1,0:T(4,128)(2,1)}), bf16[32,4,2048]{2,1,0:T(4,128)(2,1)S(1)}, u32[]{:S(2)}, u32[]{:S(2)}) %all-to-all-start.1) | async-done | bytes 524320 | tf_op jit(solution)/shard_map/all_to_all | solution.py:202
  71.6 1.1 fusion.36
  72.7 1.0 reshape.104
  73.8 2.1 %fusion.10 = f32[64,256]{1,0:T(8,128)} fusion(bf16[64,2048]{1,0:T(8,128)(2,1)S(1)} %reshape.102, bf16[1,2048,256]{2,1,0:T(8,128)(2,1)} %param.29), kind=kOutput, calls=%fused_computation.15 | convolution fusion | flops 67108864 | bytes 1376256 | tf_op jit(solution)/shard_map/dot_general | solution.py:155
  76.0 2.0 %convolution_convert_fusion.2 = bf16[64,2048]{1,0:T(8,128)(2,1)S(1)} fusion(bf16[64,2048]{1,0:T(8,128)(2,1)S(1)} %reshape.102, bf16[1,256,2048]{2,1,0:T(8,128)(2,1)S(1)} %copy-done, bf16[1,2048,256]{2,1,0:T(8,128)(2,1)} %param.30, f32[64,256]{1,0:T(8,128)} %fusion.10), kind=kOutput, calls=%fused_computation.2 | convolution fusion | flops 134447104 | bytes 2686976 | tf_op jit(solution)/shard_map/dot_general | solution.py:158
  78.0 0.9 reshape.103
  78.9 2.7 %constant_dynamic-update-slice_fusion = bf16[8,3,32,2048]{3,2,1,0:T(8,128)(2,1)} fusion(bf16[8,3,32,2048]{3,2,1,0:T(8,128)(2,1)} %constant_dynamic-update-slice_fusion.1, bf16[4,3,32,2048]{3,2,1,0:T(8,128)(2,1)} %collective-permute-done), kind=kLoop, calls=%fused_computation.53 | loop fusion | bytes 3145728 | tf_op jit(solution)/shard_map/concatenate | solution.py:209
  81.6 2.1 %fusion.35 = (bf16[8,1,32,2048]{3,2,1,0:T(8,128)(2,1)S(1)}, bf16[8,1,32,2048]{3,2,1,0:T(8,128)(2,1)S(1)}, bf16[8,1,32,2048]{3,2,1,0:T(8,128)(2,1)S(1)}) fusion(bf16[8,3,32,2048]{3,2,1,0:T(8,128)(2,1)} %constant_dynamic-update-slice_fusion), kind=kLoop, calls=%fused_computation.65 | loop fusion | bytes 6291456 | tf_op jit(solution)/shard_map/slice | solution.py:210
  83.8 1.1 fusion.39
  84.8 2.5 %convolution_convert_fusion.1 = bf16[64,2048]{1,0:T(8,128)(2,1)} fusion(bf16[256,2048]{1,0:T(8,128)(2,1)S(1)} %bitcast.54, f32[64,256]{1,0:T(8,128)} %fusion.39, bf16[64,2048]{1,0:T(8,128)(2,1)S(1)} %reshape.104, bf16[256,2048]{1,0:T(8,128)(2,1)S(1)} %bitcast.55), kind=kOutput, calls=%fused_computation.1 | convolution fusion | flops 134447104 | bytes 2686976 | tf_op jit(solution)/shard_map/dot_general | solution.py:158
  87.3 1.1 reshape.105
  88.4 2.3 %pad_maximum_fusion = bf16[32,4,2048]{2,1,0:T(4,128)(2,1)} fusion(bf16[32,2,2048]{2,1,0:T(2,128)(2,1)S(1)} %reshape.105, bf16[32,2,2048]{2,1,0:T(2,128)(2,1)} %reshape.103), kind=kLoop, calls=%fused_computation.18 | loop fusion | flops 1048576 | bytes 1048576 | tf_op jit(solution)/shard_map/concatenate | solution.py:214
  90.7 6.3 %all-to-all-start.3 = ((bf16[32,4,2048]{2,1,0:T(4,128)(2,1)}), bf16[32,4,2048]{2,1,0:T(4,128)(2,1)S(1)}, u32[]{:S(2)}, u32[]{:S(2)}) async-start(bf16[32,4,2048]{2,1,0:T(4,128)(2,1)} %pad_maximum_fusion), calls=%async_computation.3 | async-start | bytes 1048576 | tf_op jit(solution)/shard_map/all_to_all | solution.py:217
  97.0 0.7 reshape.107
  97.7 0.7 convert_element_type.50
  98.5 0.8 fusion.6
  99.3 0.8 fusion.28
  100.1 11.6 %all-to-all-done.3 = bf16[32,4,2048]{2,1,0:T(4,128)(2,1)S(1)} async-done(((bf16[32,4,2048]{2,1,0:T(4,128)(2,1)}), bf16[32,4,2048]{2,1,0:T(4,128)(2,1)S(1)}, u32[]{:S(2)}, u32[]{:S(2)}) %all-to-all-start.3) | async-done | bytes 524320 | tf_op jit(solution)/shard_map/all_to_all | solution.py:217
  112.1 0.6 copy.41
  112.7 7.4 %all-to-all-start.4 = ((bf16[8,16,256]{2,1,0:T(8,128)(2,1)}), bf16[8,16,256]{2,1,0:T(8,128)(2,1)S(1)}, u32[]{:S(2)}, u32[]{:S(2)}) async-start(bf16[8,16,256]{2,1,0:T(8,128)(2,1)} %bitcast.52), calls=%async_computation.4 | async-start | bytes 131072 | tf_op jit(solution)/shard_map/all_to_all | solution.py:228
  120.1 4.9 %all-to-all-done.4 = bf16[8,16,256]{2,1,0:T(8,128)(2,1)S(1)} async-done(((bf16[8,16,256]{2,1,0:T(8,128)(2,1)}), bf16[8,16,256]{2,1,0:T(8,128)(2,1)S(1)}, u32[]{:S(2)}, u32[]{:S(2)}) %all-to-all-start.4) | async-done | bytes 65568 | tf_op jit(solution)/shard_map/all_to_all | solution.py:228
  125.0 0.6 add_convert_fusion
  (38 shorter events, 2.3 us)
Async XLA Ops:
  0.0 76.0 %copy-start = (bf16[1,256,2048]{2,1,0:T(8,128)(2,1)S(1)}, bf16[1,256,2048]{2,1,0:T(8,128)(2,1)}, u32[]{:S(2)}) copy-start(bf16[1,256,2048]{2,1,0:T(8,128)(2,1)} %param.31) | copy-start | bytes 3145732
  0.0 14.1 %copy-start.6 = (s32[16,2]{0,1:T(2,128)S(1)}, s32[16,2]{0,1:T(2,128)}, u32[]{:S(2)}) copy-start(s32[16,2]{0,1:T(2,128)} %param.27) | copy-start | bytes 388
  0.0 14.6 %copy-start.2 = (bf16[32,2048]{1,0:T(8,128)(2,1)S(1)}, bf16[32,2048]{1,0:T(8,128)(2,1)}, u32[]{:S(2)}) copy-start(bf16[32,2048]{1,0:T(8,128)(2,1)} %param.35) | copy-start | bytes 393220
  0.0 14.6 %copy-start.3 = (bf16[32,2048]{1,0:T(8,128)(2,1)S(1)}, bf16[32,2048]{1,0:T(8,128)(2,1)}, u32[]{:S(2)}) copy-start(bf16[32,2048]{1,0:T(8,128)(2,1)} %param.34) | copy-start | bytes 393220
  0.0 14.6 %copy-start.4 = (bf16[32,2048]{1,0:T(8,128)(2,1)S(1)}, bf16[32,2048]{1,0:T(8,128)(2,1)}, u32[]{:S(2)}) copy-start(bf16[32,2048]{1,0:T(8,128)(2,1)} %param.33) | copy-start | bytes 393220
  7.5 16.0 %all-to-all-start = ((bf16[8,16,2048]{2,1,0:T(8,128)(2,1)}), bf16[8,16,2048]{2,1,0:T(8,128)(2,1)S(1)}, u32[]{:S(2)}, u32[]{:S(2)}) async-start(bf16[8,16,2048]{2,1,0:T(8,128)(2,1)} %shard_map.172), calls=%async_computation | async-start | bytes 1048576 | tf_op jit(solution)/shard_map/all_to_all | solution.py:175
  14.6 14.4 %copy-start.1 = (bf16[16,2048]{1,0:T(8,128)(2,1)S(1)}, bf16[16,2048]{1,0:T(8,128)(2,1)}, u32[]{:S(2)}) copy-start(bf16[16,2048]{1,0:T(8,128)(2,1)} %tok_ref.1) | copy-start | bytes 196612
  14.7 14.5 %copy-start.5 = (f32[2048]{0:T(1024)S(1)}, f32[2048]{0:T(1024)}, u32[]{:S(2)}) copy-start(f32[2048]{0:T(1024)} %param.26) | copy-start | bytes 24580
  24.8 23.3 %all-to-all-start.2 = ((bf16[4,3,32,2048]{3,2,1,0:T(8,128)(2,1)}), bf16[4,3,32,2048]{3,2,1,0:T(8,128)(2,1)S(1)}, u32[]{:S(2)}, u32[]{:S(2)}) async-start(bf16[4,3,32,2048]{3,2,1,0:T(8,128)(2,1)} %broadcast_in_dim.75), calls=%async_computation.2 | async-start | bytes 3145728 | tf_op jit(solution)/shard_map/all_to_all | solution.py:179
  28.4 0.6 copy-start.7
  29.2 31.5 %copy-start.8 = (f32[16]{0:T(128)}, f32[16]{0:T(128)S(1)}, u32[]{:S(2)}) copy-start(f32[16]{0:T(128)S(1)} %add_rsqrt_fusion) | copy-start | bytes 196
  48.1 23.5 %all-to-all-start.1 = ((bf16[32,4,2048]{2,1,0:T(4,128)(2,1)}), bf16[32,4,2048]{2,1,0:T(4,128)(2,1)S(1)}, u32[]{:S(2)}, u32[]{:S(2)}) async-start(bf16[32,4,2048]{2,1,0:T(4,128)(2,1)} %copy.34), calls=%async_computation.1 | async-start | bytes 1048576 | tf_op jit(solution)/shard_map/all_to_all | solution.py:202
  56.9 22.0 %collective-permute-start = (bf16[4,3,32,2048]{3,2,1,0:T(8,128)(2,1)S(1)}, bf16[4,3,32,2048]{3,2,1,0:T(8,128)(2,1)}, u32[]{:S(2)}, u32[]{:S(2)}) collective-permute-start(bf16[4,3,32,2048]{3,2,1,0:T(8,128)(2,1)S(1)} %all-to-all-done.2), channel_id=1, source_target_pairs={{0,1},{1,0},{2,3},{3,2},{4,5},{5,4},{6,7},{7,6},{8,9},{9,8},{10,11... | collective-permute-start | bytes 4718600 | tf_op jit(solution)/shard_map/ppermute | solution.py:183
  90.7 21.0 %all-to-all-start.3 = ((bf16[32,4,2048]{2,1,0:T(4,128)(2,1)}), bf16[32,4,2048]{2,1,0:T(4,128)(2,1)S(1)}, u32[]{:S(2)}, u32[]{:S(2)}) async-start(bf16[32,4,2048]{2,1,0:T(4,128)(2,1)} %pad_maximum_fusion), calls=%async_computation.3 | async-start | bytes 1048576 | tf_op jit(solution)/shard_map/all_to_all | solution.py:217
  112.7 12.3 %all-to-all-start.4 = ((bf16[8,16,256]{2,1,0:T(8,128)(2,1)}), bf16[8,16,256]{2,1,0:T(8,128)(2,1)S(1)}, u32[]{:S(2)}, u32[]{:S(2)}) async-start(bf16[8,16,256]{2,1,0:T(8,128)(2,1)} %bitcast.52), calls=%async_computation.4 | async-start | bytes 131072 | tf_op jit(solution)/shard_map/all_to_all | solution.py:228

commit v2 on v1

--- a/solution.py
+++ b/solution.py
@@ -5,9 +5,8 @@
 from jax.experimental.pallas import tpu as pltpu
 from jax.sharding import PartitionSpec as P
 
-HEADS = 16
+
 HEAD = 64
-KV_HEADS = 8
 EXPERTS = 32
 CAP = 2
 CACHE = 1024
@@ -15,6 +14,9 @@
 ROWS = 16
 LANES = 128
 HALF = 8
+MIB = 1 << 20
+MESSAGES = 512
+PART = 512
 epsilon = 1e-06
 NT = (((1,), (1,)), ((), ()))
 
@@ -117,7 +119,7 @@
 def attention(tokens, attn_gain, w_query, stick_bias, kv_cache, lengths, head_gain, w_attn_out):
     vmem = pl.BlockSpec(memory_space=pltpu.VMEM)
     smem = pl.BlockSpec(memory_space=pltpu.SMEM)
-    anywhere = pl.BlockSpec(memory_space=pl.ANY)
+    anywhere = pl.BlockSpec(memory_space=pltpu.HBM)
     return pl.pallas_call(
         attention_kernel,
         out_shape=jax.ShapeDtypeStruct((8, ROWS, WIDTH), jnp.bfloat16),
@@ -140,6 +142,147 @@
     )
 
 
+def dispatch_kernel(shares_ref, tok_ref, gain_ref, gate_ref, pick_ref, send_ref, res_ref, branch_ref):
+    total = tok_ref[...].astype(jnp.float32)
+    for i in range(8):
+        total = total + shares_ref[i].astype(jnp.float32)
+    res_ref[...] = total
+    scale = lax.rsqrt(jnp.mean(total * total, axis=-1, keepdims=True) + epsilon)
+    normed = (total * scale * gain_ref[...]).astype(jnp.bfloat16)
+    logit = jnp.sum(
+        normed.astype(jnp.float32) * gate_ref[...].astype(jnp.float32), axis=-1, keepdims=True
+    )
+    branch_ref[...] = jnp.broadcast_to(1.0 / (1.0 + jnp.exp(-logit)), branch_ref.shape)
+    stacked = jnp.concatenate([normed[:, q * PART : (q + 1) * PART] for q in range(4)], axis=0)
+    send_ref[...] = jnp.dot(
+        pick_ref[...], stacked, preferred_element_type=jnp.float32
+    ).astype(jnp.bfloat16)
+
+
+def dispatch(shares, tokens, ffn_gain, branch_gate, picks):
+    vmem = pl.BlockSpec(memory_space=pltpu.VMEM)
+    return pl.pallas_call(
+        dispatch_kernel,
+        out_shape=(
+            jax.ShapeDtypeStruct((MESSAGES, PART), jnp.bfloat16),
+            jax.ShapeDtypeStruct((ROWS, WIDTH), jnp.float32),
+            jax.ShapeDtypeStruct((ROWS, LANES), jnp.float32),
+        ),
+        in_specs=[vmem] * 5,
+        out_specs=(vmem, vmem, vmem),
+        compiler_params=pltpu.CompilerParams(vmem_limit_bytes=8 * MIB),
+        cost_estimate=pl.CostEstimate(
+            flops=40_000_000, bytes_accessed=1_500_000, transcendentals=100
+        ),
+    )(shares, tokens, ffn_gain.reshape(1, -1), branch_gate.reshape(1, -1), picks)
+
+
+def feed_kernel(
+    got_ref, eg_hbm, eu_hbm, ed_hbm, *rest,
+):
+    packs = rest[:8]
+    out_ref, wide_v, eg_v, eu_v, ed_v, dg_v, du_v, dd_v, e_sem, d_sem = rest[8:]
+    expert_copies = [
+        pltpu.make_async_copy(src, dst, e_sem.at[k])
+        for k, (src, dst) in enumerate(((eg_hbm, eg_v), (eu_hbm, eu_v), (ed_hbm, ed_v)))
+    ]
+    dense_copies = [
+        pltpu.make_async_copy(pack.at[k], dst.at[pl.ds(32 * i, 32), :], d_sem.at[3 * i + k])
+        for k, dst in enumerate((dg_v, du_v, dd_v))
+        for i, pack in enumerate(packs)
+    ]
+    for copy in expert_copies + dense_copies:
+        copy.start()
+    for l in range(4):
+        wide_v[l] = got_ref[:, l * LANES : (l + 1) * LANES].astype(jnp.float32)
+
+    def picked(kind, q, slot):
+        return pl.ds(kind * 8 + q * 2 + slot, 32, stride=16)
+
+    def unpacked(kind):
+        parts = [
+            jnp.concatenate([wide_v[l, picked(kind, q, slot), :] for slot in range(2)], axis=0)
+            for q in range(4)
+            for l in range(4)
+        ]
+        return jnp.concatenate(parts, axis=1).astype(jnp.bfloat16)
+
+    def packed(kind, value):
+        for q in range(4):
+            for l in range(4):
+                at = q * PART + l * LANES
+                for slot in range(2):
+                    wide_v[l, picked(kind, q, slot), :] = value[
+                        slot * 32 : slot * 32 + 32, at : at + LANES
+                    ]
+
+    rows = unpacked(0)
+    dense_rows = unpacked(1)
+    expert_copies[0].wait()
+    a = jnp.dot(rows, eg_v[...], preferred_element_type=jnp.float32)
+    expert_copies[1].wait()
+    b = jnp.dot(rows, eu_v[...], preferred_element_type=jnp.float32)
+    hidden = (a / (1.0 + jnp.exp(-a)) * b).astype(jnp.bfloat16)
+    expert_copies[2].wait()
+    packed(0, jnp.dot(hidden, ed_v[...], preferred_element_type=jnp.float32))
+    for copy in dense_copies:
+        copy.wait()
+    a = lax.dot_general(dense_rows, dg_v[...], NT, preferred_element_type=jnp.float32)
+    b = lax.dot_general(dense_rows, du_v[...], NT, preferred_element_type=jnp.float32)
+    hidden = (a / (1.0 + jnp.exp(-a)) * b).astype(jnp.bfloat16)
+    packed(1, jnp.dot(hidden, dd_v[...], preferred_element_type=jnp.float32))
+    for l in range(4):
+        out_ref[:, l * LANES : (l + 1) * LANES] = wide_v[l].astype(jnp.bfloat16)
+
+
+def feed(got, gate, up, down, packs):
+    vmem = pl.BlockSpec(memory_space=pltpu.VMEM)
+    hbm = pl.BlockSpec(memory_space=pltpu.HBM)
+    return pl.pallas_call(
+        feed_kernel,
+        out_shape=jax.ShapeDtypeStruct((MESSAGES, PART), jnp.bfloat16),
+        in_specs=[vmem] + [hbm] * 11,
+        out_specs=vmem,
+        scratch_shapes=[
+            pltpu.VMEM((4, MESSAGES, LANES), jnp.float32),
+            pltpu.VMEM((WIDTH, 256), jnp.bfloat16),
+            pltpu.VMEM((WIDTH, 256), jnp.bfloat16),
+            pltpu.VMEM((256, WIDTH), jnp.bfloat16),
+            pltpu.VMEM((256, WIDTH), jnp.bfloat16),
+            pltpu.VMEM((256, WIDTH), jnp.bfloat16),
+            pltpu.VMEM((256, WIDTH), jnp.bfloat16),
+            pltpu.SemaphoreType.DMA((3,)),
+            pltpu.SemaphoreType.DMA((24,)),
+        ],
+        compiler_params=pltpu.CompilerParams(vmem_limit_bytes=60 * 1024 * 1024 - 640 * 1024),
+        cost_estimate=pl.CostEstimate(
+            flops=1_000_000_000, bytes_accessed=7_000_000, transcendentals=40_000
+        ),
+    )(got, gate, up, down, *packs)
+
+
+def combine_kernel(mix_ref, got_ref, out_ref):
+    total = jnp.dot(mix_ref[...], got_ref[...], preferred_element_type=jnp.float32)
+    total = total.astype(jnp.bfloat16)
+    for t in range(8):
+        q, h = divmod(t, 2)
+        out_ref[t] = total[q * ROWS : (q + 1) * ROWS, h * 256 : (h + 1) * 256]
+
+
+def combine(mix, returned):
+    vmem = pl.BlockSpec(memory_space=pltpu.VMEM)
+    return pl.pallas_call(
+        combine_kernel,
+        out_shape=jax.ShapeDtypeStruct((8, ROWS, 256), jnp.bfloat16),
+        in_specs=[vmem] * 2,
+        out_specs=vmem,
+        compiler_params=pltpu.CompilerParams(vmem_limit_bytes=4 * MIB),
+        cost_estimate=pl.CostEstimate(
+            flops=40_000_000, bytes_accessed=600_000, transcendentals=0
+        ),
+    )(mix, returned)
+
+
 def slot_table(routes):
     ids = jnp.arange(EXPERTS, dtype=jnp.int32)
     hits = (routes[..., None] == ids).astype(jnp.int32)
@@ -151,19 +294,12 @@
     return (routes[:, :, None, None] == ids[:, None]) & (rank[:, :, None, None] == slot)
 
 
-def gated(rows, gate, up, down, dims):
-    a = lax.dot_general(rows, gate, dims, preferred_element_type=jnp.float32)
-    b = lax.dot_general(rows, up, dims, preferred_element_type=jnp.float32)
-    hidden = (jax.nn.silu(a) * b).astype(jnp.bfloat16)
-    return jnp.dot(hidden, down, preferred_element_type=jnp.float32).astype(jnp.bfloat16)
-
-
-def shards(
+def layer(
     tokens, attn_gain, w_query, stick_bias, kv_cache, lengths, head_gain, w_attn_out, ffn_gain,
     route_expert, route_weight, w_exp_gate, w_exp_up, w_exp_down, branch_gate,
     w_dense_gate, w_dense_up, w_dense_down,
 ):
-    single = jnp.float32
+    single, half = jnp.float32, jnp.bfloat16
     t = lax.axis_index("tp")
     core = t % 2
     copies = attention(
@@ -175,64 +311,51 @@
     shares = lax.all_to_all(copies, "tp", 0, 0, tiled=True)
 
     own = jnp.stack([w_dense_gate, w_dense_up, w_dense_down])
-    groups = [[z * 4 + x for x in range(4)] for z in range(8)]
-    four = lax.all_to_all(
-        jnp.broadcast_to(own[None], (4, *own.shape)), "ep", 0, 0, tiled=True,
-        axis_index_groups=groups,
-    )
-    other = lax.ppermute(four, "tp", [(i, i ^ 1) for i in range(8)])
+    packs = [own]
+    for m in (1, 4, 5):
+        packs.append(lax.ppermute(own, "ep", [(i, i ^ m) for i in range(32)]))
+    for k in range(4):
+        packs.append(lax.ppermute(packs[k], "tp", [(i, i ^ 1) for i in range(8)]))
 
     table = slot_table(route_expert)
     taken = jnp.any(table, axis=1)
+    dest = jnp.arange(32)
+    first = 4 * (2 * (dest // 4 % 2) + dest % 2) + 2 * core
+    quarter = first[:, None] + jnp.arange(2)
     expert_dest = jnp.moveaxis(taken, 0, -1)
-    quarter = 4 * (jnp.arange(32) % 4)[:, None] + 2 * core + jnp.arange(2)
     dense_dest = quarter[..., None] == jnp.arange(ROWS)
-    picks = jnp.concatenate([expert_dest, dense_dest], axis=1)
-
-    residual = tokens.astype(single) + jnp.sum(shares.astype(single), axis=0)
-    scale = lax.rsqrt(jnp.mean(residual * residual, axis=-1, keepdims=True) + epsilon)
-    normed = (residual * scale * ffn_gain).astype(jnp.bfloat16)
-    branch = jax.nn.sigmoid(jnp.dot(normed, branch_gate, preferred_element_type=single))
-    branch = branch.astype(jnp.bfloat16)
-    residual_cols = lax.dynamic_slice_in_dim(residual, t * 256, 256, 1)
-
-    send = jnp.einsum(
-        "cks,sd->ckd", picks.astype(jnp.bfloat16), normed, preferred_element_type=single
-    ).astype(jnp.bfloat16)
-    got = lax.all_to_all(send, "ep", 0, 0, tiled=True)
-
-    expert_rows = got[:, :2].reshape(64, WIDTH)
-    dense_rows = got[:, 2:].reshape(64, WIDTH)
-    expert_out = gated(
-        expert_rows, w_exp_gate[0], w_exp_up[0], w_exp_down[0], (((1,), (0,)), ((), ()))
-    )
-    weights = jnp.concatenate([four, other], axis=0)
-    gate_all = weights[:, 0].reshape(256, WIDTH)
-    up_all = weights[:, 1].reshape(256, WIDTH)
-    down_all = weights[:, 2].reshape(256, WIDTH)
-    dense_out = gated(dense_rows, gate_all, up_all, down_all, NT)
-    back = jnp.concatenate(
-        [expert_out.reshape(32, 2, WIDTH), dense_out.reshape(32, 2, WIDTH)], axis=1
-    )
-    returned = lax.all_to_all(back, "ep", 0, 0, tiled=True).reshape(128, WIDTH)
+    both = jnp.stack([expert_dest, dense_dest], axis=1)
+    eye = jnp.arange(4)[:, None] == jnp.arange(4)
+    picks = both[:, :, None, :, None, :] & eye[None, None, :, None, :, None]
+    picks = picks.reshape(MESSAGES, 4 * ROWS).astype(half)
+
+    send, residual, branch = dispatch(shares, tokens, ffn_gain, branch_gate, picks)
+    got = lax.all_to_all(send.reshape(32, 16, PART), "ep", 0, 0, tiled=True)
+
+    back = feed(
+        got.reshape(MESSAGES, PART), w_exp_gate[0], w_exp_up[0], w_exp_down[0], packs
+    )
+    returned = lax.all_to_all(back.reshape(32, 16, PART), "ep", 0, 0, tiled=True)
 
     weight = jnp.sum(
         jnp.where(table, route_weight[:, :, None, None].astype(single), 0.0), axis=1
-    ).astype(jnp.bfloat16)
+    )
     dense_weight = jnp.where(
-        jnp.moveaxis(dense_dest, -1, 0), branch[:, None, None], jnp.bfloat16(0)
-    )
-    mix = jnp.concatenate([weight, dense_weight], axis=2).reshape(ROWS, 128)
-    partial = jnp.dot(mix, returned, preferred_element_type=single).astype(jnp.bfloat16)
-    partial = jnp.moveaxis(partial.reshape(ROWS, 8, 256), 1, 0)
+        jnp.moveaxis(dense_dest, -1, 0), branch[:, :1, None], 0.0
+    )
+    mix = jnp.stack([weight, dense_weight], axis=2).astype(half)
+    mix = jnp.where(eye[:, None, None, None, :, None], mix[None, :, :, :, None, :], half(0))
+    mix = mix.reshape(4 * ROWS, MESSAGES)
+    partial = combine(mix, returned.reshape(MESSAGES, PART))
     columns = lax.all_to_all(partial, "tp", 0, 0, tiled=True)
+    residual_cols = lax.dynamic_slice_in_dim(residual, t * 256, 256, 1)
     total = jnp.sum(columns.astype(single), axis=0)
-    return (residual_cols + total).astype(jnp.bfloat16)
+    return (residual_cols + total).astype(half)
 
 
 def solution(mesh):
     return jax.shard_map(
-        shards,
+        layer,
         mesh=mesh,
         in_specs=(
             P("ep", None), P(), P(None, "tp"), P("tp"), P("ep", "tp", None, None), P("ep"),

time: 126 us -> 113 us (0.90)
  local copies, waits for them, and re-layouts: 14.8 us -> 1.91 us
  matrix products: 9.28 us -> 0 us
  Pallas kernels: 7.45 us -> 16.4 us
  starting transfers between devices: 35.2 us -> 41.8 us
  waiting for transfers between devices: 53.5 us -> 50.1 us
  other arithmetic: 5.24 us -> 2.07 us
    all_to_all x5 -> x4, waiting for transfers between devices: 53.5 us -> 28.2 us  [the longest x1 15.5 us: layer(): lax.all_to_all(back.reshape(32, 16, PART), 'ep', 0, 0, tiled=True)]
    ppermute x1 -> x7, waiting for transfers between devices: 0.01 us -> 21.9 us  [the longest x3 20.5 us: layer(): packs.append(lax.ppermute(own, 'ep', [(i, i ^ m) for i in range(32)]))]
    dot_general x7 -> x0, matrix products: 9.28 us -> none  [the longest x2 4.48 us: gated(): jnp.dot(hidden, down, preferred_element_type=jnp.float32)]
    pallas_call x0 -> x3, Pallas kernels: none -> 8.92 us  [the longest x1 6.85 us: feed(): pl.pallas_call(feed_kernel, out_shape=jax.ShapeDtypeStruct((MESSAGES, PAR...]
    ppermute x1 -> x7, starting transfers between devices: 2.47 us -> 11.4 us  [the longest x4 8.65 us: layer(): packs.append(lax.ppermute(packs[k], 'tp', [(i, i ^ 1) for i in range(8)]))]
    reshape x5 -> x1, local copies, waits for them, and re-layouts: 3.8 us -> 0.01 us  [dispatch(): branch_gate.reshape(1, -1)]
    slice x2 -> x1, local copies, waits for them, and re-layouts: 3.21 us -> 0.11 us  [layer(): branch[:, :1, None]]
    concatenate x1 -> x0, local copies, waits for them, and re-layouts: 2.73 us -> none  [shards(): weights = jnp.concatenate([four, other], axis=0)]
  transfers between devices with their start and end apart: 6 -> 11, of which waited for: 5 -> 7; matrix products, arithmetic and copies ran while one was open for 11% -> 2% of each run, Pallas kernels for 0% -> 0%
where the time goes in v2:
time: 113 us
  waiting for transfers between devices  50.1 us (44%)
  starting transfers between devices  41.8 us (37%)
  Pallas kernels  16.4 us (15%)
  other arithmetic  2.07 us (2%)
  local copies, waits for them, and re-layouts  1.91 us (2%)
    ppermute x3, waiting for transfers between devices, layer(): packs.append(lax.ppermute(own, 'ep', [(i, i ^ m) for i in range(32)]))  20.5 us
    all_to_all x1, waiting for transfers between devices, layer(): lax.all_to_all(back.reshape(32, 16, PART), 'ep', 0, 0, tiled=True)  15.5 us
    all_to_all x1, starting transfers between devices, layer(): got = lax.all_to_all(send.reshape(32, 16, PART), 'ep', 0, 0, tiled=True)  10.4 us
    ppermute x4, starting transfers between devices, layer(): packs.append(lax.ppermute(packs[k], 'tp', [(i, i ^ 1) for i in range(8)]))  8.65 us
    all_to_all x1, starting transfers between devices, layer(): lax.all_to_all(back.reshape(32, 16, PART), 'ep', 0, 0, tiled=True)  8.02 us
    all_to_all x1, waiting for transfers between devices, layer(): shares = lax.all_to_all(copies, 'tp', 0, 0, tiled=True)  7.8 us
    pallas_call x1, Pallas kernels, attention(): pl.pallas_call(attention_kernel, out_shape=jax.ShapeDtypeStruct((8, ROWS,...  7.45 us
    pallas_call x1, Pallas kernels, feed(): pl.pallas_call(feed_kernel, out_shape=jax.ShapeDtypeStruct((MESSAGES, PAR...  6.85 us
  transfers between devices with their start and end apart: 11, of which 7 were waited for; matrix products, arithmetic and copies ran while one was open for 2% of the time, Pallas kernels for 0%

profile of v2, /device:TPU:1, one launch (start us, length us, event | category | flops | bytes accessed | tf_op | source)
XLA Modules:
  0.0 112.6 jit_solution(18209210366560453045)
XLA Ops:
  0.0 7.5 %shard_map.172 = bf16[8,16,2048]{2,1,0:T(8,128)(2,1)} custom-call(s32[16]{0:T(128)} %len_ref.1, f32[2]{0:T(128)} %bias_ref.1, bf16[16,2048]{1,0:T(8,128)(2,1)} %tok_ref.3, f32[1,2048]{1,0:T(1,128)} %bitcast.33, f32[1,128]{1,0:T(1,128)} %bitcast.34, bf16[2048,128]{1,0:T(8,128)(2,1)} %wq_hbm.1, bf16[16,1,1024,128]{3,2,1,0:T(8,128)(2,1)} %kv_hbm.1, ...), custom_call_target="tpu_custom_call" | custom-call | flops 400000000 | bytes 6000000 | tf_op jit(solution)/shard_map/pallas_call | solution.py:123
  7.5 6.6 %all-to-all-start = ((bf16[8,16,2048]{2,1,0:T(8,128)(2,1)}), bf16[8,16,2048]{2,1,0:T(8,128)(2,1)S(1)}, u32[]{:S(2)}, u32[]{:S(2)}) async-start(bf16[8,16,2048]{2,1,0:T(8,128)(2,1)} %shard_map.172), calls=%async_computation | async-start | bytes 1048576 | tf_op jit(solution)/shard_map/all_to_all | solution.py:311
  14.3 0.1 select_reduce_fusion
  14.4 0.2 select_reduce_fusion.1
  14.7 0.1 copy.33
  15.0 0.4 and_convert_fusion
  15.4 0.3 reshape.189.pick_ref
  15.7 7.8 %all-to-all-done.shares_ref = bf16[8,16,2048]{2,1,0:T(8,128)(2,1)S(1)} async-done(((bf16[8,16,2048]{2,1,0:T(8,128)(2,1)}), bf16[8,16,2048]{2,1,0:T(8,128)(2,1)S(1)}, u32[]{:S(2)}, u32[]{:S(2)}) %all-to-all-start) | async-done | bytes 524320 | tf_op jit(solution)/shard_map/all_to_all | solution.py:311
  23.5 1.3 %shard_map.173 = (bf16[512,512]{1,0:T(8,128)(2,1)}, f32[16,2048]{1,0:T(8,128)S(1)}, f32[16,128]{1,0:T(8,128)S(1)}) custom-call(bf16[8,16,2048]{2,1,0:T(8,128)(2,1)S(1)} %all-to-all-done.shares_ref, bf16[16,2048]{1,0:T(8,128)(2,1)S(1)} %copy-done, f32[1,2048]{1,0:T(1,128)S(1)} %bitcast.22, bf16[1,2048]{1,0:T(2,128)(2,1)S(1)} %reshape.184.gate_ref, ...), custom_call_target="tpu_custom_call" | custom-call | flops 40000000 | bytes 1500000 | tf_op jit(solution)/shard_map/pallas_call | solution.py:164
  24.7 10.4 %all-to-all-start.1 = ((bf16[32,16,512]{2,1,0:T(8,128)(2,1)}), bf16[32,16,512]{2,1,0:T(8,128)(2,1)S(1)}, u32[]{:S(2)}, u32[]{:S(2)}) async-start(bf16[32,16,512]{2,1,0:T(8,128)(2,1)} %bitcast.6), calls=%async_computation.1 | async-start | bytes 1048576 | tf_op jit(solution)/shard_map/all_to_all | solution.py:333
  35.2 1.3 %collective-permute-start = (bf16[3,32,2048]{2,1,0:T(8,128)(2,1)S(1)}, bf16[3,32,2048]{2,1,0:T(8,128)(2,1)S(1)}, u32[]{:S(2)}, u32[]{:S(2)}) collective-permute-start(bf16[3,32,2048]{2,1,0:T(8,128)(2,1)S(1)} %pad_maximum_fusion.rest_0_), channel_id=1, source_target_pairs={{0,8},{8,0},{16,24},{24,16},{32,40},{40,32},{48,56},{56,48},{64,72... | collective-permute-start | bytes 1179656 | tf_op jit(solution)/shard_map/ppermute | solution.py:316
  36.5 1.2 %collective-permute-start.1 = (bf16[3,32,2048]{2,1,0:T(8,128)(2,1)S(1)}, bf16[3,32,2048]{2,1,0:T(8,128)(2,1)S(1)}, u32[]{:S(2)}, u32[]{:S(2)}) collective-permute-start(bf16[3,32,2048]{2,1,0:T(8,128)(2,1)S(1)} %pad_maximum_fusion.rest_0_), channel_id=1, source_target_pairs={{0,32},{8,40},{16,48},{24,56},{32,0},{40,8},{48,16},{56,24},{64,96... | collective-permute-start | bytes 1179656 | tf_op jit(solution)/shard_map/ppermute | solution.py:316
  37.7 0.2 collective-permute-start.2
  38.0 2.1 %collective-permute-start.3 = (bf16[3,32,2048]{2,1,0:T(8,128)(2,1)S(1)}, bf16[3,32,2048]{2,1,0:T(8,128)(2,1)S(1)}, u32[]{:S(2)}, u32[]{:S(2)}) collective-permute-start(bf16[3,32,2048]{2,1,0:T(8,128)(2,1)S(1)} %pad_maximum_fusion.rest_0_), channel_id=1, source_target_pairs={{0,1},{1,0},{2,3},{3,2},{4,5},{5,4},{6,7},{7,6},{8,9},{9,8},{10,11... | collective-permute-start | bytes 1179656 | tf_op jit(solution)/shard_map/ppermute | solution.py:318
  40.1 9.8 %collective-permute-done.rest_1_ = bf16[3,32,2048]{2,1,0:T(8,128)(2,1)S(1)} collective-permute-done((bf16[3,32,2048]{2,1,0:T(8,128)(2,1)S(1)}, bf16[3,32,2048]{2,1,0:T(8,128)(2,1)S(1)}, u32[]{:S(2)}, u32[]{:S(2)}) %collective-permute-start) | collective-permute-done | bytes 393248 | tf_op jit(solution)/shard_map/ppermute | solution.py:316
  49.9 2.1 %collective-permute-start.4 = (bf16[3,32,2048]{2,1,0:T(8,128)(2,1)S(1)}, bf16[3,32,2048]{2,1,0:T(8,128)(2,1)S(1)}, u32[]{:S(2)}, u32[]{:S(2)}) collective-permute-start(bf16[3,32,2048]{2,1,0:T(8,128)(2,1)S(1)} %collective-permute-done.rest_1_), channel_id=1, source_target_pairs={{0,1},{1,0},{2,3},{3,2},{4,5},{5,4},{6,7},{7,6},{8,9},{9,8},{10,11... | collective-permute-start | bytes 1179656 | tf_op jit(solution)/shard_map/ppermute | solution.py:318
  52.0 4.2 %collective-permute-done.1.rest_2_ = bf16[3,32,2048]{2,1,0:T(8,128)(2,1)S(1)} collective-permute-done((bf16[3,32,2048]{2,1,0:T(8,128)(2,1)S(1)}, bf16[3,32,2048]{2,1,0:T(8,128)(2,1)S(1)}, u32[]{:S(2)}, u32[]{:S(2)}) %collective-permute-start.1) | collective-permute-done | bytes 393248 | tf_op jit(solution)/shard_map/ppermute | solution.py:316
  56.2 2.8 %collective-permute-start.5 = (bf16[3,32,2048]{2,1,0:T(8,128)(2,1)S(1)}, bf16[3,32,2048]{2,1,0:T(8,128)(2,1)S(1)}, u32[]{:S(2)}, u32[]{:S(2)}) collective-permute-start(bf16[3,32,2048]{2,1,0:T(8,128)(2,1)S(1)} %collective-permute-done.1.rest_2_), channel_id=1, source_target_pairs={{0,1},{1,0},{2,3},{3,2},{4,5},{5,4},{6,7},{7,6},{8,9},{9,8},{10,11... | collective-permute-start | bytes 1179656 | tf_op jit(solution)/shard_map/ppermute | solution.py:318
  58.9 6.5 %collective-permute-done.2.rest_3_ = bf16[3,32,2048]{2,1,0:T(8,128)(2,1)S(1)} collective-permute-done((bf16[3,32,2048]{2,1,0:T(8,128)(2,1)S(1)}, bf16[3,32,2048]{2,1,0:T(8,128)(2,1)S(1)}, u32[]{:S(2)}, u32[]{:S(2)}) %collective-permute-start.2) | collective-permute-done | bytes 393248 | tf_op jit(solution)/shard_map/ppermute | solution.py:316
  65.4 1.7 %collective-permute-start.6 = (bf16[3,32,2048]{2,1,0:T(8,128)(2,1)S(1)}, bf16[3,32,2048]{2,1,0:T(8,128)(2,1)}, u32[]{:S(2)}, u32[]{:S(2)}) collective-permute-start(bf16[3,32,2048]{2,1,0:T(8,128)(2,1)S(1)} %collective-permute-done.2.rest_3_), channel_id=1, source_target_pairs={{0,1},{1,0},{2,3},{3,2},{4,5},{5,4},{6,7},{7,6},{8,9},{9,8},{10,11... | collective-permute-start | bytes 1179656 | tf_op jit(solution)/shard_map/ppermute | solution.py:318
  67.1 1.4 %collective-permute-done.6.rest_7_ = bf16[3,32,2048]{2,1,0:T(8,128)(2,1)} collective-permute-done((bf16[3,32,2048]{2,1,0:T(8,128)(2,1)S(1)}, bf16[3,32,2048]{2,1,0:T(8,128)(2,1)}, u32[]{:S(2)}, u32[]{:S(2)}) %collective-permute-start.6) | collective-permute-done | bytes 393248 | tf_op jit(solution)/shard_map/ppermute | solution.py:318
  68.6 0.7 copy-done.2
  69.4 6.8 %shard_map.174 = bf16[512,512]{1,0:T(8,128)(2,1)} custom-call(bf16[512,512]{1,0:T(8,128)(2,1)} %bitcast.23, bf16[2048,256]{1,0:T(8,128)(2,1)} %bitcast.25, bf16[2048,256]{1,0:T(8,128)(2,1)} %bitcast.26, bf16[256,2048]{1,0:T(8,128)(2,1)} %bitcast.27, bf16[3,32,2048]{2,1,0:T(8,128)(2,1)} %copy-done.3, bf16[3,32,2048]{2,1,0:T(8,128)(2,1)} %copy-done.4, ...), custom_call_target="tpu_custom_call" | custom-call | flops 1000000000 | bytes 7000000 | tf_op jit(solution)/shard_map/pallas_call | solution.py:241
  76.2 8.0 %all-to-all-start.2 = ((bf16[32,16,512]{2,1,0:T(8,128)(2,1)}), bf16[32,16,512]{2,1,0:T(8,128)(2,1)S(1)}, u32[]{:S(2)}, u32[]{:S(2)}) async-start(bf16[32,16,512]{2,1,0:T(8,128)(2,1)} %bitcast.24), calls=%async_computation.2 | async-start | bytes 1048576 | tf_op jit(solution)/shard_map/all_to_all | solution.py:338
  84.3 0.1 slice_reduce_fusion
  84.7 0.3 broadcast_select_fusion
  84.9 0.3 select_n.75
  85.3 15.5 %all-to-all-done.2 = bf16[32,16,512]{2,1,0:T(8,128)(2,1)S(1)} async-done(((bf16[32,16,512]{2,1,0:T(8,128)(2,1)}), bf16[32,16,512]{2,1,0:T(8,128)(2,1)S(1)}, u32[]{:S(2)}, u32[]{:S(2)}) %all-to-all-start.2) | async-done | bytes 524320 | tf_op jit(solution)/shard_map/all_to_all | solution.py:338
  100.9 0.8 shard_map.175
  101.7 5.4 %all-to-all-start.3 = ((bf16[8,16,256]{2,1,0:T(8,128)(2,1)}), bf16[8,16,256]{2,1,0:T(8,128)(2,1)S(1)}, u32[]{:S(2)}, u32[]{:S(2)}) async-start(bf16[8,16,256]{2,1,0:T(8,128)(2,1)} %shard_map.175), calls=%async_computation.3 | async-start | bytes 131072 | tf_op jit(solution)/shard_map/all_to_all | solution.py:350
  107.1 4.9 %all-to-all-done.3 = bf16[8,16,256]{2,1,0:T(8,128)(2,1)S(1)} async-done(((bf16[8,16,256]{2,1,0:T(8,128)(2,1)}), bf16[8,16,256]{2,1,0:T(8,128)(2,1)S(1)}, u32[]{:S(2)}, u32[]{:S(2)}) %all-to-all-start.3) | async-done | bytes 65568 | tf_op jit(solution)/shard_map/all_to_all | solution.py:350
  112.0 0.6 add_convert_fusion
  (55 shorter events, 0.9 us)
Async XLA Ops:
  0.0 23.5 %copy-start = (bf16[16,2048]{1,0:T(8,128)(2,1)S(1)}, bf16[16,2048]{1,0:T(8,128)(2,1)}, u32[]{:S(2)}) copy-start(bf16[16,2048]{1,0:T(8,128)(2,1)} %tok_ref.3) | copy-start | bytes 196612
  0.0 14.1 %copy-start.13 = (s32[16,2]{0,1:T(2,128)S(1)}, s32[16,2]{0,1:T(2,128)}, u32[]{:S(2)}) copy-start(s32[16,2]{0,1:T(2,128)} %param.27) | copy-start | bytes 388
  0.0 15.6 %copy-start.14 = (bf16[2048]{0:T(1024)(128)(2,1)S(1)}, bf16[2048]{0:T(1024)(128)(2,1)}, u32[]{:S(2)}) copy-start(bf16[2048]{0:T(1024)(128)(2,1)} %param.32) | copy-start | bytes 12292
  0.0 23.5 %copy-start.1 = (f32[2048]{0:T(1024)S(1)}, f32[2048]{0:T(1024)}, u32[]{:S(2)}) copy-start(f32[2048]{0:T(1024)} %param.26) | copy-start | bytes 24580
  0.0 35.1 %copy-start.10 = (bf16[32,2048]{1,0:T(8,128)(2,1)S(1)}, bf16[32,2048]{1,0:T(8,128)(2,1)}, u32[]{:S(2)}) copy-start(bf16[32,2048]{1,0:T(8,128)(2,1)} %param.35) | copy-start | bytes 393220
  0.0 35.1 %copy-start.11 = (bf16[32,2048]{1,0:T(8,128)(2,1)S(1)}, bf16[32,2048]{1,0:T(8,128)(2,1)}, u32[]{:S(2)}) copy-start(bf16[32,2048]{1,0:T(8,128)(2,1)} %param.34) | copy-start | bytes 393220
  0.0 35.1 %copy-start.12 = (bf16[32,2048]{1,0:T(8,128)(2,1)S(1)}, bf16[32,2048]{1,0:T(8,128)(2,1)}, u32[]{:S(2)}) copy-start(bf16[32,2048]{1,0:T(8,128)(2,1)} %param.33) | copy-start | bytes 393220
  7.5 16.0 %all-to-all-start = ((bf16[8,16,2048]{2,1,0:T(8,128)(2,1)}), bf16[8,16,2048]{2,1,0:T(8,128)(2,1)S(1)}, u32[]{:S(2)}, u32[]{:S(2)}) async-start(bf16[8,16,2048]{2,1,0:T(8,128)(2,1)} %shard_map.172), calls=%async_computation | async-start | bytes 1048576 | tf_op jit(solution)/shard_map/all_to_all | solution.py:311
  24.7 43.8 %all-to-all-start.1 = ((bf16[32,16,512]{2,1,0:T(8,128)(2,1)}), bf16[32,16,512]{2,1,0:T(8,128)(2,1)S(1)}, u32[]{:S(2)}, u32[]{:S(2)}) async-start(bf16[32,16,512]{2,1,0:T(8,128)(2,1)} %bitcast.6), calls=%async_computation.1 | async-start | bytes 1048576 | tf_op jit(solution)/shard_map/all_to_all | solution.py:333
  35.2 33.4 %copy-start.3 = (bf16[3,32,2048]{2,1,0:T(8,128)(2,1)}, bf16[3,32,2048]{2,1,0:T(8,128)(2,1)S(1)}, u32[]{:S(2)}) copy-start(bf16[3,32,2048]{2,1,0:T(8,128)(2,1)S(1)} %pad_maximum_fusion.rest_0_) | copy-start | bytes 1179652
  35.2 14.6 %collective-permute-start = (bf16[3,32,2048]{2,1,0:T(8,128)(2,1)S(1)}, bf16[3,32,2048]{2,1,0:T(8,128)(2,1)S(1)}, u32[]{:S(2)}, u32[]{:S(2)}) collective-permute-start(bf16[3,32,2048]{2,1,0:T(8,128)(2,1)S(1)} %pad_maximum_fusion.rest_0_), channel_id=1, source_target_pairs={{0,8},{8,0},{16,24},{24,16},{32,40},{40,32},{48,56},{56,48},{64,72... | collective-permute-start | bytes 1179656 | tf_op jit(solution)/shard_map/ppermute | solution.py:316
  36.5 19.6 %collective-permute-start.1 = (bf16[3,32,2048]{2,1,0:T(8,128)(2,1)S(1)}, bf16[3,32,2048]{2,1,0:T(8,128)(2,1)S(1)}, u32[]{:S(2)}, u32[]{:S(2)}) collective-permute-start(bf16[3,32,2048]{2,1,0:T(8,128)(2,1)S(1)} %pad_maximum_fusion.rest_0_), channel_id=1, source_target_pairs={{0,32},{8,40},{16,48},{24,56},{32,0},{40,8},{48,16},{56,24},{64,96... | collective-permute-start | bytes 1179656 | tf_op jit(solution)/shard_map/ppermute | solution.py:316
  37.7 27.7 %collective-permute-start.2 = (bf16[3,32,2048]{2,1,0:T(8,128)(2,1)S(1)}, bf16[3,32,2048]{2,1,0:T(8,128)(2,1)S(1)}, u32[]{:S(2)}, u32[]{:S(2)}) collective-permute-start(bf16[3,32,2048]{2,1,0:T(8,128)(2,1)S(1)} %pad_maximum_fusion.rest_0_), channel_id=1, source_target_pairs={{0,40},{8,32},{16,56},{24,48},{32,8},{40,0},{48,24},{56,16},{64,10... | collective-permute-start | bytes 1179656 | tf_op jit(solution)/shard_map/ppermute | solution.py:316
  38.0 29.1 %collective-permute-start.3 = (bf16[3,32,2048]{2,1,0:T(8,128)(2,1)S(1)}, bf16[3,32,2048]{2,1,0:T(8,128)(2,1)S(1)}, u32[]{:S(2)}, u32[]{:S(2)}) collective-permute-start(bf16[3,32,2048]{2,1,0:T(8,128)(2,1)S(1)} %pad_maximum_fusion.rest_0_), channel_id=1, source_target_pairs={{0,1},{1,0},{2,3},{3,2},{4,5},{5,4},{6,7},{7,6},{8,9},{9,8},{10,11... | collective-permute-start | bytes 1179656 | tf_op jit(solution)/shard_map/ppermute | solution.py:318
  49.9 18.7 %copy-start.4 = (bf16[3,32,2048]{2,1,0:T(8,128)(2,1)}, bf16[3,32,2048]{2,1,0:T(8,128)(2,1)S(1)}, u32[]{:S(2)}) copy-start(bf16[3,32,2048]{2,1,0:T(8,128)(2,1)S(1)} %collective-permute-done.rest_1_) | copy-start | bytes 1179652
  49.9 17.2 %collective-permute-start.4 = (bf16[3,32,2048]{2,1,0:T(8,128)(2,1)S(1)}, bf16[3,32,2048]{2,1,0:T(8,128)(2,1)S(1)}, u32[]{:S(2)}, u32[]{:S(2)}) collective-permute-start(bf16[3,32,2048]{2,1,0:T(8,128)(2,1)S(1)} %collective-permute-done.rest_1_), channel_id=1, source_target_pairs={{0,1},{1,0},{2,3},{3,2},{4,5},{5,4},{6,7},{7,6},{8,9},{9,8},{10,11... | collective-permute-start | bytes 1179656 | tf_op jit(solution)/shard_map/ppermute | solution.py:318
  56.2 12.4 %copy-start.5 = (bf16[3,32,2048]{2,1,0:T(8,128)(2,1)}, bf16[3,32,2048]{2,1,0:T(8,128)(2,1)S(1)}, u32[]{:S(2)}) copy-start(bf16[3,32,2048]{2,1,0:T(8,128)(2,1)S(1)} %collective-permute-done.1.rest_2_) | copy-start | bytes 1179652
  56.2 10.9 %collective-permute-start.5 = (bf16[3,32,2048]{2,1,0:T(8,128)(2,1)S(1)}, bf16[3,32,2048]{2,1,0:T(8,128)(2,1)S(1)}, u32[]{:S(2)}, u32[]{:S(2)}) collective-permute-start(bf16[3,32,2048]{2,1,0:T(8,128)(2,1)S(1)} %collective-permute-done.1.rest_2_), channel_id=1, source_target_pairs={{0,1},{1,0},{2,3},{3,2},{4,5},{5,4},{6,7},{7,6},{8,9},{9,8},{10,11... | collective-permute-start | bytes 1179656 | tf_op jit(solution)/shard_map/ppermute | solution.py:318
  65.4 3.2 %copy-start.6 = (bf16[3,32,2048]{2,1,0:T(8,128)(2,1)}, bf16[3,32,2048]{2,1,0:T(8,128)(2,1)S(1)}, u32[]{:S(2)}) copy-start(bf16[3,32,2048]{2,1,0:T(8,128)(2,1)S(1)} %collective-permute-done.2.rest_3_) | copy-start | bytes 1179652
  65.4 3.1 %collective-permute-start.6 = (bf16[3,32,2048]{2,1,0:T(8,128)(2,1)S(1)}, bf16[3,32,2048]{2,1,0:T(8,128)(2,1)}, u32[]{:S(2)}, u32[]{:S(2)}) collective-permute-start(bf16[3,32,2048]{2,1,0:T(8,128)(2,1)S(1)} %collective-permute-done.2.rest_3_), channel_id=1, source_target_pairs={{0,1},{1,0},{2,3},{3,2},{4,5},{5,4},{6,7},{7,6},{8,9},{9,8},{10,11... | collective-permute-start | bytes 1179656 | tf_op jit(solution)/shard_map/ppermute | solution.py:318
  67.1 1.5 %copy-start.7 = (bf16[3,32,2048]{2,1,0:T(8,128)(2,1)}, bf16[3,32,2048]{2,1,0:T(8,128)(2,1)S(1)}, u32[]{:S(2)}) copy-start(bf16[3,32,2048]{2,1,0:T(8,128)(2,1)S(1)} %collective-permute-done.3.rest_4_) | copy-start | bytes 1179652
  67.1 1.5 %copy-start.8 = (bf16[3,32,2048]{2,1,0:T(8,128)(2,1)}, bf16[3,32,2048]{2,1,0:T(8,128)(2,1)S(1)}, u32[]{:S(2)}) copy-start(bf16[3,32,2048]{2,1,0:T(8,128)(2,1)S(1)} %collective-permute-done.4.rest_5_) | copy-start | bytes 1179652
  67.1 1.5 %copy-start.9 = (bf16[3,32,2048]{2,1,0:T(8,128)(2,1)}, bf16[3,32,2048]{2,1,0:T(8,128)(2,1)S(1)}, u32[]{:S(2)}) copy-start(bf16[3,32,2048]{2,1,0:T(8,128)(2,1)S(1)} %collective-permute-done.5.rest_6_) | copy-start | bytes 1179652
  68.6 0.8 copy-start.2
  69.4 14.9 %copy-start.15 = (bf16[16,2]{0,1:T(2,128)(2,1)S(1)}, bf16[16,2]{0,1:T(2,128)(2,1)}, u32[]{:S(2)}) copy-start(bf16[16,2]{0,1:T(2,128)(2,1)} %param.28) | copy-start | bytes 196
  76.2 24.6 %all-to-all-start.2 = ((bf16[32,16,512]{2,1,0:T(8,128)(2,1)}), bf16[32,16,512]{2,1,0:T(8,128)(2,1)S(1)}, u32[]{:S(2)}, u32[]{:S(2)}) async-start(bf16[32,16,512]{2,1,0:T(8,128)(2,1)} %bitcast.24), calls=%async_computation.2 | async-start | bytes 1048576 | tf_op jit(solution)/shard_map/all_to_all | solution.py:338
  101.7 10.3 %all-to-all-start.3 = ((bf16[8,16,256]{2,1,0:T(8,128)(2,1)}), bf16[8,16,256]{2,1,0:T(8,128)(2,1)S(1)}, u32[]{:S(2)}, u32[]{:S(2)}) async-start(bf16[8,16,256]{2,1,0:T(8,128)(2,1)} %shard_map.175), calls=%async_computation.3 | async-start | bytes 131072 | tf_op jit(solution)/shard_map/all_to_all | solution.py:350

commit v3 on v2

v3 whole, which is shorter than its diff:
```python
import jax
import jax.numpy as jnp
from jax import lax
from jax.experimental import pallas as pl
from jax.experimental.pallas import tpu as pltpu
from jax.sharding import PartitionSpec as P


HEAD = 64
CACHE = 1024
WIDTH = 2048
ROWS = 16
LANES = 128
HALF = 8
KIB = 1024
MESSAGES = 512
PART = 512
RETURNED = 2048
epsilon = 1e-06
NT = (((1,), (1,)), ((), ()))
VMEM = pl.BlockSpec(memory_space=pltpu.VMEM)
SMEM = pl.BlockSpec(memory_space=pltpu.SMEM)
HBM = pl.BlockSpec(memory_space=pltpu.HBM)


def columns_of(pair):
    r = lax.broadcasted_iota(jnp.int32, (ROWS, ROWS), 0)
    c = lax.broadcasted_iota(jnp.int32, (ROWS, ROWS), 1)
    pair = pair.astype(jnp.float32)
    return [
        jnp.sum(jnp.where(r == c, pair[k : k + 1], 0.0), axis=-1, keepdims=True) for k in range(2)
    ]


def hits_of(routes, expert, slot):
    first, second = [expert == c.astype(jnp.int32) for c in columns_of(routes)]
    hit = (first | second).astype(jnp.float32).astype(jnp.bfloat16)
    r = lax.broadcasted_iota(jnp.int32, (ROWS, ROWS), 0)
    c = lax.broadcasted_iota(jnp.int32, (ROWS, ROWS), 1)
    before = jnp.dot(
        (c < r).astype(jnp.float32).astype(jnp.bfloat16), hit, preferred_element_type=jnp.float32
    )
    right = before == slot.astype(jnp.float32)
    return first & right, second & right


def quarter_of(device, core, slot):
    return 4 * (2 * ((device >> 2) & 1) + (device & 1)) + 2 * core + slot


def picks_of(routes):
    core = lax.axis_index("tp") % 2
    shape = (ROWS, MESSAGES)
    row = lax.broadcasted_iota(jnp.int32, shape, 0)
    col = lax.broadcasted_iota(jnp.int32, shape, 1)
    device, kind, q, slot = 31 - (col >> 4), (col >> 3) & 1, (col >> 1) & 3, col & 1
    first, second = hits_of(routes, device, slot)
    expert = (first | second) & (kind == 0)
    dense = (row == quarter_of(device, core, slot)) & (kind == 1)
    pick = jnp.where(expert | dense, 1.0, 0.0)
    stacked = jnp.concatenate([jnp.where(q == k, pick, 0.0) for k in range(4)], axis=0)
    return stacked.astype(jnp.bfloat16)


def attention_kernel(
    len_ref, bias_ref, tok_ref, gain_ref, hgain_ref, route_ref, wq_hbm, kv_hbm, wo_hbm,
    out_ref, pick_ref,
    wq_v, kv_v, key_v, value_v, wo_v, q_sem, kv_sem, o_sem,
):
    copy_q = pltpu.make_async_copy(wq_hbm, wq_v, q_sem)
    copy_q.start()
    copies = []
    for s in range(ROWS):
        copy = pltpu.make_async_copy(kv_hbm.at[s, 0], kv_v.at[s], kv_sem.at[s])
        copy.start()
        copies.append(copy)
    copy_o = pltpu.make_async_copy(wo_hbm, wo_v, o_sem)
    copy_o.start()
    wide = tok_ref[...].astype(jnp.float32)
    scale = lax.rsqrt(jnp.mean(wide * wide, axis=-1, keepdims=True) + epsilon)
    normed = (wide * scale * gain_ref[...]).astype(jnp.bfloat16)
    normed = jnp.concatenate([normed[:, : WIDTH // 2], normed[:, WIDTH // 2 :]], axis=0)
    pick_ref[...] = picks_of(route_ref[...])

    lane = lax.broadcasted_iota(jnp.int32, (HALF, LANES), 1)
    row = lax.broadcasted_iota(jnp.int32, (HALF, LANES), 0)
    tri_row = lax.broadcasted_iota(jnp.int32, (LANES, 2 * LANES), 0)
    tri_col = lax.broadcasted_iota(jnp.int32, (LANES, 2 * LANES), 1)
    tri = ((tri_row >= tri_col) | (tri_col >= LANES)).astype(jnp.bfloat16)
    position = lax.broadcasted_iota(jnp.int32, (HALF, CACHE), 1)
    bias = jnp.where(row[:, :1] < 4, bias_ref[0], bias_ref[1])
    wide_lane = lax.broadcasted_iota(jnp.int32, (CACHE, LANES), 1)
    chunks = CACHE // LANES

    copy_q.wait()
    folded = jnp.concatenate([wq_v[: WIDTH // 2], wq_v[WIDTH // 2 :]], axis=1)
    query = jnp.dot(normed, folded, preferred_element_type=jnp.float32)
    query = query[:ROWS, :LANES] + query[ROWS:, LANES:]
    query = query.astype(jnp.bfloat16).astype(jnp.float32)

    def scored(group):
        part = query[group // 2 * HALF : group // 2 * HALF + HALF]
        swapped = pltpu.roll(part, 4, 0)
        upper, under = (swapped, part) if group % 2 else (part, swapped)
        part = jnp.where(row < 4, upper, under)
        turned = pltpu.roll(part, HEAD, 1)
        first, second = jnp.where(row < 4, part, turned), jnp.where(row < 4, turned, part)
        blocks = []
        for p in range(2):
            low = (row % 4 == 2 * p) & (lane < HEAD)
            high = (row % 4 == 2 * p + 1) & (lane >= HEAD)
            blocks.append(jnp.where(low, first, jnp.where(high, second, 0.0)))
            j = group * 4 + 2 * p
            copies[j].wait()
            copies[j + 1].wait()
            even = kv_v[j]
            odd = pltpu.roll(kv_v[j + 1].astype(jnp.float32), HEAD, 1).astype(jnp.bfloat16)
            key_v[group, :, p * LANES : (p + 1) * LANES] = jnp.where(wide_lane < HEAD, even, odd)
            value_v[group, :, p * LANES : (p + 1) * LANES] = jnp.where(wide_lane < HEAD, odd, even)
        lhs = jnp.concatenate(blocks, axis=1).astype(jnp.bfloat16)
        scores = lax.dot_general(lhs, key_v[group], NT, preferred_element_type=jnp.float32)
        return scores * 0.125 + bias

    def attended(group, scores):
        length = jnp.full((HALF, 1), len_ref[group * 4], jnp.int32)
        for j in range(1, 4):
            length = jnp.where(row[:, :1] % 4 == j, len_ref[group * 4 + j], length)
        valid = position < length
        soft = jnp.maximum(scores, 0.0) + jnp.log1p(jnp.exp(-jnp.abs(scores)))
        soft = jnp.where(valid, soft, 0.0)
        stacked = jnp.concatenate(
            [soft[:, c * LANES : (c + 1) * LANES] for c in range(chunks)], axis=0
        )
        high = stacked.astype(jnp.bfloat16)
        rest = stacked - high.astype(jnp.float32)
        middle = rest.astype(jnp.bfloat16)
        low = (rest - middle.astype(jnp.float32)).astype(jnp.bfloat16)
        sums = jnp.dot(
            jnp.concatenate([high, middle, low], axis=0), tri, preferred_element_type=jnp.float32
        )
        size = chunks * HALF
        sums = sums[:size] + sums[size : 2 * size] + sums[2 * size :]
        pieces = [None] * chunks
        carry = jnp.zeros((HALF, LANES), jnp.float32)
        for c in reversed(range(chunks)):
            rows = sums[c * HALF : (c + 1) * HALF]
            pieces[c] = rows[:, :LANES] + carry
            carry = carry + rows[:, LANES:]
        later = jnp.concatenate(pieces, axis=1)
        weights = jnp.where(valid, jnp.exp(scores - later), 0.0).astype(jnp.bfloat16)
        mixed = jnp.dot(weights, value_v[group], preferred_element_type=jnp.float32)
        own = jnp.zeros((HALF, LANES), jnp.float32)
        for p in range(2):
            here = (row % 4 == 2 * p) & (lane >= HEAD)
            here = here | ((row % 4 == 2 * p + 1) & (lane < HEAD))
            own = jnp.where(here, mixed[:, p * LANES : (p + 1) * LANES], own)
        mean = jnp.sum(own * own, axis=-1, keepdims=True) * (1.0 / HEAD)
        own = (own + pltpu.roll(own, HEAD, 1)) * lax.rsqrt(mean + epsilon)
        return jnp.where(lane < HEAD, own, pltpu.roll(own, 4, 0)) * hgain_ref[...]

    scores = scored(0)
    heads = []
    for group in range(4):
        later_scores = scored(group + 1) if group < 3 else None
        heads.append(attended(group, scores))
        scores = later_scores
    head_rows = jnp.concatenate(
        [jnp.where(row < 4, heads[2 * k], pltpu.roll(heads[2 * k + 1], 4, 0)) for k in range(2)],
        axis=0,
    ).astype(jnp.bfloat16)
    copy_o.wait()
    share = jnp.dot(head_rows, wo_v[...], preferred_element_type=jnp.float32)
    out_ref[...] = share.astype(jnp.bfloat16)


def in_hbm(*arrays):
    return [pltpu.with_memory_space_constraint(a, pltpu.HBM) for a in arrays]


def attention(
    tokens, attn_gain, w_query, stick_bias, kv_cache, lengths, head_gain, w_attn_out, routes
):
    return pl.pallas_call(
        attention_kernel,
        out_shape=(
            pltpu.VMEM((ROWS, WIDTH), jnp.bfloat16),
            pltpu.VMEM((4 * ROWS, MESSAGES), jnp.bfloat16),
        ),
        in_specs=[SMEM, SMEM, VMEM, VMEM, VMEM, VMEM] + [HBM] * 3,
        out_specs=(VMEM, VMEM),
        scratch_shapes=[
            pltpu.VMEM((WIDTH, LANES), jnp.bfloat16),
            pltpu.VMEM((ROWS, CACHE, LANES), jnp.bfloat16),
            pltpu.VMEM((4, CACHE, 2 * LANES), jnp.bfloat16),
            pltpu.VMEM((4, CACHE, 2 * LANES), jnp.bfloat16),
            pltpu.VMEM((LANES, WIDTH), jnp.bfloat16),
            pltpu.SemaphoreType.DMA,
            pltpu.SemaphoreType.DMA((ROWS,)),
            pltpu.SemaphoreType.DMA,
        ],
        cost_estimate=pl.CostEstimate(
            flops=400_000_000, bytes_accessed=6_000_000, transcendentals=200_000
        ),
    )(
        lengths, stick_bias, tokens, attn_gain.reshape(1, -1), head_gain.reshape(1, -1), routes.T,
        *in_hbm(w_query, kv_cache, w_attn_out),
    )


def mix_kernel(route_ref, weight_ref, branch_ref, mix_ref):
    shape = (ROWS, RETURNED)
    row = lax.broadcasted_iota(jnp.int32, shape, 0)
    col = lax.broadcasted_iota(jnp.int32, shape, 1)
    device, t = 31 - (col >> 6), 7 - ((col >> 3) & 7)
    kind, slot, side = (col >> 2) & 1, (col >> 1) & 1, col & 1
    first, second = hits_of(route_ref[...], device, slot)
    one, two = columns_of(weight_ref[...])
    expert = jnp.where(first, one, jnp.where(second, two, 0.0))
    dense = jnp.where(row == quarter_of(device, t & 1, slot), branch_ref[:, 0:1], 0.0)
    value = jnp.where(kind == 0, expert, dense)
    both = jnp.concatenate([jnp.where(side == h, value, 0.0) for h in range(2)], axis=0)
    mix_ref[...] = both.astype(jnp.bfloat16)


def mix_table(routes, weights, branch):
    return pl.pallas_call(
        mix_kernel,
        out_shape=jax.ShapeDtypeStruct((2 * ROWS, RETURNED), jnp.bfloat16),
        in_specs=[VMEM, VMEM, VMEM],
        out_specs=VMEM,
        compiler_params=pltpu.CompilerParams(vmem_limit_bytes=8192 * KIB),
        cost_estimate=pl.CostEstimate(
            flops=1_000_000, bytes_accessed=100_000, transcendentals=0
        ),
    )(routes.T, weights.T, branch)


def dispatch_kernel(
    a_ref, b_ref, c_ref, d_ref, tok_ref, gain_ref, gate_ref, pick_ref,
    send_ref, res_ref, branch_ref,
):
    total = a_ref[...].astype(jnp.float32) + b_ref[...].astype(jnp.float32)
    total = total + (c_ref[...].astype(jnp.float32) + d_ref[...].astype(jnp.float32))
    total = total + tok_ref[...].astype(jnp.float32)
    res_ref[...] = total
    scale = lax.rsqrt(jnp.mean(total * total, axis=-1, keepdims=True) + epsilon)
    normed = (total * scale * gain_ref[...]).astype(jnp.bfloat16)
    logit = jnp.sum(
        normed.astype(jnp.float32) * gate_ref[...].astype(jnp.float32), axis=-1, keepdims=True
    )
    branch_ref[...] = jnp.broadcast_to(1.0 / (1.0 + jnp.exp(-logit)), branch_ref.shape)
    stacked = jnp.concatenate([normed[:, q * PART : (q + 1) * PART] for q in range(4)], axis=0)
    send_ref[...] = lax.dot_general(
        pick_ref[...], stacked, (((0,), (0,)), ((), ())), preferred_element_type=jnp.float32
    ).astype(jnp.bfloat16)


def dispatch(shares, tokens, ffn_gain, branch_gate, picks):
    return pl.pallas_call(
        dispatch_kernel,
        out_shape=(
            jax.ShapeDtypeStruct((MESSAGES, PART), jnp.bfloat16),
            jax.ShapeDtypeStruct((ROWS, WIDTH), jnp.float32),
            jax.ShapeDtypeStruct((ROWS, LANES), jnp.float32),
        ),
        in_specs=[VMEM] * 8,
        out_specs=(VMEM, VMEM, VMEM),
        compiler_params=pltpu.CompilerParams(vmem_limit_bytes=8192 * KIB),
        cost_estimate=pl.CostEstimate(
            flops=40_000_000, bytes_accessed=1_500_000, transcendentals=100
        ),
    )(*shares, tokens, ffn_gain.reshape(1, -1), branch_gate.reshape(1, -1), picks)


def feed_kernel(got_ref, eg_hbm, eu_hbm, ed_hbm, *rest):
    packs = rest[:8]
    out_ref, wide_v, back_v, eg_v, eu_v, ed_v, dg_v, du_v, dd_v, e_sem, d_sem = rest[8:]
    expert_copies = [
        pltpu.make_async_copy(src, dst, e_sem.at[k])
        for k, (src, dst) in enumerate(((eg_hbm, eg_v), (eu_hbm, eu_v), (ed_hbm, ed_v)))
    ]
    dense_copies = [
        pltpu.make_async_copy(pack.at[k], dst.at[pl.ds(32 * i, 32), :], d_sem.at[8 * k + i])
        for k, dst in enumerate((dg_v, du_v, dd_v))
        for i, pack in enumerate(packs)
    ]
    for copy in expert_copies + dense_copies:
        copy.start()
    for l in range(4):
        wide_v[l] = got_ref[:, l * LANES : (l + 1) * LANES].astype(jnp.float32)

    def unpacked(kind):
        parts = [
            jnp.concatenate(
                [wide_v[l, pl.ds(kind * 8 + q * 2 + slot, 32, stride=16), :] for slot in range(2)],
                axis=0,
            )
            for q in range(4)
            for l in range(4)
        ]
        return jnp.concatenate(parts, axis=1).astype(jnp.bfloat16)

    def packed(kind, value):
        for t in range(8):
            for slot in range(2):
                for h in range(2):
                    at = t * 256 + h * LANES
                    first = (7 - t) * 8 + kind * 4 + slot * 2 + h
                    back_v[pl.ds(first, 32, stride=64), :] = value[
                        slot * 32 : slot * 32 + 32, at : at + LANES
                    ]

    rows = unpacked(0)
    dense_rows = unpacked(1)
    expert_copies[0].wait()
    a = jnp.dot(rows, eg_v[...], preferred_element_type=jnp.float32)
    expert_copies[1].wait()
    b = jnp.dot(rows, eu_v[...], preferred_element_type=jnp.float32)
    hidden = (a / (1.0 + jnp.exp(-a)) * b).astype(jnp.bfloat16)
    expert_copies[2].wait()
    packed(0, jnp.dot(hidden, ed_v[...], preferred_element_type=jnp.float32))
    for copy in dense_copies[:8]:
        copy.wait()
    a = lax.dot_general(dense_rows, dg_v[...], NT, preferred_element_type=jnp.float32)
    for copy in dense_copies[8:16]:
        copy.wait()
    b = lax.dot_general(dense_rows, du_v[...], NT, preferred_element_type=jnp.float32)
    hidden = (a / (1.0 + jnp.exp(-a)) * b).astype(jnp.bfloat16)
    for copy in dense_copies[16:]:
        copy.wait()
    packed(1, jnp.dot(hidden, dd_v[...], preferred_element_type=jnp.float32))
    out_ref[...] = back_v[...].astype(jnp.bfloat16)


def feed(got, gate, up, down, packs):
    return pl.pallas_call(
        feed_kernel,
        out_shape=jax.ShapeDtypeStruct((RETURNED, LANES), jnp.bfloat16),
        in_specs=[VMEM] + [HBM] * 11,
        out_specs=VMEM,
        scratch_shapes=[
            pltpu.VMEM((4, MESSAGES, LANES), jnp.float32),
            pltpu.VMEM((RETURNED, LANES), jnp.float32),
            pltpu.VMEM((WIDTH, 256), jnp.bfloat16),
            pltpu.VMEM((WIDTH, 256), jnp.bfloat16),
            pltpu.VMEM((256, WIDTH), jnp.bfloat16),
            pltpu.VMEM((256, WIDTH), jnp.bfloat16),
            pltpu.VMEM((256, WIDTH), jnp.bfloat16),
            pltpu.VMEM((256, WIDTH), jnp.bfloat16),
            pltpu.SemaphoreType.DMA((3,)),
            pltpu.SemaphoreType.DMA((24,)),
        ],
        compiler_params=pltpu.CompilerParams(vmem_limit_bytes=24576 * KIB),
        cost_estimate=pl.CostEstimate(
            flops=1_000_000_000, bytes_accessed=7_000_000, transcendentals=40_000
        ),
    )(got, *in_hbm(gate, up, down, *packs))


def finish_kernel(mix_ref, got_ref, res_ref, out_ref):
    total = jnp.dot(mix_ref[...], got_ref[...], preferred_element_type=jnp.float32)
    total = jnp.concatenate([total[:ROWS], total[ROWS:]], axis=1)
    out_ref[...] = (res_ref[...] + total).astype(jnp.bfloat16)


def finish(mix, returned, residual):
    return pl.pallas_call(
        finish_kernel,
        out_shape=jax.ShapeDtypeStruct((ROWS, 256), jnp.bfloat16),
        in_specs=[VMEM] * 3,
        out_specs=VMEM,
        compiler_params=pltpu.CompilerParams(vmem_limit_bytes=8192 * KIB),
        cost_estimate=pl.CostEstimate(
            flops=40_000_000, bytes_accessed=600_000, transcendentals=0
        ),
    )(mix, returned, residual)


def along_y(x, step):
    return lax.ppermute(x, "tp", [(i, (i + 2 * step) % 8) for i in range(8)])


def layer(
    tokens, attn_gain, w_query, stick_bias, kv_cache, lengths, head_gain, w_attn_out, ffn_gain,
    route_expert, route_weight, w_exp_gate, w_exp_up, w_exp_down, branch_gate,
    w_dense_gate, w_dense_up, w_dense_down,
):
    single, half = jnp.float32, jnp.bfloat16
    t = lax.axis_index("tp")
    swap = [(i, i ^ 1) for i in range(8)]

    square = [(i, i ^ 1) for i in range(32)]
    own = lax.optimization_barrier(jnp.stack([w_dense_gate, w_dense_up, w_dense_down]))
    packs = [own, lax.ppermute(own, "ep", [(i, i ^ 4) for i in range(32)])]
    packs.append(lax.ppermute(own, "ep", square))
    share, picks = attention(
        tokens, attn_gain, w_query, stick_bias, kv_cache, lengths, head_gain, w_attn_out,
        route_expert,
    )
    other = lax.ppermute(share, "tp", swap)
    share = (share.astype(single) + other.astype(single)).astype(half)
    shares = [share]
    for step in (1, 3, 2):
        shares.append(along_y(share, step))
    packs.append(lax.ppermute(packs[1], "ep", square))
    send, residual, branch = dispatch(shares, tokens, ffn_gain, branch_gate, picks)
    got = lax.all_to_all(
        send.reshape(32, 16, PART), "ep", 0, 0, tiled=True,
        axis_index_groups=[list(range(31, -1, -1))],
    )

    for k in range(4):
        packs.append(lax.ppermute(packs[k], "tp", swap))
    back = feed(
        got.reshape(MESSAGES, PART), w_exp_gate[0], w_exp_up[0], w_exp_down[0], packs
    )
    returned = lax.all_to_all(
        back.reshape(256, 8, LANES), ("ep", "tp"), 0, 0, tiled=True,
        axis_index_groups=[list(range(255, -1, -1))],
    )
    mix = mix_table(route_expert, route_weight, branch)
    residual_cols = lax.dynamic_slice_in_dim(residual, t * 256, 256, 1)
    return finish(mix, returned.reshape(RETURNED, LANES), residual_cols)


def solution(mesh):
    return jax.shard_map(
        layer,
        mesh=mesh,
        in_specs=(
            P("ep", None), P(), P(None, "tp"), P("tp"), P("ep", "tp", None, None), P("ep"),
            P("tp"), P("tp", None), P(), P("ep", None), P("ep", None), P("ep", None, "tp"),
            P("ep", None, "tp"), P("ep", "tp", None), P(), P(("ep", "tp"), None),
            P(("ep", "tp"), None), P(("ep", "tp"), None),
        ),
        out_specs=P("ep", "tp"),
        check_vma=False,
    )
```

time: 113 us -> 91.6 us (0.81)
  waiting for transfers between devices: 50.1 us -> 40.3 us
  starting transfers between devices: 41.8 us -> 34.6 us
  other arithmetic: 2.07 us -> 0.06 us
  local copies, waits for them, and re-layouts: 1.91 us -> 0.08 us
    all_to_all x4 -> x2, starting transfers between devices: 30.4 us -> 17.7 us  [the longest x1 10.2 us: layer(): lax.all_to_all(send.reshape(32, 16, PART), 'ep', 0, 0, tiled=True, axis_i...]
    all_to_all x4 -> x2, waiting for transfers between devices: 28.2 us -> 19.2 us  [the longest x1 19.2 us: layer(): lax.all_to_all(back.reshape(256, 8, LANES), ('ep', 'tp'), 0, 0, tiled=Tru...]
    ppermute x7 -> x11, starting transfers between devices: 11.4 us -> 17 us  [the longest x4 8.4 us: layer(): packs.append(lax.ppermute(packs[k], 'tp', swap))]
    ppermute x7 -> x11, waiting for transfers between devices: 21.9 us -> 21 us  [the longest x1 10.2 us: layer(): packs.append(lax.ppermute(own, 'ep', square))]
    pallas_call x3 -> x4, Pallas kernels: 15.1 us -> 14.9 us  [the longest x1 7.23 us: attention(): pl.pallas_call(attention_kernel, out_shape=(pltpu.VMEM((ROWS, WIDTH), jnp...]
  transfers between devices with their start and end apart: 11 -> 13, of which waited for: 7 -> 7; matrix products, arithmetic and copies ran while one was open for 2% -> 0% of each run, Pallas kernels for 0% -> 2%
where the time goes in v3:
time: 91.6 us; the launch traced here: 91.4 us
  waiting for transfers between devices  40.3 us (44%)
  starting transfers between devices  34.6 us (38%)
  Pallas kernels  16.1 us (18%)
    all_to_all x1, waiting for transfers between devices, layer(): lax.all_to_all(back.reshape(256, 8, LANES), ('ep', 'tp'), 0, 0, tiled=Tru...  19.2 us
    all_to_all x1, starting transfers between devices, layer(): lax.all_to_all(send.reshape(32, 16, PART), 'ep', 0, 0, tiled=True, axis_i...  10.2 us
    ppermute x1, waiting for transfers between devices, layer(): packs.append(lax.ppermute(own, 'ep', square))  10.2 us
    ppermute x4, starting transfers between devices, layer(): packs.append(lax.ppermute(packs[k], 'tp', swap))  8.4 us
    all_to_all x1, starting transfers between devices, layer(): lax.all_to_all(back.reshape(256, 8, LANES), ('ep', 'tp'), 0, 0, tiled=Tru...  7.43 us
    pallas_call x1, Pallas kernels, attention(): pl.pallas_call(attention_kernel, out_shape=(pltpu.VMEM((ROWS, WIDTH), jnp...  7.23 us
    pallas_call x1, Pallas kernels, feed(): pl.pallas_call(feed_kernel, out_shape=jax.ShapeDtypeStruct((RETURNED, LAN...  6.54 us
    ppermute x1, waiting for transfers between devices, layer(): packs.append(lax.ppermute(packs[1], 'ep', square))  4.98 us
  transfers between devices with their start and end apart: 13, of which 7 were waited for; matrix products, arithmetic and copies ran while one was open for 0% of the time, Pallas kernels for 2%

profile of v3, /device:TPU:1, one launch (start us, length us, event | category | flops | bytes accessed | tf_op | source)
XLA Modules:
  0.0 91.4 jit_solution(12099136833868460647)
XLA Ops:
  0.0 7.2 %shard_map.172 = (bf16[16,2048]{1,0:T(8,128)(2,1)S(1)}, bf16[64,512]{1,0:T(8,128)(2,1)S(1)}) custom-call(s32[16]{0:T(128)} %len_ref.1, f32[2]{0:T(128)} %bias_ref.1, bf16[16,2048]{1,0:T(8,128)(2,1)} %tok_ref.3, f32[1,2048]{1,0:T(1,128)} %bitcast.27, f32[1,128]{1,0:T(1,128)} %bitcast.28, s32[2,16]{1,0:T(2,128)} %bitcast.18, bf16[2048,128]{1,0:T(8,128)(2,1)} %wq_hbm.1, ...), custom_call_target="tpu_custom_call" | custom-call | flops 400000000 | bytes 6000000 | tf_op jit(solution)/shard_map/pallas_call | solution.py:183
  7.3 3.3 %collective-permute-start = (bf16[16,2048]{1,0:T(8,128)(2,1)S(1)}, bf16[16,2048]{1,0:T(8,128)(2,1)S(1)}, u32[]{:S(2)}, u32[]{:S(2)}) collective-permute-start(bf16[16,2048]{1,0:T(8,128)(2,1)S(1)} %get-tuple-element.10), channel_id=1, source_target_pairs={{0,1},{1,0},{2,3},{3,2},{4,5},{5,4},{6,7},{7,6},{8,9},{9,8},{10,11... | collective-permute-start | bytes 196616 | tf_op jit(solution)/shard_map/ppermute | solution.py:400
  10.6 0.1 collective-permute-start.4
  10.7 0.7 collective-permute-done
  11.5 0.6 collective-permute-start.1
  12.1 2.2 %collective-permute-start.2 = (bf16[16,2048]{1,0:T(8,128)(2,1)S(1)}, bf16[16,2048]{1,0:T(8,128)(2,1)S(1)}, u32[]{:S(2)}, u32[]{:S(2)}) collective-permute-start(bf16[16,2048]{1,0:T(8,128)(2,1)S(1)} %add_convert_fusion.a_ref), channel_id=1, source_target_pairs={{0,6},{1,7},{2,0},{3,1},{4,2},{5,3},{6,4},{7,5},{8,14},{9,15},{10,... | collective-permute-start | bytes 196616 | tf_op jit(solution)/shard_map/ppermute | solution.py:380
  14.2 0.9 %collective-permute-start.3 = (bf16[16,2048]{1,0:T(8,128)(2,1)S(1)}, bf16[16,2048]{1,0:T(8,128)(2,1)S(1)}, u32[]{:S(2)}, u32[]{:S(2)}) collective-permute-start(bf16[16,2048]{1,0:T(8,128)(2,1)S(1)} %add_convert_fusion.a_ref), channel_id=1, source_target_pairs={{0,4},{1,5},{2,6},{3,7},{4,0},{5,1},{6,2},{7,3},{8,12},{9,13},{10,... | collective-permute-start | bytes 196616 | tf_op jit(solution)/shard_map/ppermute | solution.py:380
  15.2 0.7 collective-permute-done.1.b_ref
  15.9 0.0 collective-permute-done.2.c_ref
  15.9 3.0 %collective-permute-done.3.d_ref = bf16[16,2048]{1,0:T(8,128)(2,1)S(1)} collective-permute-done((bf16[16,2048]{1,0:T(8,128)(2,1)S(1)}, bf16[16,2048]{1,0:T(8,128)(2,1)S(1)}, u32[]{:S(2)}, u32[]{:S(2)}) %collective-permute-start.3) | collective-permute-done | bytes 65568 | tf_op jit(solution)/shard_map/ppermute | solution.py:380
  18.8 1.2 %shard_map.173 = (bf16[512,512]{1,0:T(8,128)(2,1)}, f32[16,2048]{1,0:T(8,128)S(1)}, f32[16,128]{1,0:T(8,128)S(1)}) custom-call(bf16[16,2048]{1,0:T(8,128)(2,1)S(1)} %add_convert_fusion.a_ref, bf16[16,2048]{1,0:T(8,128)(2,1)S(1)} %collective-permute-done.1.b_ref, bf16[16,2048]{1,0:T(8,128)(2,1)S(1)} %collective-permute-done.2.c_ref, ...), custom_call_target="tpu_custom_call" | custom-call | flops 40000000 | bytes 1500000 | tf_op jit(solution)/shard_map/pallas_call | solution.py:259
  20.1 10.2 %all-to-all-start = ((bf16[32,16,512]{2,1,0:T(8,128)(2,1)}), bf16[32,16,512]{2,1,0:T(8,128)(2,1)S(1)}, u32[]{:S(2)}, u32[]{:S(2)}) async-start(bf16[32,16,512]{2,1,0:T(8,128)(2,1)} %bitcast.5), calls=%async_computation | async-start | bytes 1048576 | tf_op jit(solution)/shard_map/all_to_all | solution.py:407
  30.3 0.7 collective-permute-start.5
  31.0 0.0 collective-permute-done.4.rest_1_
  31.0 0.9 collective-permute-start.6
  31.9 3.0 %collective-permute-start.7 = (bf16[3,32,2048]{2,1,0:T(8,128)(2,1)S(1)}, bf16[3,32,2048]{2,1,0:T(8,128)(2,1)S(1)}, u32[]{:S(2)}, u32[]{:S(2)}) collective-permute-start(bf16[3,32,2048]{2,1,0:T(8,128)(2,1)S(1)} %pad_maximum_fusion.rest_0_), channel_id=1, source_target_pairs={{0,1},{1,0},{2,3},{3,2},{4,5},{5,4},{6,7},{7,6},{8,9},{9,8},{10,11... | collective-permute-start | bytes 1179656 | tf_op jit(solution)/shard_map/ppermute | solution.py:413
  34.9 0.0 collective-permute-start.8
  34.9 10.2 %collective-permute-done.5.rest_2_ = bf16[3,32,2048]{2,1,0:T(8,128)(2,1)S(1)} collective-permute-done((bf16[3,32,2048]{2,1,0:T(8,128)(2,1)S(1)}, bf16[3,32,2048]{2,1,0:T(8,128)(2,1)S(1)}, u32[]{:S(2)}, u32[]{:S(2)}) %collective-permute-start.5) | collective-permute-done | bytes 393248 | tf_op jit(solution)/shard_map/ppermute | solution.py:395
  45.1 3.4 %collective-permute-start.9 = (bf16[3,32,2048]{2,1,0:T(8,128)(2,1)S(1)}, bf16[3,32,2048]{2,1,0:T(8,128)(2,1)S(1)}, u32[]{:S(2)}, u32[]{:S(2)}) collective-permute-start(bf16[3,32,2048]{2,1,0:T(8,128)(2,1)S(1)} %collective-permute-done.5.rest_2_), channel_id=1, source_target_pairs={{0,1},{1,0},{2,3},{3,2},{4,5},{5,4},{6,7},{7,6},{8,9},{9,8},{10,11... | collective-permute-start | bytes 1179656 | tf_op jit(solution)/shard_map/ppermute | solution.py:413
  48.6 5.0 %collective-permute-done.6.rest_3_ = bf16[3,32,2048]{2,1,0:T(8,128)(2,1)S(1)} collective-permute-done((bf16[3,32,2048]{2,1,0:T(8,128)(2,1)S(1)}, bf16[3,32,2048]{2,1,0:T(8,128)(2,1)S(1)}, u32[]{:S(2)}, u32[]{:S(2)}) %collective-permute-start.6) | collective-permute-done | bytes 393248 | tf_op jit(solution)/shard_map/ppermute | solution.py:405
  53.5 1.9 %collective-permute-start.10 = (bf16[3,32,2048]{2,1,0:T(8,128)(2,1)S(1)}, bf16[3,32,2048]{2,1,0:T(8,128)(2,1)}, u32[]{:S(2)}, u32[]{:S(2)}) collective-permute-start(bf16[3,32,2048]{2,1,0:T(8,128)(2,1)S(1)} %collective-permute-done.6.rest_3_), channel_id=1, source_target_pairs={{0,1},{1,0},{2,3},{3,2},{4,5},{5,4},{6,7},{7,6},{8,9},{9,8},{10,11... | collective-permute-start | bytes 1179656 | tf_op jit(solution)/shard_map/ppermute | solution.py:413
  55.5 0.0 collective-permute-done.7.rest_4_
  55.5 0.0 collective-permute-done.8.rest_5_
  55.5 0.0 all-to-all-done
  55.5 1.4 %collective-permute-done.10.rest_7_ = bf16[3,32,2048]{2,1,0:T(8,128)(2,1)} collective-permute-done((bf16[3,32,2048]{2,1,0:T(8,128)(2,1)S(1)}, bf16[3,32,2048]{2,1,0:T(8,128)(2,1)}, u32[]{:S(2)}, u32[]{:S(2)}) %collective-permute-start.10) | collective-permute-done | bytes 393248 | tf_op jit(solution)/shard_map/ppermute | solution.py:413
  57.0 0.0 copy-start.2
  57.0 0.0 copy-start.3
  57.0 6.5 %shard_map.175 = bf16[2048,128]{1,0:T(8,128)(2,1)} custom-call(bf16[512,512]{1,0:T(8,128)(2,1)S(1)} %bitcast.15, bf16[2048,256]{1,0:T(8,128)(2,1)} %bitcast.21, bf16[2048,256]{1,0:T(8,128)(2,1)} %bitcast.22, bf16[256,2048]{1,0:T(8,128)(2,1)} %bitcast.23, bf16[3,32,2048]{2,1,0:T(8,128)(2,1)} %copy-done.4, bf16[3,32,2048]{2,1,0:T(8,128)(2,1)} %copy-done.5, ...), custom_call_target="tpu_custom_call" | custom-call | flops 1000000000 | bytes 7000000 | tf_op jit(solution)/shard_map/pallas_call | solution.py:336
  63.6 7.4 %all-to-all-start.1 = ((bf16[256,8,128]{2,1,0:T(8,128)(2,1)}), bf16[256,8,128]{2,1,0:T(8,128)(2,1)S(1)}, u32[]{:S(2)}, u32[]{:S(2)}) async-start(bf16[256,8,128]{2,1,0:T(8,128)(2,1)} %bitcast.13), calls=%async_computation.1 | async-start | bytes 1048576 | tf_op jit(solution)/shard_map/all_to_all | solution.py:417
  71.0 0.3 shard_map.174.mix_ref
  71.3 19.2 %all-to-all-done.1 = bf16[256,8,128]{2,1,0:T(8,128)(2,1)S(1)} async-done(((bf16[256,8,128]{2,1,0:T(8,128)(2,1)}), bf16[256,8,128]{2,1,0:T(8,128)(2,1)S(1)}, u32[]{:S(2)}, u32[]{:S(2)}) %all-to-all-start.1) | async-done | bytes 524320 | tf_op jit(solution)/shard_map/all_to_all | solution.py:417
  90.6 0.8 shard_map.176
  (33 shorter events, 0.1 us)
Async XLA Ops:
  0.0 18.8 %copy-start = (bf16[16,2048]{1,0:T(8,128)(2,1)S(1)}, bf16[16,2048]{1,0:T(8,128)(2,1)}, u32[]{:S(2)}) copy-start(bf16[16,2048]{1,0:T(8,128)(2,1)} %tok_ref.3) | copy-start | bytes 196612
  0.0 10.5 %copy-start.13 = (bf16[32,2048]{1,0:T(8,128)(2,1)S(1)}, bf16[32,2048]{1,0:T(8,128)(2,1)}, u32[]{:S(2)}) copy-start(bf16[32,2048]{1,0:T(8,128)(2,1)} %param.33) | copy-start | bytes 393220
  0.0 10.5 %copy-start.12 = (bf16[32,2048]{1,0:T(8,128)(2,1)S(1)}, bf16[32,2048]{1,0:T(8,128)(2,1)}, u32[]{:S(2)}) copy-start(bf16[32,2048]{1,0:T(8,128)(2,1)} %param.34) | copy-start | bytes 393220
  0.0 10.5 %copy-start.11 = (bf16[32,2048]{1,0:T(8,128)(2,1)S(1)}, bf16[32,2048]{1,0:T(8,128)(2,1)}, u32[]{:S(2)}) copy-start(bf16[32,2048]{1,0:T(8,128)(2,1)} %param.35) | copy-start | bytes 393220
  0.0 15.1 %copy-start.14 = (bf16[2048]{0:T(1024)(128)(2,1)S(1)}, bf16[2048]{0:T(1024)(128)(2,1)}, u32[]{:S(2)}) copy-start(bf16[2048]{0:T(1024)(128)(2,1)} %param.32) | copy-start | bytes 12292
  0.0 18.8 %copy-start.1 = (f32[2048]{0:T(1024)S(1)}, f32[2048]{0:T(1024)}, u32[]{:S(2)}) copy-start(f32[2048]{0:T(1024)} %param.26) | copy-start | bytes 24580
  7.3 4.2 %collective-permute-start = (bf16[16,2048]{1,0:T(8,128)(2,1)S(1)}, bf16[16,2048]{1,0:T(8,128)(2,1)S(1)}, u32[]{:S(2)}, u32[]{:S(2)}) collective-permute-start(bf16[16,2048]{1,0:T(8,128)(2,1)S(1)} %get-tuple-element.10), channel_id=1, source_target_pairs={{0,1},{1,0},{2,3},{3,2},{4,5},{5,4},{6,7},{7,6},{8,9},{9,8},{10,11... | collective-permute-start | bytes 196616 | tf_op jit(solution)/shard_map/ppermute | solution.py:400
  10.6 46.3 %copy-start.4 = (bf16[3,32,2048]{2,1,0:T(8,128)(2,1)}, bf16[3,32,2048]{2,1,0:T(8,128)(2,1)S(1)}, u32[]{:S(2)}) copy-start(bf16[3,32,2048]{2,1,0:T(8,128)(2,1)S(1)} %pad_maximum_fusion.rest_0_) | copy-start | bytes 1179652
  10.6 20.4 %collective-permute-start.4 = (bf16[3,32,2048]{2,1,0:T(8,128)(2,1)S(1)}, bf16[3,32,2048]{2,1,0:T(8,128)(2,1)S(1)}, u32[]{:S(2)}, u32[]{:S(2)}) collective-permute-start(bf16[3,32,2048]{2,1,0:T(8,128)(2,1)S(1)} %pad_maximum_fusion.rest_0_), channel_id=1, source_target_pairs={{0,32},{8,40},{16,48},{24,56},{32,0},{40,8},{48,16},{56,24},{64,96... | collective-permute-start | bytes 1179656 | tf_op jit(solution)/shard_map/ppermute | solution.py:394
  11.5 4.4 %collective-permute-start.1 = (bf16[16,2048]{1,0:T(8,128)(2,1)S(1)}, bf16[16,2048]{1,0:T(8,128)(2,1)S(1)}, u32[]{:S(2)}, u32[]{:S(2)}) collective-permute-start(bf16[16,2048]{1,0:T(8,128)(2,1)S(1)} %add_convert_fusion.a_ref), channel_id=1, source_target_pairs={{0,2},{1,3},{2,4},{3,5},{4,6},{5,7},{6,0},{7,1},{8,10},{9,11},{10,... | collective-permute-start | bytes 196616 | tf_op jit(solution)/shard_map/ppermute | solution.py:380
  12.1 3.8 %collective-permute-start.2 = (bf16[16,2048]{1,0:T(8,128)(2,1)S(1)}, bf16[16,2048]{1,0:T(8,128)(2,1)S(1)}, u32[]{:S(2)}, u32[]{:S(2)}) collective-permute-start(bf16[16,2048]{1,0:T(8,128)(2,1)S(1)} %add_convert_fusion.a_ref), channel_id=1, source_target_pairs={{0,6},{1,7},{2,0},{3,1},{4,2},{5,3},{6,4},{7,5},{8,14},{9,15},{10,... | collective-permute-start | bytes 196616 | tf_op jit(solution)/shard_map/ppermute | solution.py:380
  14.2 4.6 %collective-permute-start.3 = (bf16[16,2048]{1,0:T(8,128)(2,1)S(1)}, bf16[16,2048]{1,0:T(8,128)(2,1)S(1)}, u32[]{:S(2)}, u32[]{:S(2)}) collective-permute-start(bf16[16,2048]{1,0:T(8,128)(2,1)S(1)} %add_convert_fusion.a_ref), channel_id=1, source_target_pairs={{0,4},{1,5},{2,6},{3,7},{4,0},{5,1},{6,2},{7,3},{8,12},{9,13},{10,... | collective-permute-start | bytes 196616 | tf_op jit(solution)/shard_map/ppermute | solution.py:380
  20.1 35.4 %all-to-all-start = ((bf16[32,16,512]{2,1,0:T(8,128)(2,1)}), bf16[32,16,512]{2,1,0:T(8,128)(2,1)S(1)}, u32[]{:S(2)}, u32[]{:S(2)}) async-start(bf16[32,16,512]{2,1,0:T(8,128)(2,1)} %bitcast.5), calls=%async_computation | async-start | bytes 1048576 | tf_op jit(solution)/shard_map/all_to_all | solution.py:407
  30.3 14.8 %collective-permute-start.5 = (bf16[3,32,2048]{2,1,0:T(8,128)(2,1)S(1)}, bf16[3,32,2048]{2,1,0:T(8,128)(2,1)S(1)}, u32[]{:S(2)}, u32[]{:S(2)}) collective-permute-start(bf16[3,32,2048]{2,1,0:T(8,128)(2,1)S(1)} %pad_maximum_fusion.rest_0_), channel_id=1, source_target_pairs={{0,8},{8,0},{16,24},{24,16},{32,40},{40,32},{48,56},{56,48},{64,72... | collective-permute-start | bytes 1179656 | tf_op jit(solution)/shard_map/ppermute | solution.py:395
  31.0 26.0 %copy-start.5 = (bf16[3,32,2048]{2,1,0:T(8,128)(2,1)}, bf16[3,32,2048]{2,1,0:T(8,128)(2,1)S(1)}, u32[]{:S(2)}) copy-start(bf16[3,32,2048]{2,1,0:T(8,128)(2,1)S(1)} %collective-permute-done.4.rest_1_) | copy-start | bytes 1179652
  31.0 22.6 %collective-permute-start.6 = (bf16[3,32,2048]{2,1,0:T(8,128)(2,1)S(1)}, bf16[3,32,2048]{2,1,0:T(8,128)(2,1)S(1)}, u32[]{:S(2)}, u32[]{:S(2)}) collective-permute-start(bf16[3,32,2048]{2,1,0:T(8,128)(2,1)S(1)} %collective-permute-done.4.rest_1_), channel_id=1, source_target_pairs={{0,8},{8,0},{16,24},{24,16},{32,40},{40,32},{48,56},{56,48},{64,72... | collective-permute-start | bytes 1179656 | tf_op jit(solution)/shard_map/ppermute | solution.py:405
  31.9 23.6 %collective-permute-start.7 = (bf16[3,32,2048]{2,1,0:T(8,128)(2,1)S(1)}, bf16[3,32,2048]{2,1,0:T(8,128)(2,1)S(1)}, u32[]{:S(2)}, u32[]{:S(2)}) collective-permute-start(bf16[3,32,2048]{2,1,0:T(8,128)(2,1)S(1)} %pad_maximum_fusion.rest_0_), channel_id=1, source_target_pairs={{0,1},{1,0},{2,3},{3,2},{4,5},{5,4},{6,7},{7,6},{8,9},{9,8},{10,11... | collective-permute-start | bytes 1179656 | tf_op jit(solution)/shard_map/ppermute | solution.py:413
  34.9 20.6 %collective-permute-start.8 = (bf16[3,32,2048]{2,1,0:T(8,128)(2,1)S(1)}, bf16[3,32,2048]{2,1,0:T(8,128)(2,1)S(1)}, u32[]{:S(2)}, u32[]{:S(2)}) collective-permute-start(bf16[3,32,2048]{2,1,0:T(8,128)(2,1)S(1)} %collective-permute-done.4.rest_1_), channel_id=1, source_target_pairs={{0,1},{1,0},{2,3},{3,2},{4,5},{5,4},{6,7},{7,6},{8,9},{9,8},{10,11... | collective-permute-start | bytes 1179656 | tf_op jit(solution)/shard_map/ppermute | solution.py:413
  45.1 11.8 %copy-start.6 = (bf16[3,32,2048]{2,1,0:T(8,128)(2,1)}, bf16[3,32,2048]{2,1,0:T(8,128)(2,1)S(1)}, u32[]{:S(2)}) copy-start(bf16[3,32,2048]{2,1,0:T(8,128)(2,1)S(1)} %collective-permute-done.5.rest_2_) | copy-start | bytes 1179652
  45.1 10.4 %collective-permute-start.9 = (bf16[3,32,2048]{2,1,0:T(8,128)(2,1)S(1)}, bf16[3,32,2048]{2,1,0:T(8,128)(2,1)S(1)}, u32[]{:S(2)}, u32[]{:S(2)}) collective-permute-start(bf16[3,32,2048]{2,1,0:T(8,128)(2,1)S(1)} %collective-permute-done.5.rest_2_), channel_id=1, source_target_pairs={{0,1},{1,0},{2,3},{3,2},{4,5},{5,4},{6,7},{7,6},{8,9},{9,8},{10,11... | collective-permute-start | bytes 1179656 | tf_op jit(solution)/shard_map/ppermute | solution.py:413
  53.5 3.4 %copy-start.7 = (bf16[3,32,2048]{2,1,0:T(8,128)(2,1)}, bf16[3,32,2048]{2,1,0:T(8,128)(2,1)S(1)}, u32[]{:S(2)}) copy-start(bf16[3,32,2048]{2,1,0:T(8,128)(2,1)S(1)} %collective-permute-done.6.rest_3_) | copy-start | bytes 1179652
  53.5 3.4 %collective-permute-start.10 = (bf16[3,32,2048]{2,1,0:T(8,128)(2,1)S(1)}, bf16[3,32,2048]{2,1,0:T(8,128)(2,1)}, u32[]{:S(2)}, u32[]{:S(2)}) collective-permute-start(bf16[3,32,2048]{2,1,0:T(8,128)(2,1)S(1)} %collective-permute-done.6.rest_3_), channel_id=1, source_target_pairs={{0,1},{1,0},{2,3},{3,2},{4,5},{5,4},{6,7},{7,6},{8,9},{9,8},{10,11... | collective-permute-start | bytes 1179656 | tf_op jit(solution)/shard_map/ppermute | solution.py:413
  55.5 1.5 %copy-start.8 = (bf16[3,32,2048]{2,1,0:T(8,128)(2,1)}, bf16[3,32,2048]{2,1,0:T(8,128)(2,1)S(1)}, u32[]{:S(2)}) copy-start(bf16[3,32,2048]{2,1,0:T(8,128)(2,1)S(1)} %collective-permute-done.7.rest_4_) | copy-start | bytes 1179652
  55.5 1.5 %copy-start.9 = (bf16[3,32,2048]{2,1,0:T(8,128)(2,1)}, bf16[3,32,2048]{2,1,0:T(8,128)(2,1)S(1)}, u32[]{:S(2)}) copy-start(bf16[3,32,2048]{2,1,0:T(8,128)(2,1)S(1)} %collective-permute-done.8.rest_5_) | copy-start | bytes 1179652
  55.5 1.5 %copy-start.10 = (bf16[3,32,2048]{2,1,0:T(8,128)(2,1)}, bf16[3,32,2048]{2,1,0:T(8,128)(2,1)S(1)}, u32[]{:S(2)}) copy-start(bf16[3,32,2048]{2,1,0:T(8,128)(2,1)S(1)} %collective-permute-done.9.rest_6_) | copy-start | bytes 1179652
  57.0 14.0 %copy-start.2 = (s32[16,2]{0,1:T(2,128)S(1)}, s32[16,2]{0,1:T(2,128)}, u32[]{:S(2)}) copy-start(s32[16,2]{0,1:T(2,128)} %param.27) | copy-start | bytes 388
  57.0 14.0 %copy-start.3 = (bf16[16,2]{0,1:T(2,128)(2,1)S(1)}, bf16[16,2]{0,1:T(2,128)(2,1)}, u32[]{:S(2)}) copy-start(bf16[16,2]{0,1:T(2,128)(2,1)} %param.28) | copy-start | bytes 196
  63.6 27.0 %all-to-all-start.1 = ((bf16[256,8,128]{2,1,0:T(8,128)(2,1)}), bf16[256,8,128]{2,1,0:T(8,128)(2,1)S(1)}, u32[]{:S(2)}, u32[]{:S(2)}) async-start(bf16[256,8,128]{2,1,0:T(8,128)(2,1)} %bitcast.13), calls=%async_computation.1 | async-start | bytes 1048576 | tf_op jit(solution)/shard_map/all_to_all | solution.py:417

commit v4 on v3

--- a/solution.py
+++ b/solution.py
@@ -15,7 +15,7 @@
 KIB = 1024
 MESSAGES = 512
 PART = 512
-RETURNED = 2048
+RETURNED = 512
 epsilon = 1e-06
 NT = (((1,), (1,)), ((), ()))
 VMEM = pl.BlockSpec(memory_space=pltpu.VMEM)
@@ -63,10 +63,20 @@
 
 
 def attention_kernel(
-    len_ref, bias_ref, tok_ref, gain_ref, hgain_ref, route_ref, wq_hbm, kv_hbm, wo_hbm,
+    len_hbm, bias_hbm, tok_hbm, gain_hbm, hgain_hbm, route_hbm, wq_hbm, kv_hbm, wo_hbm,
     out_ref, pick_ref,
-    wq_v, kv_v, key_v, value_v, wo_v, q_sem, kv_sem, o_sem,
+    len_v, bias_v, tok_v, gain_v, hgain_v, route_v,
+    wq_v, kv_v, key_v, value_v, wo_v, small_sem, q_sem, kv_sem, o_sem,
 ):
+    smalls = [
+        pltpu.make_async_copy(src, dst, small_sem.at[k])
+        for k, (src, dst) in enumerate((
+            (tok_hbm, tok_v), (gain_hbm, gain_v), (route_hbm, route_v), (len_hbm, len_v),
+            (bias_hbm, bias_v), (hgain_hbm, hgain_v),
+        ))
+    ]
+    for copy in smalls:
+        copy.start()
     copy_q = pltpu.make_async_copy(wq_hbm, wq_v, q_sem)
     copy_q.start()
     copies = []
@@ -76,11 +86,13 @@
         copies.append(copy)
     copy_o = pltpu.make_async_copy(wo_hbm, wo_v, o_sem)
     copy_o.start()
-    wide = tok_ref[...].astype(jnp.float32)
+    for copy in smalls:
+        copy.wait()
+    wide = tok_v[...].astype(jnp.float32)
     scale = lax.rsqrt(jnp.mean(wide * wide, axis=-1, keepdims=True) + epsilon)
-    normed = (wide * scale * gain_ref[...]).astype(jnp.bfloat16)
+    normed = (wide * scale * gain_v[...]).astype(jnp.bfloat16)
     normed = jnp.concatenate([normed[:, : WIDTH // 2], normed[:, WIDTH // 2 :]], axis=0)
-    pick_ref[...] = picks_of(route_ref[...])
+    pick_ref[...] = picks_of(route_v[...])
 
     lane = lax.broadcasted_iota(jnp.int32, (HALF, LANES), 1)
     row = lax.broadcasted_iota(jnp.int32, (HALF, LANES), 0)
@@ -88,7 +100,10 @@
     tri_col = lax.broadcasted_iota(jnp.int32, (LANES, 2 * LANES), 1)
     tri = ((tri_row >= tri_col) | (tri_col >= LANES)).astype(jnp.bfloat16)
     position = lax.broadcasted_iota(jnp.int32, (HALF, CACHE), 1)
-    bias = jnp.where(row[:, :1] < 4, bias_ref[0], bias_ref[1])
+    bias = jnp.where(row[:, :1] < 4, bias_v[:, 0:1], bias_v[:, 1:2])
+    lengths = len_v[...].astype(jnp.float32)
+    seq = lax.broadcasted_iota(jnp.int32, (HALF, ROWS), 1)
+    seq_row = lax.broadcasted_iota(jnp.int32, (HALF, ROWS), 0) % 4
     wide_lane = lax.broadcasted_iota(jnp.int32, (CACHE, LANES), 1)
     chunks = CACHE // LANES
 
@@ -122,10 +137,8 @@
         return scores * 0.125 + bias
 
     def attended(group, scores):
-        length = jnp.full((HALF, 1), len_ref[group * 4], jnp.int32)
-        for j in range(1, 4):
-            length = jnp.where(row[:, :1] % 4 == j, len_ref[group * 4 + j], length)
-        valid = position < length
+        mine = jnp.where(seq == group * 4 + seq_row, lengths, 0.0)
+        valid = position < jnp.sum(mine, axis=-1, keepdims=True).astype(jnp.int32)
         soft = jnp.maximum(scores, 0.0) + jnp.log1p(jnp.exp(-jnp.abs(scores)))
         soft = jnp.where(valid, soft, 0.0)
         stacked = jnp.concatenate(
@@ -156,7 +169,7 @@
             own = jnp.where(here, mixed[:, p * LANES : (p + 1) * LANES], own)
         mean = jnp.sum(own * own, axis=-1, keepdims=True) * (1.0 / HEAD)
         own = (own + pltpu.roll(own, HEAD, 1)) * lax.rsqrt(mean + epsilon)
-        return jnp.where(lane < HEAD, own, pltpu.roll(own, 4, 0)) * hgain_ref[...]
+        return jnp.where(lane < HEAD, own, pltpu.roll(own, 4, 0)) * hgain_v[...]
 
     scores = scored(0)
     heads = []
@@ -186,14 +199,21 @@
             pltpu.VMEM((ROWS, WIDTH), jnp.bfloat16),
             pltpu.VMEM((4 * ROWS, MESSAGES), jnp.bfloat16),
         ),
-        in_specs=[SMEM, SMEM, VMEM, VMEM, VMEM, VMEM] + [HBM] * 3,
+        in_specs=[HBM] * 9,
         out_specs=(VMEM, VMEM),
         scratch_shapes=[
+            pltpu.VMEM((1, ROWS), jnp.int32),
+            pltpu.VMEM((1, 2), jnp.float32),
+            pltpu.VMEM((ROWS, WIDTH), jnp.bfloat16),
+            pltpu.VMEM((1, WIDTH), jnp.float32),
+            pltpu.VMEM((1, LANES), jnp.float32),
+            pltpu.VMEM((2, ROWS), jnp.int32),
             pltpu.VMEM((WIDTH, LANES), jnp.bfloat16),
             pltpu.VMEM((ROWS, CACHE, LANES), jnp.bfloat16),
             pltpu.VMEM((4, CACHE, 2 * LANES), jnp.bfloat16),
             pltpu.VMEM((4, CACHE, 2 * LANES), jnp.bfloat16),
             pltpu.VMEM((LANES, WIDTH), jnp.bfloat16),
+            pltpu.SemaphoreType.DMA((6,)),
             pltpu.SemaphoreType.DMA,
             pltpu.SemaphoreType.DMA((ROWS,)),
             pltpu.SemaphoreType.DMA,
@@ -202,8 +222,10 @@
             flops=400_000_000, bytes_accessed=6_000_000, transcendentals=200_000
         ),
     )(
-        lengths, stick_bias, tokens, attn_gain.reshape(1, -1), head_gain.reshape(1, -1), routes.T,
-        *in_hbm(w_query, kv_cache, w_attn_out),
+        *in_hbm(
+            lengths.reshape(1, -1), stick_bias.reshape(1, -1), tokens, attn_gain.reshape(1, -1),
+            head_gain.reshape(1, -1), routes.T, w_query, kv_cache, w_attn_out,
+        ),
     )
 
 
@@ -211,13 +233,12 @@
     shape = (ROWS, RETURNED)
     row = lax.broadcasted_iota(jnp.int32, shape, 0)
     col = lax.broadcasted_iota(jnp.int32, shape, 1)
-    device, t = 31 - (col >> 6), 7 - ((col >> 3) & 7)
-    kind, slot, side = (col >> 2) & 1, (col >> 1) & 1, col & 1
+    device, kind, slot, side = 31 - (col >> 4), (col >> 2) & 3, (col >> 1) & 1, col & 1
     first, second = hits_of(route_ref[...], device, slot)
     one, two = columns_of(weight_ref[...])
     expert = jnp.where(first, one, jnp.where(second, two, 0.0))
-    dense = jnp.where(row == quarter_of(device, t & 1, slot), branch_ref[:, 0:1], 0.0)
-    value = jnp.where(kind == 0, expert, dense)
+    dense = jnp.where(row == quarter_of(device, kind - 1, slot), branch_ref[:, 0:1], 0.0)
+    value = jnp.where(kind == 0, expert, jnp.where(kind == 3, 0.0, dense))
     both = jnp.concatenate([jnp.where(side == h, value, 0.0) for h in range(2)], axis=0)
     mix_ref[...] = both.astype(jnp.bfloat16)
 
@@ -237,12 +258,14 @@
 
 def dispatch_kernel(
     a_ref, b_ref, c_ref, d_ref, tok_ref, gain_ref, gate_ref, pick_ref,
-    send_ref, res_ref, branch_ref,
+    send_ref, res_ref, branch_ref, total_v,
 ):
     total = a_ref[...].astype(jnp.float32) + b_ref[...].astype(jnp.float32)
     total = total + (c_ref[...].astype(jnp.float32) + d_ref[...].astype(jnp.float32))
     total = total + tok_ref[...].astype(jnp.float32)
-    res_ref[...] = total
+    total_v[...] = total
+    at = pl.multiple_of(lax.axis_index("tp") * 256, 256)
+    res_ref[...] = total_v[:, pl.ds(at, 256)]
     scale = lax.rsqrt(jnp.mean(total * total, axis=-1, keepdims=True) + epsilon)
     normed = (total * scale * gain_ref[...]).astype(jnp.bfloat16)
     logit = jnp.sum(
@@ -260,11 +283,12 @@
         dispatch_kernel,
         out_shape=(
             jax.ShapeDtypeStruct((MESSAGES, PART), jnp.bfloat16),
-            jax.ShapeDtypeStruct((ROWS, WIDTH), jnp.float32),
+            jax.ShapeDtypeStruct((ROWS, 256), jnp.float32),
             jax.ShapeDtypeStruct((ROWS, LANES), jnp.float32),
         ),
         in_specs=[VMEM] * 8,
         out_specs=(VMEM, VMEM, VMEM),
+        scratch_shapes=[pltpu.VMEM((ROWS, WIDTH), jnp.float32)],
         compiler_params=pltpu.CompilerParams(vmem_limit_bytes=8192 * KIB),
         cost_estimate=pl.CostEstimate(
             flops=40_000_000, bytes_accessed=1_500_000, transcendentals=100
@@ -272,19 +296,42 @@
     )(*shares, tokens, ffn_gain.reshape(1, -1), branch_gate.reshape(1, -1), picks)
 
 
-def feed_kernel(got_ref, eg_hbm, eu_hbm, ed_hbm, *rest):
+def warm_kernel(gate_hbm, up_hbm, gate_out, up_out, sems):
+    copies = [
+        pltpu.make_async_copy(gate_hbm, gate_out, sems.at[0]),
+        pltpu.make_async_copy(up_hbm, up_out, sems.at[1]),
+    ]
+    for copy in copies:
+        copy.start()
+    for copy in copies:
+        copy.wait()
+
+
+def warm(gate, up):
+    return pl.pallas_call(
+        warm_kernel,
+        out_shape=(pltpu.VMEM((WIDTH, 256), jnp.bfloat16),) * 2,
+        in_specs=[HBM] * 2,
+        out_specs=(VMEM, VMEM),
+        scratch_shapes=[pltpu.SemaphoreType.DMA((2,))],
+        compiler_params=pltpu.CompilerParams(vmem_limit_bytes=4096 * KIB),
+        cost_estimate=pl.CostEstimate(
+            flops=1_000_000, bytes_accessed=4_000_000, transcendentals=0
+        ),
+    )(*in_hbm(gate, up))
+
+
+def feed_kernel(got_ref, eg_ref, eu_ref, ed_hbm, *rest):
     packs = rest[:8]
-    out_ref, wide_v, back_v, eg_v, eu_v, ed_v, dg_v, du_v, dd_v, e_sem, d_sem = rest[8:]
-    expert_copies = [
-        pltpu.make_async_copy(src, dst, e_sem.at[k])
-        for k, (src, dst) in enumerate(((eg_hbm, eg_v), (eu_hbm, eu_v), (ed_hbm, ed_v)))
-    ]
+    keep_ref, send_ref, wide_v, ed_v, dg_v, du_v, dd_v, e_sem, d_sem = rest[8:]
+    lower = lax.axis_index("tp") % 2 == 0
+    copy_e = pltpu.make_async_copy(ed_hbm, ed_v, e_sem)
     dense_copies = [
         pltpu.make_async_copy(pack.at[k], dst.at[pl.ds(32 * i, 32), :], d_sem.at[8 * k + i])
         for k, dst in enumerate((dg_v, du_v, dd_v))
         for i, pack in enumerate(packs)
     ]
-    for copy in expert_copies + dense_copies:
+    for copy in [copy_e] + dense_copies:
         copy.start()
     for l in range(4):
         wide_v[l] = got_ref[:, l * LANES : (l + 1) * LANES].astype(jnp.float32)
@@ -301,23 +348,20 @@
         return jnp.concatenate(parts, axis=1).astype(jnp.bfloat16)
 
     def packed(kind, value):
-        for t in range(8):
-            for slot in range(2):
-                for h in range(2):
-                    at = t * 256 + h * LANES
-                    first = (7 - t) * 8 + kind * 4 + slot * 2 + h
-                    back_v[pl.ds(first, 32, stride=64), :] = value[
-                        slot * 32 : slot * 32 + 32, at : at + LANES
-                    ]
+        here = slice(kind * 64, kind * 64 + 64)
+        for y in range(4):
+            even = value[:, 512 * y : 512 * y + 256]
+            odd = value[:, 512 * y + 256 : 512 * y + 512]
+            there = slice(256 * y, 256 * y + 256)
+            keep_ref[here, there] = jnp.where(lower, even, odd)
+            send_ref[here, there] = jnp.where(lower, odd, even).astype(jnp.bfloat16)
 
     rows = unpacked(0)
     dense_rows = unpacked(1)
-    expert_copies[0].wait()
-    a = jnp.dot(rows, eg_v[...], preferred_element_type=jnp.float32)
-    expert_copies[1].wait()
-    b = jnp.dot(rows, eu_v[...], preferred_element_type=jnp.float32)
+    a = jnp.dot(rows, eg_ref[...], preferred_element_type=jnp.float32)
+    b = jnp.dot(rows, eu_ref[...], preferred_element_type=jnp.float32)
     hidden = (a / (1.0 + jnp.exp(-a)) * b).astype(jnp.bfloat16)
-    expert_copies[2].wait()
+    copy_e.wait()
     packed(0, jnp.dot(hidden, ed_v[...], preferred_element_type=jnp.float32))
     for copy in dense_copies[:8]:
         copy.wait()
@@ -329,32 +373,89 @@
     for copy in dense_copies[16:]:
         copy.wait()
     packed(1, jnp.dot(hidden, dd_v[...], preferred_element_type=jnp.float32))
-    out_ref[...] = back_v[...].astype(jnp.bfloat16)
 
 
 def feed(got, gate, up, down, packs):
     return pl.pallas_call(
         feed_kernel,
-        out_shape=jax.ShapeDtypeStruct((RETURNED, LANES), jnp.bfloat16),
-        in_specs=[VMEM] + [HBM] * 11,
-        out_specs=VMEM,
+        out_shape=(
+            jax.ShapeDtypeStruct((128, 1024), jnp.float32),
+            jax.ShapeDtypeStruct((128, 1024), jnp.bfloat16),
+        ),
+        in_specs=[VMEM] * 3 + [HBM] * 9,
+        out_specs=(VMEM, VMEM),
         scratch_shapes=[
             pltpu.VMEM((4, MESSAGES, LANES), jnp.float32),
-            pltpu.VMEM((RETURNED, LANES), jnp.float32),
-            pltpu.VMEM((WIDTH, 256), jnp.bfloat16),
-            pltpu.VMEM((WIDTH, 256), jnp.bfloat16),
             pltpu.VMEM((256, WIDTH), jnp.bfloat16),
             pltpu.VMEM((256, WIDTH), jnp.bfloat16),
             pltpu.VMEM((256, WIDTH), jnp.bfloat16),
             pltpu.VMEM((256, WIDTH), jnp.bfloat16),
-            pltpu.SemaphoreType.DMA((3,)),
+            pltpu.SemaphoreType.DMA,
             pltpu.SemaphoreType.DMA((24,)),
         ],
         compiler_params=pltpu.CompilerParams(vmem_limit_bytes=24576 * KIB),
         cost_estimate=pl.CostEstimate(
             flops=1_000_000_000, bytes_accessed=7_000_000, transcendentals=40_000
         ),
-    )(got, *in_hbm(gate, up, down, *packs))
+    )(got, gate, up, *in_hbm(down, *packs))
+
+
+def halve_kernel(keep_ref, got_ref, out_ref, one_ref, two_ref, three_ref, sum_v):
+    lower = lax.axis_index("tp") % 2 == 0
+    y = lax.axis_index("tp") // 2
+    for k in range(4):
+        there = slice(256 * k, 256 * k + 256)
+        own, other = keep_ref[64:, there], got_ref[64:, there].astype(jnp.float32)
+        sum_v[k, :64] = keep_ref[:64, there] + got_ref[:64, there].astype(jnp.float32)
+        sum_v[k, 64:128] = jnp.where(lower, own, other)
+        sum_v[k, 128:] = jnp.where(lower, other, own)
+    out_ref[...] = sum_v[y]
+    for step, ref in ((1, one_ref), (2, two_ref), (3, three_ref)):
+        ref[...] = sum_v[(y + step) % 4].astype(jnp.bfloat16)
+
+
+def halve(keep, got):
+    return pl.pallas_call(
+        halve_kernel,
+        out_shape=(jax.ShapeDtypeStruct((192, 256), jnp.float32),)
+        + (jax.ShapeDtypeStruct((192, 256), jnp.bfloat16),) * 3,
+        in_specs=[VMEM] * 2,
+        out_specs=(VMEM,) * 4,
+        scratch_shapes=[pltpu.VMEM((4, 192, 256), jnp.float32)],
+        compiler_params=pltpu.CompilerParams(vmem_limit_bytes=8192 * KIB),
+        cost_estimate=pl.CostEstimate(
+            flops=1_000_000, bytes_accessed=1_000_000, transcendentals=0
+        ),
+    )(keep, got)
+
+
+def pack_kernel(a_ref, b_ref, c_ref, d_ref, out_ref, back_v):
+    total = a_ref[...] + b_ref[...].astype(jnp.float32)
+    total = total + (c_ref[...].astype(jnp.float32) + d_ref[...].astype(jnp.float32))
+    for kind in range(4):
+        for slot in range(2):
+            for h in range(2):
+                at = kind * 64 + slot * 32
+                if kind < 3:
+                    piece = total[at : at + 32, h * LANES : (h + 1) * LANES]
+                else:
+                    piece = jnp.zeros((32, LANES), jnp.float32)
+                back_v[pl.ds(kind * 4 + slot * 2 + h, 32, stride=16), :] = piece
+    out_ref[...] = back_v[...].astype(jnp.bfloat16)
+
+
+def pack(blocks):
+    return pl.pallas_call(
+        pack_kernel,
+        out_shape=jax.ShapeDtypeStruct((RETURNED, LANES), jnp.bfloat16),
+        in_specs=[VMEM] * 4,
+        out_specs=VMEM,
+        scratch_shapes=[pltpu.VMEM((RETURNED, LANES), jnp.float32)],
+        compiler_params=pltpu.CompilerParams(vmem_limit_bytes=8192 * KIB),
+        cost_estimate=pl.CostEstimate(
+            flops=1_000_000, bytes_accessed=500_000, transcendentals=0
+        ),
+    )(*blocks)
 
 
 def finish_kernel(mix_ref, got_ref, res_ref, out_ref):
@@ -386,7 +487,6 @@
     w_dense_gate, w_dense_up, w_dense_down,
 ):
     single, half = jnp.float32, jnp.bfloat16
-    t = lax.axis_index("tp")
     swap = [(i, i ^ 1) for i in range(8)]
 
     square = [(i, i ^ 1) for i in range(32)]
@@ -411,16 +511,20 @@
 
     for k in range(4):
         packs.append(lax.ppermute(packs[k], "tp", swap))
-    back = feed(
-        got.reshape(MESSAGES, PART), w_exp_gate[0], w_exp_up[0], w_exp_down[0], packs
-    )
+    mix = mix_table(route_expert, route_weight, branch)
+    gate, up = warm(w_exp_gate[0], w_exp_up[0])
+    keep, give = feed(got.reshape(MESSAGES, PART), gate, up, w_exp_down[0], packs)
+    taken = lax.ppermute(give, "tp", swap)
+    mine, *others = halve(keep, taken)
+    blocks = [mine]
+    for step in (1, 3, 2):
+        blocks.append(along_y(others[step - 1], step))
+    back = pack(blocks)
     returned = lax.all_to_all(
-        back.reshape(256, 8, LANES), ("ep", "tp"), 0, 0, tiled=True,
-        axis_index_groups=[list(range(255, -1, -1))],
-    )
-    mix = mix_table(route_expert, route_weight, branch)
-    residual_cols = lax.dynamic_slice_in_dim(residual, t * 256, 256, 1)
-    return finish(mix, returned.reshape(RETURNED, LANES), residual_cols)
+        back.reshape(32, 16, LANES), "ep", 0, 0, tiled=True,
+        axis_index_groups=[list(range(31, -1, -1))],
+    )
+    return finish(mix, returned.reshape(RETURNED, LANES), residual)
 
 
 def solution(mesh):

time: 91.6 us -> 90.7 us (level); the launches traced: 91.4 us -> 89 us
  waiting for transfers between devices: 40.3 us -> 31.2 us
  starting transfers between devices: 34.6 us -> 39.7 us
  local copies, waits for them, and re-layouts: 0.08 us -> 1.55 us
    all_to_all x1, waiting for transfers between devices: 19.2 us -> 5.28 us  [layer(): lax.all_to_all(back.reshape(32, 16, LANES), 'ep', 0, 0, tiled=True, axis_...]
    ppermute x3 -> x6, waiting for transfers between devices: 3.69 us -> 8.33 us  [along_y(): return lax.ppermute(x, 'tp', [(i, (i + 2 * step) % 8) for i in range(8)])]
    ppermute x3 -> x6, starting transfers between devices: 3.67 us -> 6.75 us  [along_y(): return lax.ppermute(x, 'tp', [(i, (i + 2 * step) % 8) for i in range(8)])]
    all_to_all x1, starting transfers between devices: 7.43 us -> 9.18 us  [layer(): lax.all_to_all(back.reshape(32, 16, LANES), 'ep', 0, 0, tiled=True, axis_...]
    ppermute x0 -> x1, waiting for transfers between devices: none -> 1.52 us  [layer(): taken = lax.ppermute(give, 'tp', swap)]
    unnamed x30 -> x26, local copies, waits for them, and re-layouts: 0.06 us -> 1.54 us
    ppermute x4, waiting for transfers between devices: 1.44 us -> 0.01 us  [layer(): packs.append(lax.ppermute(packs[k], 'tp', swap))]
    pallas_call x1 -> x4, Pallas kernels: 6.54 us -> 7.44 us  [the longest x1 4.98 us: feed(): pl.pallas_call(feed_kernel, out_shape=(jax.ShapeDtypeStruct((128, 1024),...]
  transfers between devices with their start and end apart: 13 -> 17, of which waited for: 7 -> 9; matrix products, arithmetic and copies ran while one was open for 0% -> 0% of each run, Pallas kernels for 2% -> 3%
where the time goes in v4:
time: 90.7 us; the launch traced here: 89 us
  starting transfers between devices  39.7 us (44%)
  waiting for transfers between devices  31.2 us (34%)
  Pallas kernels  16.3 us (18%)
  local copies, waits for them, and re-layouts  1.55 us (2%)
    all_to_all x1, starting transfers between devices, layer(): lax.all_to_all(send.reshape(32, 16, PART), 'ep', 0, 0, tiled=True, axis_i...  10.2 us
    ppermute x1, waiting for transfers between devices, layer(): packs.append(lax.ppermute(own, 'ep', square))  10.2 us
    all_to_all x1, starting transfers between devices, layer(): lax.all_to_all(back.reshape(32, 16, LANES), 'ep', 0, 0, tiled=True, axis_...  9.18 us
    ppermute x4, starting transfers between devices, layer(): packs.append(lax.ppermute(packs[k], 'tp', swap))  8.4 us
    ppermute x6, waiting for transfers between devices, along_y(): return lax.ppermute(x, 'tp', [(i, (i + 2 * step) % 8) for i in range(8)])  8.33 us
    ppermute x6, starting transfers between devices, along_y(): return lax.ppermute(x, 'tp', [(i, (i + 2 * step) % 8) for i in range(8)])  6.75 us
    pallas_call x1, Pallas kernels, attention(): pl.pallas_call(attention_kernel, out_shape=(pltpu.VMEM((ROWS, WIDTH), jnp...  6.67 us
    all_to_all x1, waiting for transfers between devices, layer(): lax.all_to_all(back.reshape(32, 16, LANES), 'ep', 0, 0, tiled=True, axis_...  5.28 us
  transfers between devices with their start and end apart: 17, of which 9 were waited for; matrix products, arithmetic and copies ran while one was open for 0% of the time, Pallas kernels for 3%

profile of v4, /device:TPU:1, one launch (start us, length us, event | category | flops | bytes accessed | tf_op | source)
XLA Modules:
  0.0 89.0 jit_solution(6119247637371014681)
XLA Ops:
  0.0 6.7 %shard_map.172 = (bf16[16,2048]{1,0:T(8,128)(2,1)S(1)}, bf16[64,512]{1,0:T(8,128)(2,1)S(1)}) custom-call(s32[1,16]{1,0:T(1,128)} %bitcast.30, f32[1,2]{1,0:T(1,128)} %bitcast.31, bf16[16,2048]{1,0:T(8,128)(2,1)} %tok_ref.1, f32[1,2048]{1,0:T(1,128)} %bitcast.29, f32[1,128]{1,0:T(1,128)} %bitcast.32, s32[2,16]{1,0:T(2,128)} %bitcast.20, ...), custom_call_target="tpu_custom_call" | custom-call | flops 400000000 | bytes 6000000 | tf_op jit(solution)/shard_map/pallas_call | solution.py:196
  6.7 3.3 %collective-permute-start = (bf16[16,2048]{1,0:T(8,128)(2,1)S(1)}, bf16[16,2048]{1,0:T(8,128)(2,1)S(1)}, u32[]{:S(2)}, u32[]{:S(2)}) collective-permute-start(bf16[16,2048]{1,0:T(8,128)(2,1)S(1)} %get-tuple-element.18), channel_id=1, source_target_pairs={{0,1},{1,0},{2,3},{3,2},{4,5},{5,4},{6,7},{7,6},{8,9},{9,8},{10,11... | collective-permute-start | bytes 196616 | tf_op jit(solution)/shard_map/ppermute | solution.py:500
  10.2 0.7 collective-permute-done
  10.9 0.6 collective-permute-start.1
  11.5 2.2 %collective-permute-start.2 = (bf16[16,2048]{1,0:T(8,128)(2,1)S(1)}, bf16[16,2048]{1,0:T(8,128)(2,1)S(1)}, u32[]{:S(2)}, u32[]{:S(2)}) collective-permute-start(bf16[16,2048]{1,0:T(8,128)(2,1)S(1)} %add_convert_fusion.a_ref), channel_id=1, source_target_pairs={{0,6},{1,7},{2,0},{3,1},{4,2},{5,3},{6,4},{7,5},{8,14},{9,15},{10,... | collective-permute-start | bytes 196616 | tf_op jit(solution)/shard_map/ppermute | solution.py:481
  13.7 0.9 %collective-permute-start.3 = (bf16[16,2048]{1,0:T(8,128)(2,1)S(1)}, bf16[16,2048]{1,0:T(8,128)(2,1)S(1)}, u32[]{:S(2)}, u32[]{:S(2)}) collective-permute-start(bf16[16,2048]{1,0:T(8,128)(2,1)S(1)} %add_convert_fusion.a_ref), channel_id=1, source_target_pairs={{0,4},{1,5},{2,6},{3,7},{4,0},{5,1},{6,2},{7,3},{8,12},{9,13},{10,... | collective-permute-start | bytes 196616 | tf_op jit(solution)/shard_map/ppermute | solution.py:481
  14.6 0.7 collective-permute-done.1.b_ref
  15.3 3.0 %collective-permute-done.3.d_ref = bf16[16,2048]{1,0:T(8,128)(2,1)S(1)} collective-permute-done((bf16[16,2048]{1,0:T(8,128)(2,1)S(1)}, bf16[16,2048]{1,0:T(8,128)(2,1)S(1)}, u32[]{:S(2)}, u32[]{:S(2)}) %collective-permute-start.3) | collective-permute-done | bytes 65568 | tf_op jit(solution)/shard_map/ppermute | solution.py:481
  18.3 1.2 %shard_map.173 = (bf16[512,512]{1,0:T(8,128)(2,1)}, f32[16,256]{1,0:T(8,128)S(1)}, f32[16,128]{1,0:T(8,128)S(1)}) custom-call(bf16[16,2048]{1,0:T(8,128)(2,1)S(1)} %add_convert_fusion.a_ref, bf16[16,2048]{1,0:T(8,128)(2,1)S(1)} %collective-permute-done.1.b_ref, bf16[16,2048]{1,0:T(8,128)(2,1)S(1)} %collective-permute-done.2.c_ref, ...), custom_call_target="tpu_custom_call" | custom-call | flops 40000000 | bytes 1500000 | tf_op jit(solution)/shard_map/pallas_call | solution.py:282
  19.5 10.2 %all-to-all-start = ((bf16[32,16,512]{2,1,0:T(8,128)(2,1)}), bf16[32,16,512]{2,1,0:T(8,128)(2,1)S(1)}, u32[]{:S(2)}, u32[]{:S(2)}) async-start(bf16[32,16,512]{2,1,0:T(8,128)(2,1)} %bitcast.7), calls=%async_computation | async-start | bytes 1048576 | tf_op jit(solution)/shard_map/all_to_all | solution.py:507
  29.7 0.7 collective-permute-start.5
  30.4 0.9 %collective-permute-start.6 = (bf16[3,32,2048]{2,1,0:T(8,128)(2,1)S(1)}, bf16[3,32,2048]{2,1,0:T(8,128)(2,1)}, u32[]{:S(2)}, u32[]{:S(2)}) collective-permute-start(bf16[3,32,2048]{2,1,0:T(8,128)(2,1)S(1)} %collective-permute-done.4.rest_1_), channel_id=1, source_target_pairs={{0,8},{8,0},{16,24},{24,16},{32,40},{40,32},{48,56},{56,48},{64,72... | collective-permute-start | bytes 1179656 | tf_op jit(solution)/shard_map/ppermute | solution.py:505
  31.3 3.0 %collective-permute-start.7 = (bf16[3,32,2048]{2,1,0:T(8,128)(2,1)S(1)}, bf16[3,32,2048]{2,1,0:T(8,128)(2,1)S(1)}, u32[]{:S(2)}, u32[]{:S(2)}) collective-permute-start(bf16[3,32,2048]{2,1,0:T(8,128)(2,1)S(1)} %pad_maximum_fusion.rest_0_), channel_id=1, source_target_pairs={{0,1},{1,0},{2,3},{3,2},{4,5},{5,4},{6,7},{7,6},{8,9},{9,8},{10,11... | collective-permute-start | bytes 1179656 | tf_op jit(solution)/shard_map/ppermute | solution.py:513
  34.3 10.2 %collective-permute-done.5.rest_2_ = bf16[3,32,2048]{2,1,0:T(8,128)(2,1)S(1)} collective-permute-done((bf16[3,32,2048]{2,1,0:T(8,128)(2,1)S(1)}, bf16[3,32,2048]{2,1,0:T(8,128)(2,1)S(1)}, u32[]{:S(2)}, u32[]{:S(2)}) %collective-permute-start.5) | collective-permute-done | bytes 393248 | tf_op jit(solution)/shard_map/ppermute | solution.py:495
  44.5 3.4 %collective-permute-start.9 = (bf16[3,32,2048]{2,1,0:T(8,128)(2,1)S(1)}, bf16[3,32,2048]{2,1,0:T(8,128)(2,1)}, u32[]{:S(2)}, u32[]{:S(2)}) collective-permute-start(bf16[3,32,2048]{2,1,0:T(8,128)(2,1)S(1)} %collective-permute-done.5.rest_2_), channel_id=1, source_target_pairs={{0,1},{1,0},{2,3},{3,2},{4,5},{5,4},{6,7},{7,6},{8,9},{9,8},{10,11... | collective-permute-start | bytes 1179656 | tf_op jit(solution)/shard_map/ppermute | solution.py:513
  48.0 5.1 %collective-permute-done.6.rest_3_ = bf16[3,32,2048]{2,1,0:T(8,128)(2,1)} collective-permute-done((bf16[3,32,2048]{2,1,0:T(8,128)(2,1)S(1)}, bf16[3,32,2048]{2,1,0:T(8,128)(2,1)}, u32[]{:S(2)}, u32[]{:S(2)}) %collective-permute-start.6) | collective-permute-done | bytes 393248 | tf_op jit(solution)/shard_map/ppermute | solution.py:505
  53.1 1.9 %collective-permute-start.10 = (bf16[3,32,2048]{2,1,0:T(8,128)(2,1)}, bf16[3,32,2048]{2,1,0:T(8,128)(2,1)}, u32[]{:S(2)}, u32[]{:S(2)}) collective-permute-start(bf16[3,32,2048]{2,1,0:T(8,128)(2,1)} %collective-permute-done.6.rest_3_), channel_id=1, source_target_pairs={{0,1},{1,0},{2,3},{3,2},{4,5},{5,4},{6,7},{7,6},{8,9},{9,8},{10,11... | collective-permute-start | bytes 1179656 | tf_op jit(solution)/shard_map/ppermute | solution.py:513
  55.0 1.6 %shard_map.175 = (bf16[2048,256]{1,0:T(8,128)(2,1)S(1)}, bf16[2048,256]{1,0:T(8,128)(2,1)S(1)}) custom-call(bf16[2048,256]{1,0:T(8,128)(2,1)} %bitcast.23, bf16[2048,256]{1,0:T(8,128)(2,1)} %bitcast.24), custom_call_target="tpu_custom_call" | custom-call | flops 1000000 | bytes 4000000 | tf_op jit(solution)/shard_map/pallas_call | solution.py:311
  56.6 0.7 copy-done.7
  57.3 0.8 copy-done.8
  58.1 5.0 %shard_map.176 = (f32[128,1024]{1,0:T(8,128)S(1)}, bf16[128,1024]{1,0:T(8,128)(2,1)S(1)}) custom-call(bf16[512,512]{1,0:T(8,128)(2,1)S(1)} %bitcast.17, bf16[2048,256]{1,0:T(8,128)(2,1)S(1)} %get-tuple-element.22.eg_ref, bf16[2048,256]{1,0:T(8,128)(2,1)S(1)} %get-tuple-element.23.eu_ref, bf16[256,2048]{1,0:T(8,128)(2,1)} %bitcast.25, ...), custom_call_target="tpu_custom_call" | custom-call | flops 1000000000 | bytes 7000000 | tf_op jit(solution)/shard_map/pallas_call | solution.py:379
  63.1 0.3 collective-permute-start.11
  63.4 1.5 %collective-permute-done.11.got_ref = bf16[128,1024]{1,0:T(8,128)(2,1)S(1)} collective-permute-done((bf16[128,1024]{1,0:T(8,128)(2,1)S(1)}, bf16[128,1024]{1,0:T(8,128)(2,1)S(1)}, u32[]{:S(2)}, u32[]{:S(2)}) %collective-permute-start.11) | collective-permute-done | bytes 262176 | tf_op jit(solution)/shard_map/ppermute | solution.py:517
  65.0 0.6 collective-permute-start.12
  65.6 2.2 %collective-permute-start.13 = (bf16[192,256]{1,0:T(8,128)(2,1)S(1)}, bf16[192,256]{1,0:T(8,128)(2,1)S(1)}, u32[]{:S(2)}, u32[]{:S(2)}) collective-permute-start(bf16[192,256]{1,0:T(8,128)(2,1)S(1)} %get-tuple-element.28), channel_id=1, source_target_pairs={{0,6},{1,7},{2,0},{3,1},{4,2},{5,3},{6,4},{7,5},{8,14},{9,15},{10,... | collective-permute-start | bytes 294920 | tf_op jit(solution)/shard_map/ppermute | solution.py:481
  67.8 0.3 collective-permute-start.14
  68.1 2.4 %collective-permute-done.12.b_ref = bf16[192,256]{1,0:T(8,128)(2,1)S(1)} collective-permute-done((bf16[192,256]{1,0:T(8,128)(2,1)S(1)}, bf16[192,256]{1,0:T(8,128)(2,1)S(1)}, u32[]{:S(2)}, u32[]{:S(2)}) %collective-permute-start.12) | collective-permute-done | bytes 98336 | tf_op jit(solution)/shard_map/ppermute | solution.py:481
  70.6 2.2 %collective-permute-done.14.d_ref = bf16[192,256]{1,0:T(8,128)(2,1)S(1)} collective-permute-done((bf16[192,256]{1,0:T(8,128)(2,1)S(1)}, bf16[192,256]{1,0:T(8,128)(2,1)S(1)}, u32[]{:S(2)}, u32[]{:S(2)}) %collective-permute-start.14) | collective-permute-done | bytes 98336 | tf_op jit(solution)/shard_map/ppermute | solution.py:481
  72.8 0.8 shard_map.178
  73.6 9.2 %all-to-all-start.1 = ((bf16[32,16,128]{2,1,0:T(8,128)(2,1)}), bf16[32,16,128]{2,1,0:T(8,128)(2,1)S(1)}, u32[]{:S(2)}, u32[]{:S(2)}) async-start(bf16[32,16,128]{2,1,0:T(8,128)(2,1)} %bitcast.15), calls=%async_computation.1 | async-start | bytes 262144 | tf_op jit(solution)/shard_map/all_to_all | solution.py:523
  83.0 5.3 %all-to-all-done.1 = bf16[32,16,128]{2,1,0:T(8,128)(2,1)S(1)} async-done(((bf16[32,16,128]{2,1,0:T(8,128)(2,1)}), bf16[32,16,128]{2,1,0:T(8,128)(2,1)S(1)}, u32[]{:S(2)}, u32[]{:S(2)}) %all-to-all-start.1) | async-done | bytes 131104 | tf_op jit(solution)/shard_map/all_to_all | solution.py:523
  88.3 0.7 shard_map.179
  (39 shorter events, 0.6 us)
Async XLA Ops:
  0.0 18.3 %copy-start = (bf16[16,2048]{1,0:T(8,128)(2,1)S(1)}, bf16[16,2048]{1,0:T(8,128)(2,1)}, u32[]{:S(2)}) copy-start(bf16[16,2048]{1,0:T(8,128)(2,1)} %tok_ref.1) | copy-start | bytes 196612
  0.0 10.0 %copy-start.11 = (bf16[32,2048]{1,0:T(8,128)(2,1)S(1)}, bf16[32,2048]{1,0:T(8,128)(2,1)}, u32[]{:S(2)}) copy-start(bf16[32,2048]{1,0:T(8,128)(2,1)} %param.33) | copy-start | bytes 393220
  0.0 10.0 %copy-start.10 = (bf16[32,2048]{1,0:T(8,128)(2,1)S(1)}, bf16[32,2048]{1,0:T(8,128)(2,1)}, u32[]{:S(2)}) copy-start(bf16[32,2048]{1,0:T(8,128)(2,1)} %param.34) | copy-start | bytes 393220
  0.0 10.0 %copy-start.9 = (bf16[32,2048]{1,0:T(8,128)(2,1)S(1)}, bf16[32,2048]{1,0:T(8,128)(2,1)}, u32[]{:S(2)}) copy-start(bf16[32,2048]{1,0:T(8,128)(2,1)} %param.35) | copy-start | bytes 393220
  0.0 14.6 %copy-start.12 = (bf16[2048]{0:T(1024)(128)(2,1)S(1)}, bf16[2048]{0:T(1024)(128)(2,1)}, u32[]{:S(2)}) copy-start(bf16[2048]{0:T(1024)(128)(2,1)} %param.32) | copy-start | bytes 12292
  0.0 18.3 %copy-start.1 = (f32[2048]{0:T(1024)S(1)}, f32[2048]{0:T(1024)}, u32[]{:S(2)}) copy-start(f32[2048]{0:T(1024)} %param.26) | copy-start | bytes 24580
  6.7 4.2 %collective-permute-start = (bf16[16,2048]{1,0:T(8,128)(2,1)S(1)}, bf16[16,2048]{1,0:T(8,128)(2,1)S(1)}, u32[]{:S(2)}, u32[]{:S(2)}) collective-permute-start(bf16[16,2048]{1,0:T(8,128)(2,1)S(1)} %get-tuple-element.18), channel_id=1, source_target_pairs={{0,1},{1,0},{2,3},{3,2},{4,5},{5,4},{6,7},{7,6},{8,9},{9,8},{10,11... | collective-permute-start | bytes 196616 | tf_op jit(solution)/shard_map/ppermute | solution.py:500
  10.1 48.1 %copy-start.4 = (bf16[3,32,2048]{2,1,0:T(8,128)(2,1)}, bf16[3,32,2048]{2,1,0:T(8,128)(2,1)S(1)}, u32[]{:S(2)}) copy-start(bf16[3,32,2048]{2,1,0:T(8,128)(2,1)S(1)} %pad_maximum_fusion.rest_0_) | copy-start | bytes 1179652
  10.1 20.3 %collective-permute-start.4 = (bf16[3,32,2048]{2,1,0:T(8,128)(2,1)S(1)}, bf16[3,32,2048]{2,1,0:T(8,128)(2,1)S(1)}, u32[]{:S(2)}, u32[]{:S(2)}) collective-permute-start(bf16[3,32,2048]{2,1,0:T(8,128)(2,1)S(1)} %pad_maximum_fusion.rest_0_), channel_id=1, source_target_pairs={{0,32},{8,40},{16,48},{24,56},{32,0},{40,8},{48,16},{56,24},{64,96... | collective-permute-start | bytes 1179656 | tf_op jit(solution)/shard_map/ppermute | solution.py:494
  10.9 4.4 %collective-permute-start.1 = (bf16[16,2048]{1,0:T(8,128)(2,1)S(1)}, bf16[16,2048]{1,0:T(8,128)(2,1)S(1)}, u32[]{:S(2)}, u32[]{:S(2)}) collective-permute-start(bf16[16,2048]{1,0:T(8,128)(2,1)S(1)} %add_convert_fusion.a_ref), channel_id=1, source_target_pairs={{0,2},{1,3},{2,4},{3,5},{4,6},{5,7},{6,0},{7,1},{8,10},{9,11},{10,... | collective-permute-start | bytes 196616 | tf_op jit(solution)/shard_map/ppermute | solution.py:481
  11.5 3.8 %collective-permute-start.2 = (bf16[16,2048]{1,0:T(8,128)(2,1)S(1)}, bf16[16,2048]{1,0:T(8,128)(2,1)S(1)}, u32[]{:S(2)}, u32[]{:S(2)}) collective-permute-start(bf16[16,2048]{1,0:T(8,128)(2,1)S(1)} %add_convert_fusion.a_ref), channel_id=1, source_target_pairs={{0,6},{1,7},{2,0},{3,1},{4,2},{5,3},{6,4},{7,5},{8,14},{9,15},{10,... | collective-permute-start | bytes 196616 | tf_op jit(solution)/shard_map/ppermute | solution.py:481
  13.7 4.6 %collective-permute-start.3 = (bf16[16,2048]{1,0:T(8,128)(2,1)S(1)}, bf16[16,2048]{1,0:T(8,128)(2,1)S(1)}, u32[]{:S(2)}, u32[]{:S(2)}) collective-permute-start(bf16[16,2048]{1,0:T(8,128)(2,1)S(1)} %add_convert_fusion.a_ref), channel_id=1, source_target_pairs={{0,4},{1,5},{2,6},{3,7},{4,0},{5,1},{6,2},{7,3},{8,12},{9,13},{10,... | collective-permute-start | bytes 196616 | tf_op jit(solution)/shard_map/ppermute | solution.py:481
  19.5 38.6 %all-to-all-start = ((bf16[32,16,512]{2,1,0:T(8,128)(2,1)}), bf16[32,16,512]{2,1,0:T(8,128)(2,1)S(1)}, u32[]{:S(2)}, u32[]{:S(2)}) async-start(bf16[32,16,512]{2,1,0:T(8,128)(2,1)} %bitcast.7), calls=%async_computation | async-start | bytes 1048576 | tf_op jit(solution)/shard_map/all_to_all | solution.py:507
  29.7 14.8 %collective-permute-start.5 = (bf16[3,32,2048]{2,1,0:T(8,128)(2,1)S(1)}, bf16[3,32,2048]{2,1,0:T(8,128)(2,1)S(1)}, u32[]{:S(2)}, u32[]{:S(2)}) collective-permute-start(bf16[3,32,2048]{2,1,0:T(8,128)(2,1)S(1)} %pad_maximum_fusion.rest_0_), channel_id=1, source_target_pairs={{0,8},{8,0},{16,24},{24,16},{32,40},{40,32},{48,56},{56,48},{64,72... | collective-permute-start | bytes 1179656 | tf_op jit(solution)/shard_map/ppermute | solution.py:495
  30.4 27.7 %copy-start.5 = (bf16[3,32,2048]{2,1,0:T(8,128)(2,1)}, bf16[3,32,2048]{2,1,0:T(8,128)(2,1)S(1)}, u32[]{:S(2)}) copy-start(bf16[3,32,2048]{2,1,0:T(8,128)(2,1)S(1)} %collective-permute-done.4.rest_1_) | copy-start | bytes 1179652
  30.4 22.7 %collective-permute-start.6 = (bf16[3,32,2048]{2,1,0:T(8,128)(2,1)S(1)}, bf16[3,32,2048]{2,1,0:T(8,128)(2,1)}, u32[]{:S(2)}, u32[]{:S(2)}) collective-permute-start(bf16[3,32,2048]{2,1,0:T(8,128)(2,1)S(1)} %collective-permute-done.4.rest_1_), channel_id=1, source_target_pairs={{0,8},{8,0},{16,24},{24,16},{32,40},{40,32},{48,56},{56,48},{64,72... | collective-permute-start | bytes 1179656 | tf_op jit(solution)/shard_map/ppermute | solution.py:505
  31.3 25.2 %collective-permute-start.7 = (bf16[3,32,2048]{2,1,0:T(8,128)(2,1)S(1)}, bf16[3,32,2048]{2,1,0:T(8,128)(2,1)S(1)}, u32[]{:S(2)}, u32[]{:S(2)}) collective-permute-start(bf16[3,32,2048]{2,1,0:T(8,128)(2,1)S(1)} %pad_maximum_fusion.rest_0_), channel_id=1, source_target_pairs={{0,1},{1,0},{2,3},{3,2},{4,5},{5,4},{6,7},{7,6},{8,9},{9,8},{10,11... | collective-permute-start | bytes 1179656 | tf_op jit(solution)/shard_map/ppermute | solution.py:513
  34.3 22.2 %collective-permute-start.8 = (bf16[3,32,2048]{2,1,0:T(8,128)(2,1)S(1)}, bf16[3,32,2048]{2,1,0:T(8,128)(2,1)S(1)}, u32[]{:S(2)}, u32[]{:S(2)}) collective-permute-start(bf16[3,32,2048]{2,1,0:T(8,128)(2,1)S(1)} %collective-permute-done.4.rest_1_), channel_id=1, source_target_pairs={{0,1},{1,0},{2,3},{3,2},{4,5},{5,4},{6,7},{7,6},{8,9},{9,8},{10,11... | collective-permute-start | bytes 1179656 | tf_op jit(solution)/shard_map/ppermute | solution.py:513
  44.5 12.0 %copy-start.6 = (bf16[3,32,2048]{2,1,0:T(8,128)(2,1)}, bf16[3,32,2048]{2,1,0:T(8,128)(2,1)S(1)}, u32[]{:S(2)}) copy-start(bf16[3,32,2048]{2,1,0:T(8,128)(2,1)S(1)} %collective-permute-done.5.rest_2_) | copy-start | bytes 1179652
  44.5 13.6 %collective-permute-start.9 = (bf16[3,32,2048]{2,1,0:T(8,128)(2,1)S(1)}, bf16[3,32,2048]{2,1,0:T(8,128)(2,1)}, u32[]{:S(2)}, u32[]{:S(2)}) collective-permute-start(bf16[3,32,2048]{2,1,0:T(8,128)(2,1)S(1)} %collective-permute-done.5.rest_2_), channel_id=1, source_target_pairs={{0,1},{1,0},{2,3},{3,2},{4,5},{5,4},{6,7},{7,6},{8,9},{9,8},{10,11... | collective-permute-start | bytes 1179656 | tf_op jit(solution)/shard_map/ppermute | solution.py:513
  53.1 5.0 %collective-permute-start.10 = (bf16[3,32,2048]{2,1,0:T(8,128)(2,1)}, bf16[3,32,2048]{2,1,0:T(8,128)(2,1)}, u32[]{:S(2)}, u32[]{:S(2)}) collective-permute-start(bf16[3,32,2048]{2,1,0:T(8,128)(2,1)} %collective-permute-done.6.rest_3_), channel_id=1, source_target_pairs={{0,1},{1,0},{2,3},{3,2},{4,5},{5,4},{6,7},{7,6},{8,9},{9,8},{10,11... | collective-permute-start | bytes 1179656 | tf_op jit(solution)/shard_map/ppermute | solution.py:513
  56.6 0.8 copy-start.7
  57.3 0.8 copy-start.8
  58.1 24.6 %copy-start.2 = (s32[16,2]{0,1:T(2,128)S(1)}, s32[16,2]{0,1:T(2,128)}, u32[]{:S(2)}) copy-start(s32[16,2]{0,1:T(2,128)} %param.27) | copy-start | bytes 388
  58.1 24.6 %copy-start.3 = (bf16[16,2]{0,1:T(2,128)(2,1)S(1)}, bf16[16,2]{0,1:T(2,128)(2,1)}, u32[]{:S(2)}) copy-start(bf16[16,2]{0,1:T(2,128)(2,1)} %param.28) | copy-start | bytes 196
  63.1 1.8 %collective-permute-start.11 = (bf16[128,1024]{1,0:T(8,128)(2,1)S(1)}, bf16[128,1024]{1,0:T(8,128)(2,1)S(1)}, u32[]{:S(2)}, u32[]{:S(2)}) collective-permute-start(bf16[128,1024]{1,0:T(8,128)(2,1)S(1)} %get-tuple-element.25), channel_id=1, source_target_pairs={{0,1},{1,0},{2,3},{3,2},{4,5},{5,4},{6,7},{7,6},{8,9},{9,8},{10,11... | collective-permute-start | bytes 786440 | tf_op jit(solution)/shard_map/ppermute | solution.py:517
  65.0 5.5 %collective-permute-start.12 = (bf16[192,256]{1,0:T(8,128)(2,1)S(1)}, bf16[192,256]{1,0:T(8,128)(2,1)S(1)}, u32[]{:S(2)}, u32[]{:S(2)}) collective-permute-start(bf16[192,256]{1,0:T(8,128)(2,1)S(1)} %get-tuple-element.27), channel_id=1, source_target_pairs={{0,2},{1,3},{2,4},{3,5},{4,6},{5,7},{6,0},{7,1},{8,10},{9,11},{10,... | collective-permute-start | bytes 294920 | tf_op jit(solution)/shard_map/ppermute | solution.py:481
  65.6 4.9 %collective-permute-start.13 = (bf16[192,256]{1,0:T(8,128)(2,1)S(1)}, bf16[192,256]{1,0:T(8,128)(2,1)S(1)}, u32[]{:S(2)}, u32[]{:S(2)}) collective-permute-start(bf16[192,256]{1,0:T(8,128)(2,1)S(1)} %get-tuple-element.28), channel_id=1, source_target_pairs={{0,6},{1,7},{2,0},{3,1},{4,2},{5,3},{6,4},{7,5},{8,14},{9,15},{10,... | collective-permute-start | bytes 294920 | tf_op jit(solution)/shard_map/ppermute | solution.py:481
  67.8 5.0 %collective-permute-start.14 = (bf16[192,256]{1,0:T(8,128)(2,1)S(1)}, bf16[192,256]{1,0:T(8,128)(2,1)S(1)}, u32[]{:S(2)}, u32[]{:S(2)}) collective-permute-start(bf16[192,256]{1,0:T(8,128)(2,1)S(1)} %get-tuple-element.29), channel_id=1, source_target_pairs={{0,4},{1,5},{2,6},{3,7},{4,0},{5,1},{6,2},{7,3},{8,12},{9,13},{10,... | collective-permute-start | bytes 294920 | tf_op jit(solution)/shard_map/ppermute | solution.py:481
  73.6 14.7 %all-to-all-start.1 = ((bf16[32,16,128]{2,1,0:T(8,128)(2,1)}), bf16[32,16,128]{2,1,0:T(8,128)(2,1)S(1)}, u32[]{:S(2)}, u32[]{:S(2)}) async-start(bf16[32,16,128]{2,1,0:T(8,128)(2,1)} %bitcast.15), calls=%async_computation.1 | async-start | bytes 262144 | tf_op jit(solution)/shard_map/all_to_all | solution.py:523

commit v5 on v4

--- a/solution.py
+++ b/solution.py
@@ -13,8 +13,9 @@
 LANES = 128
 HALF = 8
 KIB = 1024
-MESSAGES = 512
-PART = 512
+MESSAGES = 768
+PART = 256
+EACH = 24
 RETURNED = 512
 epsilon = 1e-06
 NT = (((1,), (1,)), ((), ()))
@@ -44,19 +45,25 @@
     return first & right, second & right
 
 
-def quarter_of(device, core, slot):
-    return 4 * (2 * ((device >> 2) & 1) + (device & 1)) + 2 * core + slot
+def quarter_of(device):
+    return 4 * (2 * ((device >> 2) & 1) + (device & 1))
 
 
 def picks_of(routes):
-    core = lax.axis_index("tp") % 2
     shape = (ROWS, MESSAGES)
     row = lax.broadcasted_iota(jnp.int32, shape, 0)
     col = lax.broadcasted_iota(jnp.int32, shape, 1)
-    device, kind, q, slot = 31 - (col >> 4), (col >> 3) & 1, (col >> 1) & 3, col & 1
-    first, second = hits_of(routes, device, slot)
-    expert = (first | second) & (kind == 0)
-    dense = (row == quarter_of(device, core, slot)) & (kind == 1)
+    block = jnp.zeros(shape, jnp.int32)
+    for k in range(1, 32):
+        block = block + (col >= k * EACH).astype(jnp.int32)
+    inner = col - block * EACH
+    q = jnp.zeros(shape, jnp.int32)
+    for k in range(1, 4):
+        q = q + (inner >= k * 6).astype(jnp.int32)
+    place, device = inner - 6 * q, 31 - block
+    first, second = hits_of(routes, device, place)
+    expert = (first | second) & (place < 2)
+    dense = (row == quarter_of(device) + place - 2) & (place >= 2)
     pick = jnp.where(expert | dense, 1.0, 0.0)
     stacked = jnp.concatenate([jnp.where(q == k, pick, 0.0) for k in range(4)], axis=0)
     return stacked.astype(jnp.bfloat16)
@@ -233,12 +240,13 @@
     shape = (ROWS, RETURNED)
     row = lax.broadcasted_iota(jnp.int32, shape, 0)
     col = lax.broadcasted_iota(jnp.int32, shape, 1)
-    device, kind, slot, side = 31 - (col >> 4), (col >> 2) & 3, (col >> 1) & 1, col & 1
-    first, second = hits_of(route_ref[...], device, slot)
+    device, place, side = 31 - (col >> 4), (col >> 1) & 7, col & 1
+    first, second = hits_of(route_ref[...], device, place)
     one, two = columns_of(weight_ref[...])
     expert = jnp.where(first, one, jnp.where(second, two, 0.0))
-    dense = jnp.where(row == quarter_of(device, kind - 1, slot), branch_ref[:, 0:1], 0.0)
-    value = jnp.where(kind == 0, expert, jnp.where(kind == 3, 0.0, dense))
+    here = (row == quarter_of(device) + place - 2) & (place < 6)
+    dense = jnp.where(here, branch_ref[:, 0:1], 0.0)
+    value = jnp.where(place < 2, expert, dense)
     both = jnp.concatenate([jnp.where(side == h, value, 0.0) for h in range(2)], axis=0)
     mix_ref[...] = both.astype(jnp.bfloat16)
 
@@ -272,6 +280,10 @@
         normed.astype(jnp.float32) * gate_ref[...].astype(jnp.float32), axis=-1, keepdims=True
     )
     branch_ref[...] = jnp.broadcast_to(1.0 / (1.0 + jnp.exp(-logit)), branch_ref.shape)
+    lower = lax.axis_index("tp") % 2 == 0
+    normed = jnp.where(
+        lower, normed[:, : WIDTH // 2].astype(jnp.float32), normed[:, WIDTH // 2 :].astype(jnp.float32)
+    ).astype(jnp.bfloat16)
     stacked = jnp.concatenate([normed[:, q * PART : (q + 1) * PART] for q in range(4)], axis=0)
     send_ref[...] = lax.dot_general(
         pick_ref[...], stacked, (((0,), (0,)), ((), ())), preferred_element_type=jnp.float32
@@ -321,34 +333,40 @@
     )(*in_hbm(gate, up))
 
 
-def feed_kernel(got_ref, eg_ref, eu_ref, ed_hbm, *rest):
-    packs = rest[:8]
-    keep_ref, send_ref, wide_v, ed_v, dg_v, du_v, dd_v, e_sem, d_sem = rest[8:]
+def feed_kernel(got_ref, other_ref, eg_ref, eu_ref, ed_hbm, *rest):
+    packs = rest[:4]
+    keep_ref, send_ref, wide_v, ed_v, both_v, dd_v, e_sem, d_sem = rest[4:]
     lower = lax.axis_index("tp") % 2 == 0
     copy_e = pltpu.make_async_copy(ed_hbm, ed_v, e_sem)
+    targets = ((both_v, 0), (both_v, 128), (dd_v, 0))
     dense_copies = [
-        pltpu.make_async_copy(pack.at[k], dst.at[pl.ds(32 * i, 32), :], d_sem.at[8 * k + i])
-        for k, dst in enumerate((dg_v, du_v, dd_v))
+        pltpu.make_async_copy(
+            pack.at[k], dst.at[pl.ds(at + 32 * i, 32), :], d_sem.at[4 * k + i]
+        )
+        for k, (dst, at) in enumerate(targets)
         for i, pack in enumerate(packs)
     ]
     for copy in [copy_e] + dense_copies:
         copy.start()
-    for l in range(4):
-        wide_v[l] = got_ref[:, l * LANES : (l + 1) * LANES].astype(jnp.float32)
-
-    def unpacked(kind):
+    for l in range(2):
+        mine = got_ref[:, l * LANES : (l + 1) * LANES].astype(jnp.float32)
+        theirs = other_ref[:, l * LANES : (l + 1) * LANES].astype(jnp.float32)
+        wide_v[l] = jnp.where(lower, mine, theirs)
+        wide_v[2 + l] = jnp.where(lower, theirs, mine)
+
+    def unpacked(places):
         parts = [
             jnp.concatenate(
-                [wide_v[l, pl.ds(kind * 8 + q * 2 + slot, 32, stride=16), :] for slot in range(2)],
-                axis=0,
+                [wide_v[2 * s + l, pl.ds(q * 6 + j, 32, stride=EACH), :] for j in places], axis=0
             )
+            for s in range(2)
             for q in range(4)
-            for l in range(4)
+            for l in range(2)
         ]
         return jnp.concatenate(parts, axis=1).astype(jnp.bfloat16)
 
-    def packed(kind, value):
-        here = slice(kind * 64, kind * 64 + 64)
+    def packed(first, value):
+        here = slice(first, first + value.shape[0])
         for y in range(4):
             even = value[:, 512 * y : 512 * y + 256]
             odd = value[:, 512 * y + 256 : 512 * y + 512]
@@ -356,8 +374,8 @@
             keep_ref[here, there] = jnp.where(lower, even, odd)
             send_ref[here, there] = jnp.where(lower, odd, even).astype(jnp.bfloat16)
 
-    rows = unpacked(0)
-    dense_rows = unpacked(1)
+    rows = unpacked((0, 1))
+    dense_rows = unpacked((2, 3, 4, 5))
     a = jnp.dot(rows, eg_ref[...], preferred_element_type=jnp.float32)
     b = jnp.dot(rows, eu_ref[...], preferred_element_type=jnp.float32)
     hidden = (a / (1.0 + jnp.exp(-a)) * b).astype(jnp.bfloat16)
@@ -365,50 +383,43 @@
     packed(0, jnp.dot(hidden, ed_v[...], preferred_element_type=jnp.float32))
     for copy in dense_copies[:8]:
         copy.wait()
-    a = lax.dot_general(dense_rows, dg_v[...], NT, preferred_element_type=jnp.float32)
-    for copy in dense_copies[8:16]:
+    both = lax.dot_general(dense_rows, both_v[...], NT, preferred_element_type=jnp.float32)
+    a, b = both[:, :128], both[:, 128:]
+    hidden = (a / (1.0 + jnp.exp(-a)) * b).astype(jnp.bfloat16)
+    for copy in dense_copies[8:]:
         copy.wait()
-    b = lax.dot_general(dense_rows, du_v[...], NT, preferred_element_type=jnp.float32)
-    hidden = (a / (1.0 + jnp.exp(-a)) * b).astype(jnp.bfloat16)
-    for copy in dense_copies[16:]:
-        copy.wait()
-    packed(1, jnp.dot(hidden, dd_v[...], preferred_element_type=jnp.float32))
-
-
-def feed(got, gate, up, down, packs):
+    packed(64, jnp.dot(hidden, dd_v[...], preferred_element_type=jnp.float32))
+
+
+def feed(got, other, gate, up, down, packs):
     return pl.pallas_call(
         feed_kernel,
         out_shape=(
-            jax.ShapeDtypeStruct((128, 1024), jnp.float32),
-            jax.ShapeDtypeStruct((128, 1024), jnp.bfloat16),
-        ),
-        in_specs=[VMEM] * 3 + [HBM] * 9,
+            jax.ShapeDtypeStruct((192, 1024), jnp.float32),
+            jax.ShapeDtypeStruct((192, 1024), jnp.bfloat16),
+        ),
+        in_specs=[VMEM] * 4 + [HBM] * 5,
         out_specs=(VMEM, VMEM),
         scratch_shapes=[
             pltpu.VMEM((4, MESSAGES, LANES), jnp.float32),
             pltpu.VMEM((256, WIDTH), jnp.bfloat16),
             pltpu.VMEM((256, WIDTH), jnp.bfloat16),
-            pltpu.VMEM((256, WIDTH), jnp.bfloat16),
-            pltpu.VMEM((256, WIDTH), jnp.bfloat16),
+            pltpu.VMEM((128, WIDTH), jnp.bfloat16),
             pltpu.SemaphoreType.DMA,
-            pltpu.SemaphoreType.DMA((24,)),
+            pltpu.SemaphoreType.DMA((12,)),
         ],
         compiler_params=pltpu.CompilerParams(vmem_limit_bytes=24576 * KIB),
         cost_estimate=pl.CostEstimate(
             flops=1_000_000_000, bytes_accessed=7_000_000, transcendentals=40_000
         ),
-    )(got, gate, up, *in_hbm(down, *packs))
+    )(got, other, gate, up, *in_hbm(down), *packs)
 
 
 def halve_kernel(keep_ref, got_ref, out_ref, one_ref, two_ref, three_ref, sum_v):
-    lower = lax.axis_index("tp") % 2 == 0
     y = lax.axis_index("tp") // 2
     for k in range(4):
         there = slice(256 * k, 256 * k + 256)
-        own, other = keep_ref[64:, there], got_ref[64:, there].astype(jnp.float32)
-        sum_v[k, :64] = keep_ref[:64, there] + got_ref[:64, there].astype(jnp.float32)
-        sum_v[k, 64:128] = jnp.where(lower, own, other)
-        sum_v[k, 128:] = jnp.where(lower, other, own)
+        sum_v[k] = keep_ref[:, there] + got_ref[:, there].astype(jnp.float32)
     out_ref[...] = sum_v[y]
     for step, ref in ((1, one_ref), (2, two_ref), (3, three_ref)):
         ref[...] = sum_v[(y + step) % 4].astype(jnp.bfloat16)
@@ -432,15 +443,13 @@
 def pack_kernel(a_ref, b_ref, c_ref, d_ref, out_ref, back_v):
     total = a_ref[...] + b_ref[...].astype(jnp.float32)
     total = total + (c_ref[...].astype(jnp.float32) + d_ref[...].astype(jnp.float32))
-    for kind in range(4):
-        for slot in range(2):
-            for h in range(2):
-                at = kind * 64 + slot * 32
-                if kind < 3:
-                    piece = total[at : at + 32, h * LANES : (h + 1) * LANES]
-                else:
-                    piece = jnp.zeros((32, LANES), jnp.float32)
-                back_v[pl.ds(kind * 4 + slot * 2 + h, 32, stride=16), :] = piece
+    for place in range(8):
+        for h in range(2):
+            if place < 6:
+                piece = total[place * 32 : place * 32 + 32, h * LANES : (h + 1) * LANES]
+            else:
+                piece = jnp.zeros((32, LANES), jnp.float32)
+            back_v[pl.ds(place * 2 + h, 32, stride=16), :] = piece
     out_ref[...] = back_v[...].astype(jnp.bfloat16)
 
 
@@ -505,15 +514,15 @@
     packs.append(lax.ppermute(packs[1], "ep", square))
     send, residual, branch = dispatch(shares, tokens, ffn_gain, branch_gate, picks)
     got = lax.all_to_all(
-        send.reshape(32, 16, PART), "ep", 0, 0, tiled=True,
+        send.reshape(32, EACH, PART), "ep", 0, 0, tiled=True,
         axis_index_groups=[list(range(31, -1, -1))],
     )
 
-    for k in range(4):
-        packs.append(lax.ppermute(packs[k], "tp", swap))
     mix = mix_table(route_expert, route_weight, branch)
     gate, up = warm(w_exp_gate[0], w_exp_up[0])
-    keep, give = feed(got.reshape(MESSAGES, PART), gate, up, w_exp_down[0], packs)
+    got = got.reshape(MESSAGES, PART)
+    other = lax.ppermute(got, "tp", swap)
+    keep, give = feed(got, other, gate, up, w_exp_down[0], packs)
     taken = lax.ppermute(give, "tp", swap)
     mine, *others = halve(keep, taken)
     blocks = [mine]

time: 90.7 us -> 90.3 us (level)
  waiting for transfers between devices: 31.2 us -> 38.8 us
  starting transfers between devices: 39.7 us -> 35 us
  local copies, waits for them, and re-layouts: 1.55 us -> 0.04 us
    ppermute x1, waiting for transfers between devices: 0.01 us -> 15.8 us  [layer(): packs = [own, lax.ppermute(own, 'ep', [(i, i ^ 4) for i in range(32)])]]
    ppermute x1, waiting for transfers between devices: 10.2 us -> 0.01 us  [layer(): packs.append(lax.ppermute(own, 'ep', square))]
    ppermute x4 -> x1, starting transfers between devices: 8.4 us -> 2.28 us  [layer(): other = lax.ppermute(got, 'tp', swap)]
    ppermute x6, waiting for transfers between devices: 8.33 us -> 11.4 us  [along_y(): return lax.ppermute(x, 'tp', [(i, (i + 2 * step) % 8) for i in range(8)])]
    ppermute x1, starting transfers between devices: 0.28 us -> 2.99 us  [layer(): taken = lax.ppermute(give, 'tp', swap)]
    unnamed x26 -> x16, local copies, waits for them, and re-layouts: 1.54 us -> 0.04 us
    ppermute x6, starting transfers between devices: 6.75 us -> 5.29 us  [along_y(): return lax.ppermute(x, 'tp', [(i, (i + 2 * step) % 8) for i in range(8)])]
    ppermute x1, starting transfers between devices: 0.09 us -> 1.24 us  [layer(): packs = [own, lax.ppermute(own, 'ep', [(i, i ^ 4) for i in range(32)])]]
  transfers between devices with their start and end apart: 17 -> 14, of which waited for: 9 -> 11; matrix products, arithmetic and copies ran while one was open for 0% -> 0% of each run, Pallas kernels for 3% -> 2%
where the time goes in v5:
time: 90.3 us; the launch traced here: 89.5 us
  waiting for transfers between devices  38.8 us (43%)
  starting transfers between devices  35 us (39%)
  Pallas kernels  15.4 us (17%)
    ppermute x1, waiting for transfers between devices, layer(): packs = [own, lax.ppermute(own, 'ep', [(i, i ^ 4) for i in range(32)])]  15.8 us
    ppermute x6, waiting for transfers between devices, along_y(): return lax.ppermute(x, 'tp', [(i, (i + 2 * step) % 8) for i in range(8)])  11.4 us
    all_to_all x1, starting transfers between devices, layer(): lax.all_to_all(send.reshape(32, EACH, PART), 'ep', 0, 0, tiled=True, axis...  10.2 us
    all_to_all x1, starting transfers between devices, layer(): lax.all_to_all(back.reshape(32, 16, LANES), 'ep', 0, 0, tiled=True, axis_...  8.52 us
    pallas_call x1, Pallas kernels, attention(): pl.pallas_call(attention_kernel, out_shape=(pltpu.VMEM((ROWS, WIDTH), jnp...  6.65 us
    ppermute x6, starting transfers between devices, along_y(): return lax.ppermute(x, 'tp', [(i, (i + 2 * step) % 8) for i in range(8)])  5.29 us
    all_to_all x1, waiting for transfers between devices, layer(): lax.all_to_all(back.reshape(32, 16, LANES), 'ep', 0, 0, tiled=True, axis_...  5.28 us
    pallas_call x1, Pallas kernels, feed(): pl.pallas_call(feed_kernel, out_shape=(jax.ShapeDtypeStruct((192, 1024),...  4.15 us
  transfers between devices with their start and end apart: 14, of which 11 were waited for; matrix products, arithmetic and copies ran while one was open for 0% of the time, Pallas kernels for 2%

profile of v5, /device:TPU:1, one launch (start us, length us, event | category | flops | bytes accessed | tf_op | source)
XLA Modules:
  0.0 89.5 jit_solution(3677353861963616865)
XLA Ops:
  0.0 6.7 %shard_map.172 = (bf16[16,2048]{1,0:T(8,128)(2,1)S(1)}, bf16[64,768]{1,0:T(8,128)(2,1)S(1)}) custom-call(s32[1,16]{1,0:T(1,128)} %bitcast.31, f32[1,2]{1,0:T(1,128)} %bitcast.32, bf16[16,2048]{1,0:T(8,128)(2,1)} %tok_ref.1, f32[1,2048]{1,0:T(1,128)} %bitcast.30, f32[1,128]{1,0:T(1,128)} %bitcast.33, s32[2,16]{1,0:T(2,128)} %bitcast.21, ...), custom_call_target="tpu_custom_call" | custom-call | flops 400000000 | bytes 6000000 | tf_op jit(solution)/shard_map/pallas_call | solution.py:203
  6.7 3.3 %collective-permute-start = (bf16[16,2048]{1,0:T(8,128)(2,1)S(1)}, bf16[16,2048]{1,0:T(8,128)(2,1)S(1)}, u32[]{:S(2)}, u32[]{:S(2)}) collective-permute-start(bf16[16,2048]{1,0:T(8,128)(2,1)S(1)} %get-tuple-element.18), channel_id=1, source_target_pairs={{0,1},{1,0},{2,3},{3,2},{4,5},{5,4},{6,7},{7,6},{8,9},{9,8},{10,11... | collective-permute-start | bytes 196616 | tf_op jit(solution)/shard_map/ppermute | solution.py:509
  10.0 0.9 %collective-permute-done = bf16[16,2048]{1,0:T(8,128)(2,1)S(1)} collective-permute-done((bf16[16,2048]{1,0:T(8,128)(2,1)S(1)}, bf16[16,2048]{1,0:T(8,128)(2,1)S(1)}, u32[]{:S(2)}, u32[]{:S(2)}) %collective-permute-start) | collective-permute-done | bytes 65568 | tf_op jit(solution)/shard_map/ppermute | solution.py:509
  10.9 0.1 collective-permute-start.1
  11.0 2.7 %collective-permute-start.2 = (bf16[16,2048]{1,0:T(8,128)(2,1)S(1)}, bf16[16,2048]{1,0:T(8,128)(2,1)S(1)}, u32[]{:S(2)}, u32[]{:S(2)}) collective-permute-start(bf16[16,2048]{1,0:T(8,128)(2,1)S(1)} %add_convert_fusion.a_ref), channel_id=1, source_target_pairs={{0,6},{1,7},{2,0},{3,1},{4,2},{5,3},{6,4},{7,5},{8,14},{9,15},{10,... | collective-permute-start | bytes 196616 | tf_op jit(solution)/shard_map/ppermute | solution.py:490
  13.7 0.0 collective-permute-start.3
  13.7 1.6 %collective-permute-done.1.b_ref = bf16[16,2048]{1,0:T(8,128)(2,1)S(1)} collective-permute-done((bf16[16,2048]{1,0:T(8,128)(2,1)S(1)}, bf16[16,2048]{1,0:T(8,128)(2,1)S(1)}, u32[]{:S(2)}, u32[]{:S(2)}) %collective-permute-start.1) | collective-permute-done | bytes 65568 | tf_op jit(solution)/shard_map/ppermute | solution.py:490
  15.3 0.4 collective-permute-done.2.c_ref
  15.7 2.5 %collective-permute-done.3.d_ref = bf16[16,2048]{1,0:T(8,128)(2,1)S(1)} collective-permute-done((bf16[16,2048]{1,0:T(8,128)(2,1)S(1)}, bf16[16,2048]{1,0:T(8,128)(2,1)S(1)}, u32[]{:S(2)}, u32[]{:S(2)}) %collective-permute-start.3) | collective-permute-done | bytes 65568 | tf_op jit(solution)/shard_map/ppermute | solution.py:490
  18.3 1.2 %shard_map.173 = (bf16[768,256]{1,0:T(8,128)(2,1)}, f32[16,256]{1,0:T(8,128)S(1)}, f32[16,128]{1,0:T(8,128)S(1)}) custom-call(bf16[16,2048]{1,0:T(8,128)(2,1)S(1)} %add_convert_fusion.a_ref, bf16[16,2048]{1,0:T(8,128)(2,1)S(1)} %collective-permute-done.1.b_ref, bf16[16,2048]{1,0:T(8,128)(2,1)S(1)} %collective-permute-done.2.c_ref, ...), custom_call_target="tpu_custom_call" | custom-call | flops 40000000 | bytes 1500000 | tf_op jit(solution)/shard_map/pallas_call | solution.py:294
  19.4 10.2 %all-to-all-start = ((bf16[32,24,256]{2,1,0:T(8,128)(2,1)}), bf16[32,24,256]{2,1,0:T(8,128)(2,1)S(1)}, u32[]{:S(2)}, u32[]{:S(2)}) async-start(bf16[32,24,256]{2,1,0:T(8,128)(2,1)} %bitcast.7), calls=%async_computation | async-start | bytes 786432 | tf_op jit(solution)/shard_map/all_to_all | solution.py:516
  29.7 1.2 %collective-permute-start.5 = (bf16[3,32,2048]{2,1,0:T(8,128)(2,1)S(1)}, bf16[3,32,2048]{2,1,0:T(8,128)(2,1)S(1)}, u32[]{:S(2)}, u32[]{:S(2)}) collective-permute-start(bf16[3,32,2048]{2,1,0:T(8,128)(2,1)S(1)} %pad_maximum_fusion.rest_0_), channel_id=1, source_target_pairs={{0,32},{8,40},{16,48},{24,56},{32,0},{40,8},{48,16},{56,24},{64,96... | collective-permute-start | bytes 1179656 | tf_op jit(solution)/shard_map/ppermute | solution.py:503
  31.0 0.6 collective-permute-start.6
  31.6 15.8 %collective-permute-done.5.rest_1_ = bf16[3,32,2048]{2,1,0:T(8,128)(2,1)S(1)} collective-permute-done((bf16[3,32,2048]{2,1,0:T(8,128)(2,1)S(1)}, bf16[3,32,2048]{2,1,0:T(8,128)(2,1)S(1)}, u32[]{:S(2)}, u32[]{:S(2)}) %collective-permute-start.5) | collective-permute-done | bytes 393248 | tf_op jit(solution)/shard_map/ppermute | solution.py:503
  47.3 0.6 collective-permute-start.7
  48.0 2.3 %collective-permute-start.4 = (bf16[768,256]{1,0:T(8,128)(2,1)S(1)}, bf16[768,256]{1,0:T(8,128)(2,1)S(1)}, u32[]{:S(2)}, u32[]{:S(2)}) collective-permute-start(bf16[768,256]{1,0:T(8,128)(2,1)S(1)} %bitcast.17), channel_id=1, source_target_pairs={{0,1},{1,0},{2,3},{3,2},{4,5},{5,4},{6,7},{7,6},{8,9},{9,8},{10,11... | collective-permute-start | bytes 1179656 | tf_op jit(solution)/shard_map/ppermute | solution.py:524
  50.3 1.6 %shard_map.175 = (bf16[2048,256]{1,0:T(8,128)(2,1)S(1)}, bf16[2048,256]{1,0:T(8,128)(2,1)S(1)}) custom-call(bf16[2048,256]{1,0:T(8,128)(2,1)} %bitcast.24, bf16[2048,256]{1,0:T(8,128)(2,1)} %bitcast.25), custom_call_target="tpu_custom_call" | custom-call | flops 1000000 | bytes 4000000 | tf_op jit(solution)/shard_map/pallas_call | solution.py:323
  51.9 4.1 %collective-permute-done.7.rest_3_ = bf16[3,32,2048]{2,1,0:T(8,128)(2,1)S(1)} collective-permute-done((bf16[3,32,2048]{2,1,0:T(8,128)(2,1)S(1)}, bf16[3,32,2048]{2,1,0:T(8,128)(2,1)S(1)}, u32[]{:S(2)}, u32[]{:S(2)}) %collective-permute-start.7) | collective-permute-done | bytes 393248 | tf_op jit(solution)/shard_map/ppermute | solution.py:514
  56.0 4.2 %shard_map.176 = (f32[192,1024]{1,0:T(8,128)S(1)}, bf16[192,1024]{1,0:T(8,128)(2,1)S(1)}) custom-call(bf16[768,256]{1,0:T(8,128)(2,1)S(1)} %bitcast.18, bf16[768,256]{1,0:T(8,128)(2,1)S(1)} %collective-permute-done.4.other_ref, bf16[2048,256]{1,0:T(8,128)(2,1)S(1)} %get-tuple-element.22.eg_ref, bf16[2048,256]{1,0:T(8,128)(2,1)S(1)} %get-tuple-element.23.eu_ref, ...), custom_call_target="tpu_custom_call" | custom-call | flops 1000000000 | bytes 7000000 | tf_op jit(solution)/shard_map/pallas_call | solution.py:395
  60.1 3.0 %collective-permute-start.8 = (bf16[192,1024]{1,0:T(8,128)(2,1)S(1)}, bf16[192,1024]{1,0:T(8,128)(2,1)S(1)}, u32[]{:S(2)}, u32[]{:S(2)}) collective-permute-start(bf16[192,1024]{1,0:T(8,128)(2,1)S(1)} %get-tuple-element.25), channel_id=1, source_target_pairs={{0,1},{1,0},{2,3},{3,2},{4,5},{5,4},{6,7},{7,6},{8,9},{9,8},{10,11... | collective-permute-start | bytes 1179656 | tf_op jit(solution)/shard_map/ppermute | solution.py:526
  63.1 1.3 %collective-permute-done.8.got_ref = bf16[192,1024]{1,0:T(8,128)(2,1)S(1)} collective-permute-done((bf16[192,1024]{1,0:T(8,128)(2,1)S(1)}, bf16[192,1024]{1,0:T(8,128)(2,1)S(1)}, u32[]{:S(2)}, u32[]{:S(2)}) %collective-permute-start.8) | collective-permute-done | bytes 393248 | tf_op jit(solution)/shard_map/ppermute | solution.py:526
  64.5 0.1 shard_map.177
  64.6 1.5 %collective-permute-start.10 = (bf16[192,256]{1,0:T(8,128)(2,1)S(1)}, bf16[192,256]{1,0:T(8,128)(2,1)S(1)}, u32[]{:S(2)}, u32[]{:S(2)}) collective-permute-start(bf16[192,256]{1,0:T(8,128)(2,1)S(1)} %get-tuple-element.28), channel_id=1, source_target_pairs={{0,6},{1,7},{2,0},{3,1},{4,2},{5,3},{6,4},{7,5},{8,14},{9,15},{10,... | collective-permute-start | bytes 294920 | tf_op jit(solution)/shard_map/ppermute | solution.py:490
  66.1 1.1 %collective-permute-start.11 = (bf16[192,256]{1,0:T(8,128)(2,1)S(1)}, bf16[192,256]{1,0:T(8,128)(2,1)S(1)}, u32[]{:S(2)}, u32[]{:S(2)}) collective-permute-start(bf16[192,256]{1,0:T(8,128)(2,1)S(1)} %get-tuple-element.29), channel_id=1, source_target_pairs={{0,4},{1,5},{2,6},{3,7},{4,0},{5,1},{6,2},{7,3},{8,12},{9,13},{10,... | collective-permute-start | bytes 294920 | tf_op jit(solution)/shard_map/ppermute | solution.py:490
  67.1 1.5 %collective-permute-done.10.c_ref = bf16[192,256]{1,0:T(8,128)(2,1)S(1)} collective-permute-done((bf16[192,256]{1,0:T(8,128)(2,1)S(1)}, bf16[192,256]{1,0:T(8,128)(2,1)S(1)}, u32[]{:S(2)}, u32[]{:S(2)}) %collective-permute-start.10) | collective-permute-done | bytes 98336 | tf_op jit(solution)/shard_map/ppermute | solution.py:490
  68.7 2.4 %collective-permute-done.11.d_ref = bf16[192,256]{1,0:T(8,128)(2,1)S(1)} collective-permute-done((bf16[192,256]{1,0:T(8,128)(2,1)S(1)}, bf16[192,256]{1,0:T(8,128)(2,1)S(1)}, u32[]{:S(2)}, u32[]{:S(2)}) %collective-permute-start.11) | collective-permute-done | bytes 98336 | tf_op jit(solution)/shard_map/ppermute | solution.py:490
  71.1 2.8 %collective-permute-done.9.b_ref = bf16[192,256]{1,0:T(8,128)(2,1)S(1)} collective-permute-done((bf16[192,256]{1,0:T(8,128)(2,1)S(1)}, bf16[192,256]{1,0:T(8,128)(2,1)S(1)}, u32[]{:S(2)}, u32[]{:S(2)}) %collective-permute-start.9) | collective-permute-done | bytes 98336 | tf_op jit(solution)/shard_map/ppermute | solution.py:490
  73.9 0.8 shard_map.178
  74.7 8.5 %all-to-all-start.1 = ((bf16[32,16,128]{2,1,0:T(8,128)(2,1)}), bf16[32,16,128]{2,1,0:T(8,128)(2,1)S(1)}, u32[]{:S(2)}, u32[]{:S(2)}) async-start(bf16[32,16,128]{2,1,0:T(8,128)(2,1)} %bitcast.15), calls=%async_computation.1 | async-start | bytes 262144 | tf_op jit(solution)/shard_map/all_to_all | solution.py:532
  83.3 0.2 shard_map.174.mix_ref
  83.5 5.3 %all-to-all-done.1 = bf16[32,16,128]{2,1,0:T(8,128)(2,1)S(1)} async-done(((bf16[32,16,128]{2,1,0:T(8,128)(2,1)}), bf16[32,16,128]{2,1,0:T(8,128)(2,1)S(1)}, u32[]{:S(2)}, u32[]{:S(2)}) %all-to-all-start.1) | async-done | bytes 131104 | tf_op jit(solution)/shard_map/all_to_all | solution.py:532
  88.8 0.7 shard_map.179
  (23 shorter events, 0.1 us)
Async XLA Ops:
  0.0 18.3 %copy-start = (bf16[16,2048]{1,0:T(8,128)(2,1)S(1)}, bf16[16,2048]{1,0:T(8,128)(2,1)}, u32[]{:S(2)}) copy-start(bf16[16,2048]{1,0:T(8,128)(2,1)} %tok_ref.1) | copy-start | bytes 196612
  0.0 13.7 %copy-start.7 = (bf16[2048]{0:T(1024)(128)(2,1)S(1)}, bf16[2048]{0:T(1024)(128)(2,1)}, u32[]{:S(2)}) copy-start(bf16[2048]{0:T(1024)(128)(2,1)} %param.32) | copy-start | bytes 12292
  0.0 18.3 %copy-start.1 = (f32[2048]{0:T(1024)S(1)}, f32[2048]{0:T(1024)}, u32[]{:S(2)}) copy-start(f32[2048]{0:T(1024)} %param.26) | copy-start | bytes 24580
  0.0 29.7 %copy-start.6 = (bf16[32,2048]{1,0:T(8,128)(2,1)S(1)}, bf16[32,2048]{1,0:T(8,128)(2,1)}, u32[]{:S(2)}) copy-start(bf16[32,2048]{1,0:T(8,128)(2,1)} %param.33) | copy-start | bytes 393220
  0.0 29.7 %copy-start.5 = (bf16[32,2048]{1,0:T(8,128)(2,1)S(1)}, bf16[32,2048]{1,0:T(8,128)(2,1)}, u32[]{:S(2)}) copy-start(bf16[32,2048]{1,0:T(8,128)(2,1)} %param.34) | copy-start | bytes 393220
  0.0 29.7 %copy-start.4 = (bf16[32,2048]{1,0:T(8,128)(2,1)S(1)}, bf16[32,2048]{1,0:T(8,128)(2,1)}, u32[]{:S(2)}) copy-start(bf16[32,2048]{1,0:T(8,128)(2,1)} %param.35) | copy-start | bytes 393220
  6.7 4.2 %collective-permute-start = (bf16[16,2048]{1,0:T(8,128)(2,1)S(1)}, bf16[16,2048]{1,0:T(8,128)(2,1)S(1)}, u32[]{:S(2)}, u32[]{:S(2)}) collective-permute-start(bf16[16,2048]{1,0:T(8,128)(2,1)S(1)} %get-tuple-element.18), channel_id=1, source_target_pairs={{0,1},{1,0},{2,3},{3,2},{4,5},{5,4},{6,7},{7,6},{8,9},{9,8},{10,11... | collective-permute-start | bytes 196616 | tf_op jit(solution)/shard_map/ppermute | solution.py:509
  10.9 4.4 %collective-permute-start.1 = (bf16[16,2048]{1,0:T(8,128)(2,1)S(1)}, bf16[16,2048]{1,0:T(8,128)(2,1)S(1)}, u32[]{:S(2)}, u32[]{:S(2)}) collective-permute-start(bf16[16,2048]{1,0:T(8,128)(2,1)S(1)} %add_convert_fusion.a_ref), channel_id=1, source_target_pairs={{0,2},{1,3},{2,4},{3,5},{4,6},{5,7},{6,0},{7,1},{8,10},{9,11},{10,... | collective-permute-start | bytes 196616 | tf_op jit(solution)/shard_map/ppermute | solution.py:490
  11.0 4.7 %collective-permute-start.2 = (bf16[16,2048]{1,0:T(8,128)(2,1)S(1)}, bf16[16,2048]{1,0:T(8,128)(2,1)S(1)}, u32[]{:S(2)}, u32[]{:S(2)}) collective-permute-start(bf16[16,2048]{1,0:T(8,128)(2,1)S(1)} %add_convert_fusion.a_ref), channel_id=1, source_target_pairs={{0,6},{1,7},{2,0},{3,1},{4,2},{5,3},{6,4},{7,5},{8,14},{9,15},{10,... | collective-permute-start | bytes 196616 | tf_op jit(solution)/shard_map/ppermute | solution.py:490
  13.7 4.6 %collective-permute-start.3 = (bf16[16,2048]{1,0:T(8,128)(2,1)S(1)}, bf16[16,2048]{1,0:T(8,128)(2,1)S(1)}, u32[]{:S(2)}, u32[]{:S(2)}) collective-permute-start(bf16[16,2048]{1,0:T(8,128)(2,1)S(1)} %add_convert_fusion.a_ref), channel_id=1, source_target_pairs={{0,4},{1,5},{2,6},{3,7},{4,0},{5,1},{6,2},{7,3},{8,12},{9,13},{10,... | collective-permute-start | bytes 196616 | tf_op jit(solution)/shard_map/ppermute | solution.py:490
  19.4 28.5 %all-to-all-start = ((bf16[32,24,256]{2,1,0:T(8,128)(2,1)}), bf16[32,24,256]{2,1,0:T(8,128)(2,1)S(1)}, u32[]{:S(2)}, u32[]{:S(2)}) async-start(bf16[32,24,256]{2,1,0:T(8,128)(2,1)} %bitcast.7), calls=%async_computation | async-start | bytes 786432 | tf_op jit(solution)/shard_map/all_to_all | solution.py:516
  29.7 17.6 %collective-permute-start.5 = (bf16[3,32,2048]{2,1,0:T(8,128)(2,1)S(1)}, bf16[3,32,2048]{2,1,0:T(8,128)(2,1)S(1)}, u32[]{:S(2)}, u32[]{:S(2)}) collective-permute-start(bf16[3,32,2048]{2,1,0:T(8,128)(2,1)S(1)} %pad_maximum_fusion.rest_0_), channel_id=1, source_target_pairs={{0,32},{8,40},{16,48},{24,56},{32,0},{40,8},{48,16},{56,24},{64,96... | collective-permute-start | bytes 1179656 | tf_op jit(solution)/shard_map/ppermute | solution.py:503
  31.0 20.9 %collective-permute-start.6 = (bf16[3,32,2048]{2,1,0:T(8,128)(2,1)S(1)}, bf16[3,32,2048]{2,1,0:T(8,128)(2,1)S(1)}, u32[]{:S(2)}, u32[]{:S(2)}) collective-permute-start(bf16[3,32,2048]{2,1,0:T(8,128)(2,1)S(1)} %pad_maximum_fusion.rest_0_), channel_id=1, source_target_pairs={{0,8},{8,0},{16,24},{24,16},{32,40},{40,32},{48,56},{56,48},{64,72... | collective-permute-start | bytes 1179656 | tf_op jit(solution)/shard_map/ppermute | solution.py:504
  47.3 8.6 %collective-permute-start.7 = (bf16[3,32,2048]{2,1,0:T(8,128)(2,1)S(1)}, bf16[3,32,2048]{2,1,0:T(8,128)(2,1)S(1)}, u32[]{:S(2)}, u32[]{:S(2)}) collective-permute-start(bf16[3,32,2048]{2,1,0:T(8,128)(2,1)S(1)} %collective-permute-done.5.rest_1_), channel_id=1, source_target_pairs={{0,8},{8,0},{16,24},{24,16},{32,40},{40,32},{48,56},{56,48},{64,72... | collective-permute-start | bytes 1179656 | tf_op jit(solution)/shard_map/ppermute | solution.py:514
  48.0 8.0 %collective-permute-start.4 = (bf16[768,256]{1,0:T(8,128)(2,1)S(1)}, bf16[768,256]{1,0:T(8,128)(2,1)S(1)}, u32[]{:S(2)}, u32[]{:S(2)}) collective-permute-start(bf16[768,256]{1,0:T(8,128)(2,1)S(1)} %bitcast.17), channel_id=1, source_target_pairs={{0,1},{1,0},{2,3},{3,2},{4,5},{5,4},{6,7},{7,6},{8,9},{9,8},{10,11... | collective-permute-start | bytes 1179656 | tf_op jit(solution)/shard_map/ppermute | solution.py:524
  51.8 31.4 %copy-start.2 = (s32[16,2]{0,1:T(2,128)S(1)}, s32[16,2]{0,1:T(2,128)}, u32[]{:S(2)}) copy-start(s32[16,2]{0,1:T(2,128)} %param.27) | copy-start | bytes 388
  51.8 31.4 %copy-start.3 = (bf16[16,2]{0,1:T(2,128)(2,1)S(1)}, bf16[16,2]{0,1:T(2,128)(2,1)}, u32[]{:S(2)}) copy-start(bf16[16,2]{0,1:T(2,128)(2,1)} %param.28) | copy-start | bytes 196
  60.1 4.3 %collective-permute-start.8 = (bf16[192,1024]{1,0:T(8,128)(2,1)S(1)}, bf16[192,1024]{1,0:T(8,128)(2,1)S(1)}, u32[]{:S(2)}, u32[]{:S(2)}) collective-permute-start(bf16[192,1024]{1,0:T(8,128)(2,1)S(1)} %get-tuple-element.25), channel_id=1, source_target_pairs={{0,1},{1,0},{2,3},{3,2},{4,5},{5,4},{6,7},{7,6},{8,9},{9,8},{10,11... | collective-permute-start | bytes 1179656 | tf_op jit(solution)/shard_map/ppermute | solution.py:526
  64.6 4.1 %collective-permute-start.10 = (bf16[192,256]{1,0:T(8,128)(2,1)S(1)}, bf16[192,256]{1,0:T(8,128)(2,1)S(1)}, u32[]{:S(2)}, u32[]{:S(2)}) collective-permute-start(bf16[192,256]{1,0:T(8,128)(2,1)S(1)} %get-tuple-element.28), channel_id=1, source_target_pairs={{0,6},{1,7},{2,0},{3,1},{4,2},{5,3},{6,4},{7,5},{8,14},{9,15},{10,... | collective-permute-start | bytes 294920 | tf_op jit(solution)/shard_map/ppermute | solution.py:490
  66.1 5.0 %collective-permute-start.11 = (bf16[192,256]{1,0:T(8,128)(2,1)S(1)}, bf16[192,256]{1,0:T(8,128)(2,1)S(1)}, u32[]{:S(2)}, u32[]{:S(2)}) collective-permute-start(bf16[192,256]{1,0:T(8,128)(2,1)S(1)} %get-tuple-element.29), channel_id=1, source_target_pairs={{0,4},{1,5},{2,6},{3,7},{4,0},{5,1},{6,2},{7,3},{8,12},{9,13},{10,... | collective-permute-start | bytes 294920 | tf_op jit(solution)/shard_map/ppermute | solution.py:490
  67.1 6.8 %collective-permute-start.9 = (bf16[192,256]{1,0:T(8,128)(2,1)S(1)}, bf16[192,256]{1,0:T(8,128)(2,1)S(1)}, u32[]{:S(2)}, u32[]{:S(2)}) collective-permute-start(bf16[192,256]{1,0:T(8,128)(2,1)S(1)} %get-tuple-element.27), channel_id=1, source_target_pairs={{0,2},{1,3},{2,4},{3,5},{4,6},{5,7},{6,0},{7,1},{8,10},{9,11},{10,... | collective-permute-start | bytes 294920 | tf_op jit(solution)/shard_map/ppermute | solution.py:490
  74.7 14.1 %all-to-all-start.1 = ((bf16[32,16,128]{2,1,0:T(8,128)(2,1)}), bf16[32,16,128]{2,1,0:T(8,128)(2,1)S(1)}, u32[]{:S(2)}, u32[]{:S(2)}) async-start(bf16[32,16,128]{2,1,0:T(8,128)(2,1)} %bitcast.15), calls=%async_computation.1 | async-start | bytes 262144 | tf_op jit(solution)/shard_map/all_to_all | solution.py:532

commit v6 on v5

--- a/solution.py
+++ b/solution.py
@@ -308,10 +308,11 @@
     )(*shares, tokens, ffn_gain.reshape(1, -1), branch_gate.reshape(1, -1), picks)
 
 
-def warm_kernel(gate_hbm, up_hbm, gate_out, up_out, sems):
+def warm_kernel(gate_hbm, up_hbm, down_hbm, gate_out, up_out, down_out, sems):
     copies = [
         pltpu.make_async_copy(gate_hbm, gate_out, sems.at[0]),
         pltpu.make_async_copy(up_hbm, up_out, sems.at[1]),
+        pltpu.make_async_copy(down_hbm, down_out, sems.at[2]),
     ]
     for copy in copies:
         copy.start()
@@ -319,25 +320,25 @@
         copy.wait()
 
 
-def warm(gate, up):
+def warm(gate, up, down):
     return pl.pallas_call(
         warm_kernel,
-        out_shape=(pltpu.VMEM((WIDTH, 256), jnp.bfloat16),) * 2,
-        in_specs=[HBM] * 2,
-        out_specs=(VMEM, VMEM),
-        scratch_shapes=[pltpu.SemaphoreType.DMA((2,))],
+        out_shape=(pltpu.VMEM((WIDTH, 256), jnp.bfloat16),) * 2
+        + (pltpu.VMEM((256, WIDTH), jnp.bfloat16),),
+        in_specs=[HBM] * 3,
+        out_specs=(VMEM,) * 3,
+        scratch_shapes=[pltpu.SemaphoreType.DMA((3,))],
         compiler_params=pltpu.CompilerParams(vmem_limit_bytes=4096 * KIB),
         cost_estimate=pl.CostEstimate(
             flops=1_000_000, bytes_accessed=4_000_000, transcendentals=0
         ),
-    )(*in_hbm(gate, up))
-
-
-def feed_kernel(got_ref, other_ref, eg_ref, eu_ref, ed_hbm, *rest):
+    )(*in_hbm(gate, up, down))
+
+
+def feed_kernel(got_ref, other_ref, eg_ref, eu_ref, ed_ref, *rest):
     packs = rest[:4]
-    keep_ref, send_ref, wide_v, ed_v, both_v, dd_v, e_sem, d_sem = rest[4:]
+    keep_ref, send_ref, wide_v, both_v, dd_v, d_sem = rest[4:]
     lower = lax.axis_index("tp") % 2 == 0
-    copy_e = pltpu.make_async_copy(ed_hbm, ed_v, e_sem)
     targets = ((both_v, 0), (both_v, 128), (dd_v, 0))
     dense_copies = [
         pltpu.make_async_copy(
@@ -346,7 +347,7 @@
         for k, (dst, at) in enumerate(targets)
         for i, pack in enumerate(packs)
     ]
-    for copy in [copy_e] + dense_copies:
+    for copy in dense_copies:
         copy.start()
     for l in range(2):
         mine = got_ref[:, l * LANES : (l + 1) * LANES].astype(jnp.float32)
@@ -379,8 +380,7 @@
     a = jnp.dot(rows, eg_ref[...], preferred_element_type=jnp.float32)
     b = jnp.dot(rows, eu_ref[...], preferred_element_type=jnp.float32)
     hidden = (a / (1.0 + jnp.exp(-a)) * b).astype(jnp.bfloat16)
-    copy_e.wait()
-    packed(0, jnp.dot(hidden, ed_v[...], preferred_element_type=jnp.float32))
+    packed(0, jnp.dot(hidden, ed_ref[...], preferred_element_type=jnp.float32))
     for copy in dense_copies[:8]:
         copy.wait()
     both = lax.dot_general(dense_rows, both_v[...], NT, preferred_element_type=jnp.float32)
@@ -398,21 +398,19 @@
             jax.ShapeDtypeStruct((192, 1024), jnp.float32),
             jax.ShapeDtypeStruct((192, 1024), jnp.bfloat16),
         ),
-        in_specs=[VMEM] * 4 + [HBM] * 5,
+        in_specs=[VMEM] * 5 + [HBM] * 4,
         out_specs=(VMEM, VMEM),
         scratch_shapes=[
             pltpu.VMEM((4, MESSAGES, LANES), jnp.float32),
             pltpu.VMEM((256, WIDTH), jnp.bfloat16),
-            pltpu.VMEM((256, WIDTH), jnp.bfloat16),
             pltpu.VMEM((128, WIDTH), jnp.bfloat16),
-            pltpu.SemaphoreType.DMA,
             pltpu.SemaphoreType.DMA((12,)),
         ],
         compiler_params=pltpu.CompilerParams(vmem_limit_bytes=24576 * KIB),
         cost_estimate=pl.CostEstimate(
             flops=1_000_000_000, bytes_accessed=7_000_000, transcendentals=40_000
         ),
-    )(got, other, gate, up, *in_hbm(down), *packs)
+    )(got, other, gate, up, down, *packs)
 
 
 def halve_kernel(keep_ref, got_ref, out_ref, one_ref, two_ref, three_ref, sum_v):
@@ -519,10 +517,10 @@
     )
 
     mix = mix_table(route_expert, route_weight, branch)
-    gate, up = warm(w_exp_gate[0], w_exp_up[0])
+    gate, up, down = warm(w_exp_gate[0], w_exp_up[0], w_exp_down[0])
     got = got.reshape(MESSAGES, PART)
     other = lax.ppermute(got, "tp", swap)
-    keep, give = feed(got, other, gate, up, w_exp_down[0], packs)
+    keep, give = feed(got, other, gate, up, down, packs)
     taken = lax.ppermute(give, "tp", swap)
     mine, *others = halve(keep, taken)
     blocks = [mine]

time: 90.3 us -> 90.2 us (level)
  no operation moved by 1% of the time
where the time goes in v6:
time: 90.2 us; the launch traced here: 89.5 us
  waiting for transfers between devices  38.5 us (43%)
  starting transfers between devices  35 us (39%)
  Pallas kernels  15.7 us (17%)
    ppermute x1, waiting for transfers between devices, layer(): packs = [own, lax.ppermute(own, 'ep', [(i, i ^ 4) for i in range(32)])]  15.8 us
    ppermute x6, waiting for transfers between devices, along_y(): return lax.ppermute(x, 'tp', [(i, (i + 2 * step) % 8) for i in range(8)])  11.4 us
    all_to_all x1, starting transfers between devices, layer(): lax.all_to_all(send.reshape(32, EACH, PART), 'ep', 0, 0, tiled=True, axis...  10.2 us
    all_to_all x1, starting transfers between devices, layer(): lax.all_to_all(back.reshape(32, 16, LANES), 'ep', 0, 0, tiled=True, axis_...  8.52 us
    pallas_call x1, Pallas kernels, attention(): pl.pallas_call(attention_kernel, out_shape=(pltpu.VMEM((ROWS, WIDTH), jnp...  6.65 us
    ppermute x6, starting transfers between devices, along_y(): return lax.ppermute(x, 'tp', [(i, (i + 2 * step) % 8) for i in range(8)])  5.3 us
    all_to_all x1, waiting for transfers between devices, layer(): lax.all_to_all(back.reshape(32, 16, LANES), 'ep', 0, 0, tiled=True, axis_...  5.28 us
    pallas_call x1, Pallas kernels, feed(): pl.pallas_call(feed_kernel, out_shape=(jax.ShapeDtypeStruct((192, 1024),...  4.07 us
  transfers between devices with their start and end apart: 14, of which 11 were waited for; matrix products, arithmetic and copies ran while one was open for 0% of the time, Pallas kernels for 2%

profile of v6, /device:TPU:1, one launch (start us, length us, event | category | flops | bytes accessed | tf_op | source)
XLA Modules:
  0.0 89.5 jit_solution(11714835740816738269)
XLA Ops:
  0.0 6.7 %shard_map.172 = (bf16[16,2048]{1,0:T(8,128)(2,1)S(1)}, bf16[64,768]{1,0:T(8,128)(2,1)S(1)}) custom-call(s32[1,16]{1,0:T(1,128)} %bitcast.31, f32[1,2]{1,0:T(1,128)} %bitcast.32, bf16[16,2048]{1,0:T(8,128)(2,1)} %tok_ref.1, f32[1,2048]{1,0:T(1,128)} %bitcast.30, f32[1,128]{1,0:T(1,128)} %bitcast.33, s32[2,16]{1,0:T(2,128)} %bitcast.21, ...), custom_call_target="tpu_custom_call" | custom-call | flops 400000000 | bytes 6000000 | tf_op jit(solution)/shard_map/pallas_call | solution.py:203
  6.7 3.3 %collective-permute-start = (bf16[16,2048]{1,0:T(8,128)(2,1)S(1)}, bf16[16,2048]{1,0:T(8,128)(2,1)S(1)}, u32[]{:S(2)}, u32[]{:S(2)}) collective-permute-start(bf16[16,2048]{1,0:T(8,128)(2,1)S(1)} %get-tuple-element.19), channel_id=1, source_target_pairs={{0,1},{1,0},{2,3},{3,2},{4,5},{5,4},{6,7},{7,6},{8,9},{9,8},{10,11... | collective-permute-start | bytes 196616 | tf_op jit(solution)/shard_map/ppermute | solution.py:507
  10.0 0.9 %collective-permute-done = bf16[16,2048]{1,0:T(8,128)(2,1)S(1)} collective-permute-done((bf16[16,2048]{1,0:T(8,128)(2,1)S(1)}, bf16[16,2048]{1,0:T(8,128)(2,1)S(1)}, u32[]{:S(2)}, u32[]{:S(2)}) %collective-permute-start) | collective-permute-done | bytes 65568 | tf_op jit(solution)/shard_map/ppermute | solution.py:507
  10.9 0.1 collective-permute-start.1
  11.0 2.7 %collective-permute-start.2 = (bf16[16,2048]{1,0:T(8,128)(2,1)S(1)}, bf16[16,2048]{1,0:T(8,128)(2,1)S(1)}, u32[]{:S(2)}, u32[]{:S(2)}) collective-permute-start(bf16[16,2048]{1,0:T(8,128)(2,1)S(1)} %add_convert_fusion.a_ref), channel_id=1, source_target_pairs={{0,6},{1,7},{2,0},{3,1},{4,2},{5,3},{6,4},{7,5},{8,14},{9,15},{10,... | collective-permute-start | bytes 196616 | tf_op jit(solution)/shard_map/ppermute | solution.py:488
  13.7 0.0 collective-permute-start.3
  13.7 1.6 %collective-permute-done.1.b_ref = bf16[16,2048]{1,0:T(8,128)(2,1)S(1)} collective-permute-done((bf16[16,2048]{1,0:T(8,128)(2,1)S(1)}, bf16[16,2048]{1,0:T(8,128)(2,1)S(1)}, u32[]{:S(2)}, u32[]{:S(2)}) %collective-permute-start.1) | collective-permute-done | bytes 65568 | tf_op jit(solution)/shard_map/ppermute | solution.py:488
  15.3 0.4 collective-permute-done.2.c_ref
  15.7 2.5 %collective-permute-done.3.d_ref = bf16[16,2048]{1,0:T(8,128)(2,1)S(1)} collective-permute-done((bf16[16,2048]{1,0:T(8,128)(2,1)S(1)}, bf16[16,2048]{1,0:T(8,128)(2,1)S(1)}, u32[]{:S(2)}, u32[]{:S(2)}) %collective-permute-start.3) | collective-permute-done | bytes 65568 | tf_op jit(solution)/shard_map/ppermute | solution.py:488
  18.3 1.2 %shard_map.173 = (bf16[768,256]{1,0:T(8,128)(2,1)}, f32[16,256]{1,0:T(8,128)S(1)}, f32[16,128]{1,0:T(8,128)S(1)}) custom-call(bf16[16,2048]{1,0:T(8,128)(2,1)S(1)} %add_convert_fusion.a_ref, bf16[16,2048]{1,0:T(8,128)(2,1)S(1)} %collective-permute-done.1.b_ref, bf16[16,2048]{1,0:T(8,128)(2,1)S(1)} %collective-permute-done.2.c_ref, ...), custom_call_target="tpu_custom_call" | custom-call | flops 40000000 | bytes 1500000 | tf_op jit(solution)/shard_map/pallas_call | solution.py:294
  19.4 10.2 %all-to-all-start = ((bf16[32,24,256]{2,1,0:T(8,128)(2,1)}), bf16[32,24,256]{2,1,0:T(8,128)(2,1)S(1)}, u32[]{:S(2)}, u32[]{:S(2)}) async-start(bf16[32,24,256]{2,1,0:T(8,128)(2,1)} %bitcast.7), calls=%async_computation | async-start | bytes 786432 | tf_op jit(solution)/shard_map/all_to_all | solution.py:514
  29.7 1.2 %collective-permute-start.5 = (bf16[3,32,2048]{2,1,0:T(8,128)(2,1)S(1)}, bf16[3,32,2048]{2,1,0:T(8,128)(2,1)S(1)}, u32[]{:S(2)}, u32[]{:S(2)}) collective-permute-start(bf16[3,32,2048]{2,1,0:T(8,128)(2,1)S(1)} %pad_maximum_fusion.rest_0_), channel_id=1, source_target_pairs={{0,32},{8,40},{16,48},{24,56},{32,0},{40,8},{48,16},{56,24},{64,96... | collective-permute-start | bytes 1179656 | tf_op jit(solution)/shard_map/ppermute | solution.py:501
  31.0 0.6 collective-permute-start.6
  31.6 15.8 %collective-permute-done.5.rest_1_ = bf16[3,32,2048]{2,1,0:T(8,128)(2,1)S(1)} collective-permute-done((bf16[3,32,2048]{2,1,0:T(8,128)(2,1)S(1)}, bf16[3,32,2048]{2,1,0:T(8,128)(2,1)S(1)}, u32[]{:S(2)}, u32[]{:S(2)}) %collective-permute-start.5) | collective-permute-done | bytes 393248 | tf_op jit(solution)/shard_map/ppermute | solution.py:501
  47.3 0.6 collective-permute-start.7
  48.0 2.3 %collective-permute-start.4 = (bf16[768,256]{1,0:T(8,128)(2,1)S(1)}, bf16[768,256]{1,0:T(8,128)(2,1)S(1)}, u32[]{:S(2)}, u32[]{:S(2)}) collective-permute-start(bf16[768,256]{1,0:T(8,128)(2,1)S(1)} %bitcast.17), channel_id=1, source_target_pairs={{0,1},{1,0},{2,3},{3,2},{4,5},{5,4},{6,7},{7,6},{8,9},{9,8},{10,11... | collective-permute-start | bytes 1179656 | tf_op jit(solution)/shard_map/ppermute | solution.py:522
  50.3 1.9 %shard_map.175 = (bf16[2048,256]{1,0:T(8,128)(2,1)S(1)}, bf16[2048,256]{1,0:T(8,128)(2,1)S(1)}, bf16[256,2048]{1,0:T(8,128)(2,1)S(1)}) custom-call(bf16[2048,256]{1,0:T(8,128)(2,1)} %bitcast.24, bf16[2048,256]{1,0:T(8,128)(2,1)} %bitcast.25, bf16[256,2048]{1,0:T(8,128)(2,1)} %bitcast.26), custom_call_target="tpu_custom_call" | custom-call | flops 1000000 | bytes 4000000 | tf_op jit(solution)/shard_map/pallas_call | solution.py:324
  52.2 3.8 %collective-permute-done.7.rest_3_ = bf16[3,32,2048]{2,1,0:T(8,128)(2,1)S(1)} collective-permute-done((bf16[3,32,2048]{2,1,0:T(8,128)(2,1)S(1)}, bf16[3,32,2048]{2,1,0:T(8,128)(2,1)S(1)}, u32[]{:S(2)}, u32[]{:S(2)}) %collective-permute-start.7) | collective-permute-done | bytes 393248 | tf_op jit(solution)/shard_map/ppermute | solution.py:512
  56.0 4.1 %shard_map.176 = (f32[192,1024]{1,0:T(8,128)S(1)}, bf16[192,1024]{1,0:T(8,128)(2,1)S(1)}) custom-call(bf16[768,256]{1,0:T(8,128)(2,1)S(1)} %bitcast.18, bf16[768,256]{1,0:T(8,128)(2,1)S(1)} %collective-permute-done.4.other_ref, bf16[2048,256]{1,0:T(8,128)(2,1)S(1)} %get-tuple-element.23.eg_ref, bf16[2048,256]{1,0:T(8,128)(2,1)S(1)} %get-tuple-element.24.eu_ref, ...), custom_call_target="tpu_custom_call" | custom-call | flops 1000000000 | bytes 7000000 | tf_op jit(solution)/shard_map/pallas_call | solution.py:395
  60.1 3.0 %collective-permute-start.8 = (bf16[192,1024]{1,0:T(8,128)(2,1)S(1)}, bf16[192,1024]{1,0:T(8,128)(2,1)S(1)}, u32[]{:S(2)}, u32[]{:S(2)}) collective-permute-start(bf16[192,1024]{1,0:T(8,128)(2,1)S(1)} %get-tuple-element.27), channel_id=1, source_target_pairs={{0,1},{1,0},{2,3},{3,2},{4,5},{5,4},{6,7},{7,6},{8,9},{9,8},{10,11... | collective-permute-start | bytes 1179656 | tf_op jit(solution)/shard_map/ppermute | solution.py:524
  63.0 1.3 %collective-permute-done.8.got_ref = bf16[192,1024]{1,0:T(8,128)(2,1)S(1)} collective-permute-done((bf16[192,1024]{1,0:T(8,128)(2,1)S(1)}, bf16[192,1024]{1,0:T(8,128)(2,1)S(1)}, u32[]{:S(2)}, u32[]{:S(2)}) %collective-permute-start.8) | collective-permute-done | bytes 393248 | tf_op jit(solution)/shard_map/ppermute | solution.py:524
  64.4 0.1 shard_map.177
  64.5 1.5 %collective-permute-start.10 = (bf16[192,256]{1,0:T(8,128)(2,1)S(1)}, bf16[192,256]{1,0:T(8,128)(2,1)S(1)}, u32[]{:S(2)}, u32[]{:S(2)}) collective-permute-start(bf16[192,256]{1,0:T(8,128)(2,1)S(1)} %get-tuple-element.30), channel_id=1, source_target_pairs={{0,6},{1,7},{2,0},{3,1},{4,2},{5,3},{6,4},{7,5},{8,14},{9,15},{10,... | collective-permute-start | bytes 294920 | tf_op jit(solution)/shard_map/ppermute | solution.py:488
  66.0 1.1 %collective-permute-start.11 = (bf16[192,256]{1,0:T(8,128)(2,1)S(1)}, bf16[192,256]{1,0:T(8,128)(2,1)S(1)}, u32[]{:S(2)}, u32[]{:S(2)}) collective-permute-start(bf16[192,256]{1,0:T(8,128)(2,1)S(1)} %get-tuple-element.31), channel_id=1, source_target_pairs={{0,4},{1,5},{2,6},{3,7},{4,0},{5,1},{6,2},{7,3},{8,12},{9,13},{10,... | collective-permute-start | bytes 294920 | tf_op jit(solution)/shard_map/ppermute | solution.py:488
  67.1 1.5 %collective-permute-done.10.c_ref = bf16[192,256]{1,0:T(8,128)(2,1)S(1)} collective-permute-done((bf16[192,256]{1,0:T(8,128)(2,1)S(1)}, bf16[192,256]{1,0:T(8,128)(2,1)S(1)}, u32[]{:S(2)}, u32[]{:S(2)}) %collective-permute-start.10) | collective-permute-done | bytes 98336 | tf_op jit(solution)/shard_map/ppermute | solution.py:488
  68.6 2.4 %collective-permute-done.11.d_ref = bf16[192,256]{1,0:T(8,128)(2,1)S(1)} collective-permute-done((bf16[192,256]{1,0:T(8,128)(2,1)S(1)}, bf16[192,256]{1,0:T(8,128)(2,1)S(1)}, u32[]{:S(2)}, u32[]{:S(2)}) %collective-permute-start.11) | collective-permute-done | bytes 98336 | tf_op jit(solution)/shard_map/ppermute | solution.py:488
  71.0 2.8 %collective-permute-done.9.b_ref = bf16[192,256]{1,0:T(8,128)(2,1)S(1)} collective-permute-done((bf16[192,256]{1,0:T(8,128)(2,1)S(1)}, bf16[192,256]{1,0:T(8,128)(2,1)S(1)}, u32[]{:S(2)}, u32[]{:S(2)}) %collective-permute-start.9) | collective-permute-done | bytes 98336 | tf_op jit(solution)/shard_map/ppermute | solution.py:488
  73.8 0.8 shard_map.178
  74.7 8.5 %all-to-all-start.1 = ((bf16[32,16,128]{2,1,0:T(8,128)(2,1)}), bf16[32,16,128]{2,1,0:T(8,128)(2,1)S(1)}, u32[]{:S(2)}, u32[]{:S(2)}) async-start(bf16[32,16,128]{2,1,0:T(8,128)(2,1)} %bitcast.15), calls=%async_computation.1 | async-start | bytes 262144 | tf_op jit(solution)/shard_map/all_to_all | solution.py:530
  83.2 0.2 shard_map.174.mix_ref
  83.4 5.3 %all-to-all-done.1 = bf16[32,16,128]{2,1,0:T(8,128)(2,1)S(1)} async-done(((bf16[32,16,128]{2,1,0:T(8,128)(2,1)}), bf16[32,16,128]{2,1,0:T(8,128)(2,1)S(1)}, u32[]{:S(2)}, u32[]{:S(2)}) %all-to-all-start.1) | async-done | bytes 131104 | tf_op jit(solution)/shard_map/all_to_all | solution.py:530
  88.7 0.7 shard_map.179
  (23 shorter events, 0.1 us)
Async XLA Ops:
  0.0 18.3 %copy-start = (bf16[16,2048]{1,0:T(8,128)(2,1)S(1)}, bf16[16,2048]{1,0:T(8,128)(2,1)}, u32[]{:S(2)}) copy-start(bf16[16,2048]{1,0:T(8,128)(2,1)} %tok_ref.1) | copy-start | bytes 196612
  0.0 13.7 %copy-start.7 = (bf16[2048]{0:T(1024)(128)(2,1)S(1)}, bf16[2048]{0:T(1024)(128)(2,1)}, u32[]{:S(2)}) copy-start(bf16[2048]{0:T(1024)(128)(2,1)} %param.32) | copy-start | bytes 12292
  0.0 18.3 %copy-start.1 = (f32[2048]{0:T(1024)S(1)}, f32[2048]{0:T(1024)}, u32[]{:S(2)}) copy-start(f32[2048]{0:T(1024)} %param.26) | copy-start | bytes 24580
  0.0 29.7 %copy-start.6 = (bf16[32,2048]{1,0:T(8,128)(2,1)S(1)}, bf16[32,2048]{1,0:T(8,128)(2,1)}, u32[]{:S(2)}) copy-start(bf16[32,2048]{1,0:T(8,128)(2,1)} %param.33) | copy-start | bytes 393220
  0.0 29.7 %copy-start.5 = (bf16[32,2048]{1,0:T(8,128)(2,1)S(1)}, bf16[32,2048]{1,0:T(8,128)(2,1)}, u32[]{:S(2)}) copy-start(bf16[32,2048]{1,0:T(8,128)(2,1)} %param.34) | copy-start | bytes 393220
  0.0 29.7 %copy-start.4 = (bf16[32,2048]{1,0:T(8,128)(2,1)S(1)}, bf16[32,2048]{1,0:T(8,128)(2,1)}, u32[]{:S(2)}) copy-start(bf16[32,2048]{1,0:T(8,128)(2,1)} %param.35) | copy-start | bytes 393220
  6.7 4.2 %collective-permute-start = (bf16[16,2048]{1,0:T(8,128)(2,1)S(1)}, bf16[16,2048]{1,0:T(8,128)(2,1)S(1)}, u32[]{:S(2)}, u32[]{:S(2)}) collective-permute-start(bf16[16,2048]{1,0:T(8,128)(2,1)S(1)} %get-tuple-element.19), channel_id=1, source_target_pairs={{0,1},{1,0},{2,3},{3,2},{4,5},{5,4},{6,7},{7,6},{8,9},{9,8},{10,11... | collective-permute-start | bytes 196616 | tf_op jit(solution)/shard_map/ppermute | solution.py:507
  10.9 4.4 %collective-permute-start.1 = (bf16[16,2048]{1,0:T(8,128)(2,1)S(1)}, bf16[16,2048]{1,0:T(8,128)(2,1)S(1)}, u32[]{:S(2)}, u32[]{:S(2)}) collective-permute-start(bf16[16,2048]{1,0:T(8,128)(2,1)S(1)} %add_convert_fusion.a_ref), channel_id=1, source_target_pairs={{0,2},{1,3},{2,4},{3,5},{4,6},{5,7},{6,0},{7,1},{8,10},{9,11},{10,... | collective-permute-start | bytes 196616 | tf_op jit(solution)/shard_map/ppermute | solution.py:488
  11.0 4.7 %collective-permute-start.2 = (bf16[16,2048]{1,0:T(8,128)(2,1)S(1)}, bf16[16,2048]{1,0:T(8,128)(2,1)S(1)}, u32[]{:S(2)}, u32[]{:S(2)}) collective-permute-start(bf16[16,2048]{1,0:T(8,128)(2,1)S(1)} %add_convert_fusion.a_ref), channel_id=1, source_target_pairs={{0,6},{1,7},{2,0},{3,1},{4,2},{5,3},{6,4},{7,5},{8,14},{9,15},{10,... | collective-permute-start | bytes 196616 | tf_op jit(solution)/shard_map/ppermute | solution.py:488
  13.7 4.6 %collective-permute-start.3 = (bf16[16,2048]{1,0:T(8,128)(2,1)S(1)}, bf16[16,2048]{1,0:T(8,128)(2,1)S(1)}, u32[]{:S(2)}, u32[]{:S(2)}) collective-permute-start(bf16[16,2048]{1,0:T(8,128)(2,1)S(1)} %add_convert_fusion.a_ref), channel_id=1, source_target_pairs={{0,4},{1,5},{2,6},{3,7},{4,0},{5,1},{6,2},{7,3},{8,12},{9,13},{10,... | collective-permute-start | bytes 196616 | tf_op jit(solution)/shard_map/ppermute | solution.py:488
  19.4 28.5 %all-to-all-start = ((bf16[32,24,256]{2,1,0:T(8,128)(2,1)}), bf16[32,24,256]{2,1,0:T(8,128)(2,1)S(1)}, u32[]{:S(2)}, u32[]{:S(2)}) async-start(bf16[32,24,256]{2,1,0:T(8,128)(2,1)} %bitcast.7), calls=%async_computation | async-start | bytes 786432 | tf_op jit(solution)/shard_map/all_to_all | solution.py:514
  29.7 17.6 %collective-permute-start.5 = (bf16[3,32,2048]{2,1,0:T(8,128)(2,1)S(1)}, bf16[3,32,2048]{2,1,0:T(8,128)(2,1)S(1)}, u32[]{:S(2)}, u32[]{:S(2)}) collective-permute-start(bf16[3,32,2048]{2,1,0:T(8,128)(2,1)S(1)} %pad_maximum_fusion.rest_0_), channel_id=1, source_target_pairs={{0,32},{8,40},{16,48},{24,56},{32,0},{40,8},{48,16},{56,24},{64,96... | collective-permute-start | bytes 1179656 | tf_op jit(solution)/shard_map/ppermute | solution.py:501
  31.0 21.2 %collective-permute-start.6 = (bf16[3,32,2048]{2,1,0:T(8,128)(2,1)S(1)}, bf16[3,32,2048]{2,1,0:T(8,128)(2,1)S(1)}, u32[]{:S(2)}, u32[]{:S(2)}) collective-permute-start(bf16[3,32,2048]{2,1,0:T(8,128)(2,1)S(1)} %pad_maximum_fusion.rest_0_), channel_id=1, source_target_pairs={{0,8},{8,0},{16,24},{24,16},{32,40},{40,32},{48,56},{56,48},{64,72... | collective-permute-start | bytes 1179656 | tf_op jit(solution)/shard_map/ppermute | solution.py:502
  47.3 8.6 %collective-permute-start.7 = (bf16[3,32,2048]{2,1,0:T(8,128)(2,1)S(1)}, bf16[3,32,2048]{2,1,0:T(8,128)(2,1)S(1)}, u32[]{:S(2)}, u32[]{:S(2)}) collective-permute-start(bf16[3,32,2048]{2,1,0:T(8,128)(2,1)S(1)} %collective-permute-done.5.rest_1_), channel_id=1, source_target_pairs={{0,8},{8,0},{16,24},{24,16},{32,40},{40,32},{48,56},{56,48},{64,72... | collective-permute-start | bytes 1179656 | tf_op jit(solution)/shard_map/ppermute | solution.py:512
  48.0 8.0 %collective-permute-start.4 = (bf16[768,256]{1,0:T(8,128)(2,1)S(1)}, bf16[768,256]{1,0:T(8,128)(2,1)S(1)}, u32[]{:S(2)}, u32[]{:S(2)}) collective-permute-start(bf16[768,256]{1,0:T(8,128)(2,1)S(1)} %bitcast.17), channel_id=1, source_target_pairs={{0,1},{1,0},{2,3},{3,2},{4,5},{5,4},{6,7},{7,6},{8,9},{9,8},{10,11... | collective-permute-start | bytes 1179656 | tf_op jit(solution)/shard_map/ppermute | solution.py:522
  52.1 31.0 %copy-start.2 = (s32[16,2]{0,1:T(2,128)S(1)}, s32[16,2]{0,1:T(2,128)}, u32[]{:S(2)}) copy-start(s32[16,2]{0,1:T(2,128)} %param.27) | copy-start | bytes 388
  52.2 31.0 %copy-start.3 = (bf16[16,2]{0,1:T(2,128)(2,1)S(1)}, bf16[16,2]{0,1:T(2,128)(2,1)}, u32[]{:S(2)}) copy-start(bf16[16,2]{0,1:T(2,128)(2,1)} %param.28) | copy-start | bytes 196
  60.1 4.3 %collective-permute-start.8 = (bf16[192,1024]{1,0:T(8,128)(2,1)S(1)}, bf16[192,1024]{1,0:T(8,128)(2,1)S(1)}, u32[]{:S(2)}, u32[]{:S(2)}) collective-permute-start(bf16[192,1024]{1,0:T(8,128)(2,1)S(1)} %get-tuple-element.27), channel_id=1, source_target_pairs={{0,1},{1,0},{2,3},{3,2},{4,5},{5,4},{6,7},{7,6},{8,9},{9,8},{10,11... | collective-permute-start | bytes 1179656 | tf_op jit(solution)/shard_map/ppermute | solution.py:524
  64.5 4.1 %collective-permute-start.10 = (bf16[192,256]{1,0:T(8,128)(2,1)S(1)}, bf16[192,256]{1,0:T(8,128)(2,1)S(1)}, u32[]{:S(2)}, u32[]{:S(2)}) collective-permute-start(bf16[192,256]{1,0:T(8,128)(2,1)S(1)} %get-tuple-element.30), channel_id=1, source_target_pairs={{0,6},{1,7},{2,0},{3,1},{4,2},{5,3},{6,4},{7,5},{8,14},{9,15},{10,... | collective-permute-start | bytes 294920 | tf_op jit(solution)/shard_map/ppermute | solution.py:488
  66.0 5.0 %collective-permute-start.11 = (bf16[192,256]{1,0:T(8,128)(2,1)S(1)}, bf16[192,256]{1,0:T(8,128)(2,1)S(1)}, u32[]{:S(2)}, u32[]{:S(2)}) collective-permute-start(bf16[192,256]{1,0:T(8,128)(2,1)S(1)} %get-tuple-element.31), channel_id=1, source_target_pairs={{0,4},{1,5},{2,6},{3,7},{4,0},{5,1},{6,2},{7,3},{8,12},{9,13},{10,... | collective-permute-start | bytes 294920 | tf_op jit(solution)/shard_map/ppermute | solution.py:488
  67.1 6.8 %collective-permute-start.9 = (bf16[192,256]{1,0:T(8,128)(2,1)S(1)}, bf16[192,256]{1,0:T(8,128)(2,1)S(1)}, u32[]{:S(2)}, u32[]{:S(2)}) collective-permute-start(bf16[192,256]{1,0:T(8,128)(2,1)S(1)} %get-tuple-element.29), channel_id=1, source_target_pairs={{0,2},{1,3},{2,4},{3,5},{4,6},{5,7},{6,0},{7,1},{8,10},{9,11},{10,... | collective-permute-start | bytes 294920 | tf_op jit(solution)/shard_map/ppermute | solution.py:488
  74.7 14.1 %all-to-all-start.1 = ((bf16[32,16,128]{2,1,0:T(8,128)(2,1)}), bf16[32,16,128]{2,1,0:T(8,128)(2,1)S(1)}, u32[]{:S(2)}, u32[]{:S(2)}) async-start(bf16[32,16,128]{2,1,0:T(8,128)(2,1)} %bitcast.15), calls=%async_computation.1 | async-start | bytes 262144 | tf_op jit(solution)/shard_map/all_to_all | solution.py:530
